TPU v7x, 1024 devices: a whole 8x8x8 slice. The times are simulated.
1024 devices in a mesh: ep: 64 (over z, y), tp: 16 (over x, core).
Axes of the slice: x: 8, y: 8, z: 8, core: 2. Of those that a mesh axis runs over, the one named last changes fastest.
Arguments:
- tokens: bfloat16 [512, 2048], P('ep'), may hold values from -48 to 48
- past_lengths: int32 [512], P('ep'), may hold values from 1024 to 16383
- state: float32 [512, 16, 128, 256], P('ep', 'tp'), may hold values from -0.625 to 0.625
- norm1_gain: float32 [2048], replicated, may hold values from 0.1 to 1.9
- query_weight: bfloat16 [2048, 2048], P(None, 'tp'), may hold values from -0.125 to 0.125
- key_weight: bfloat16 [2048, 2048], P(None, 'tp'), may hold values from -0.125 to 0.125
- value_weight: bfloat16 [2048, 4096], P(None, 'tp'), may hold values from -0.125 to 0.125
- out_weight: bfloat16 [4096, 2048], P('tp'), may hold values from -0.09375 to 0.09375
- norm2_gain: float32 [2048], replicated, may hold values from 0.1 to 1.9
- branch_gate: float32 [2048], replicated, may hold values from -0.125 to 0.125
- route_ids: int32 [512, 2], P('ep'), may hold values from 0 to 15, all different within a row; in each aligned block of 8 rows (0 to 7, 8 to 15, ...) at most 2 rows name the same one
- route_weights: float32 [512, 2], P('ep'), may hold values from 0.2 to 1
- expert_gate: bfloat16 [64, 2048, 1792], P('ep', None, 'tp'), may hold values from -0.125 to 0.125
- expert_up: bfloat16 [64, 2048, 1792], P('ep', None, 'tp'), may hold values from -0.125 to 0.125
- expert_down: bfloat16 [64, 1792, 2048], P('ep', 'tp'), may hold values from -0.0625 to 0.0625
- dense_gate: bfloat16 [2048, 5632], P('tp', 'ep'), may hold values from -0.125 to 0.125
- dense_up: bfloat16 [2048, 5632], P('tp', 'ep'), may hold values from -0.125 to 0.125
- dense_down: bfloat16 [5632, 2048], P('ep', 'tp'), may hold values from -0.15625 to 0.15625
Outputs:
- layer_out: bfloat16 [512, 2048], P('ep', 'tp')
- new_state: float32 [512, 16, 128, 256], P('ep', 'tp')
Inputs may be any that keep to these rules, and one draw needn't show every extreme that they name: `route_ids`: in each aligned block of 8 rows no expert is named by more than 2 rows, and some block names one expert exactly 2 times.
All inputs are finite; a program needn't handle non-finite values.
Results may differ from a plain program's by a relative error of at most 0.006.
Values may be sent and summed in bfloat16 or wider, within the bound.
No kernel may reach another device: no remote copies, remote signals or barrier semaphores. Data moves between devices by JAX's collectives and lax.ppermute only.
A program may use at most 64 MiB of HBM per device.

v0:
```python
import jax
import jax.numpy as jnp
from jax import lax
from jax.sharding import PartitionSpec as P

RMS_EPSILON = 1e-06
GROUP_EPSILON = 1e-05
PRECISE = lax.Precision.HIGHEST


def in_blocks(x, dim, size):
    lengths = x.shape
    tiles = x.reshape(*lengths[:dim], size, lengths[dim] // size, *lengths[dim + 1 :])
    return jnp.moveaxis(tiles, dim, 0)


def sum_at_owner(x, axis, dim):
    size = lax.axis_size(axis)
    tiles = lax.all_to_all(in_blocks(x, dim, size), axis, 0, 0, tiled=True)
    return jnp.sum(tiles, axis=0)


def sent_to_all(x, axis):
    size = lax.axis_size(axis)
    return lax.all_to_all(jnp.broadcast_to(x[None], (size, *x.shape)), axis, 0, 0, tiled=True)


def over_copies(x, axis):
    everything = sent_to_all(x, axis)
    return jnp.sum(everything, axis=0)


def together(arrays, axis):
    ends = [0]
    for a in arrays:
        ends.append(ends[-1] + a.size)
    total = over_copies(jnp.concatenate([a.ravel() for a in arrays]), axis)
    return tuple((total[b:e].reshape(a.shape) for a, b, e in zip(arrays, ends, ends[1:])))


def sum_at_owner_2(x, axis, dim):
    size = lax.axis_size(axis)
    tiles = lax.all_to_all(in_blocks(x, dim, size), axis, 0, 0, tiled=True)
    return jnp.sum(tiles.astype(jnp.float32), axis=0)


def laid_out(tiles, dim):
    tiles = jnp.moveaxis(tiles, 0, dim)
    lengths = tiles.shape
    return tiles.reshape(*lengths[:dim], lengths[dim] * lengths[dim + 1], *lengths[dim + 2 :])


def collect(x, axis, dim):
    return laid_out(sent_to_all(x, axis), dim)


def over_pieces(x, axis):
    tiles = lax.all_gather(x, axis)
    return tiles.sum(axis=0)


def head_decay(head_index, head_total):
    return jnp.exp(
        jnp.log1p(-jnp.exp2(-5.0 - 7.0 * head_index.astype(jnp.float32) / (head_total - 1)))
    )


def rotate_heads(features, positions):
    half_size = features.shape[-1] // 2
    inverse = 10000.0 ** (-jnp.arange(half_size, dtype=jnp.float32) / half_size)
    angles = positions.astype(jnp.float32)[:, None] * inverse[None, :]
    cosine = jnp.cos(angles)[:, None, :]
    sine_part = jnp.sin(angles)[:, None, :]
    first_half = features[..., :half_size]
    second_half = features[..., half_size:]
    return jnp.concatenate(
        [
            first_half * cosine - second_half * sine_part,
            first_half * sine_part + second_half * cosine,
        ],
        axis=-1,
    )


def retention_step(
    normed_in, positions, state, query_weight, key_weight, value_weight, head_index, head_total
):
    row_count, head_count, key_size, value_size = state.shape
    query = jnp.dot(normed_in, query_weight, preferred_element_type=jnp.float32).reshape(
        row_count, head_count, key_size
    )
    keys = jnp.dot(normed_in, key_weight, preferred_element_type=jnp.float32).reshape(
        row_count, head_count, key_size
    )
    values = jnp.dot(normed_in, value_weight, preferred_element_type=jnp.float32).reshape(
        row_count, head_count, value_size
    )
    query = rotate_heads(query, positions)
    keys = rotate_heads(keys, positions) * key_size ** (-0.5)
    decay = head_decay(head_index, head_total)
    new_state = state * decay[None, :, None, None] + keys[:, :, :, None] * values[:, :, None, :]
    retained = jnp.einsum("shk,shkv->shv", query, new_state, precision=PRECISE)
    centered = retained - jnp.mean(retained, axis=-1, keepdims=True)
    normed = centered * lax.rsqrt(
        jnp.mean(centered * centered, axis=-1, keepdims=True) + GROUP_EPSILON
    )
    return (normed.astype(jnp.bfloat16).reshape(row_count, head_count * value_size), new_state)


def local(
    tokens,
    past_lengths,
    state,
    norm1_gain,
    query_weight,
    key_weight,
    value_weight,
    out_weight,
    norm2_gain,
    branch_gate,
    route_ids,
    route_weights,
    expert_gate,
    expert_up,
    expert_down,
    dense_gate,
    dense_up,
    dense_down,
):
    row_count = tokens.shape[0]
    model_width = tokens.shape[1]
    tp_count = lax.axis_size("tp")
    ep_count = lax.axis_size("ep")
    col_width = model_width // tp_count
    col_start = lax.axis_index("tp") * col_width
    heads_here = state.shape[1]
    head_index = lax.axis_index("tp") * heads_here + jnp.arange(heads_here)
    inputs = tokens.astype(jnp.float32)
    normed_in = (
        inputs
        * lax.rsqrt(jnp.mean(inputs * inputs, axis=-1, keepdims=True) + RMS_EPSILON)
        * norm1_gain
    ).astype(jnp.bfloat16)
    normed, new_state = retention_step(
        normed_in,
        past_lengths,
        state,
        query_weight,
        key_weight,
        value_weight,
        head_index,
        heads_here * tp_count,
    )
    partial_mix = jnp.dot(normed, out_weight, preferred_element_type=jnp.float32)
    gain_cols = lax.dynamic_slice_in_dim(norm2_gain, col_start, col_width, 0)
    gate_cols = lax.dynamic_slice_in_dim(branch_gate, col_start, col_width, 0)
    mix_cols = sum_at_owner(partial_mix, "tp", 1)
    mixed = lax.dynamic_slice_in_dim(inputs, col_start, col_width, 1) + mix_cols
    squares, along = together(
        (jnp.sum(mixed * mixed, axis=1), jnp.sum(mixed * gain_cols * gate_cols, axis=1)), "tp"
    )
    scale = lax.rsqrt(squares / model_width + RMS_EPSILON)[:, None]
    normed_cols = (mixed * scale * gain_cols).astype(jnp.bfloat16)
    branch_weight = jax.nn.sigmoid(scale * along[:, None])
    expert_count = ep_count // 4
    route_count = route_ids.shape[1]
    capacity = min(row_count, max(2, 2 * row_count * route_count // expert_count))
    route_flat = route_ids.reshape(-1)
    onehot = (route_flat[:, None] == jnp.arange(expert_count, dtype=jnp.int32)[None, :]).astype(
        jnp.int32
    )
    earlier = jnp.cumsum(onehot, axis=0) - onehot
    slot_index = jnp.sum(earlier * onehot, axis=1)
    target = route_flat * capacity + slot_index
    placed = (
        target[:, None] == jnp.arange(expert_count * capacity, dtype=jnp.int32)[None, :]
    ).astype(jnp.float32)
    placed = placed.reshape(row_count, route_count, expert_count * capacity)
    selector = jnp.sum(placed, axis=1).T.astype(jnp.bfloat16)
    combiner = jnp.sum(placed * route_weights[:, :, None], axis=1)
    full = lax.all_gather(normed_cols, "tp", axis=1, tiled=True)
    picked = jnp.dot(selector, full, preferred_element_type=jnp.float32).astype(jnp.bfloat16)
    outgoing = jnp.repeat(picked.reshape(expert_count, capacity, model_width), 4, axis=0)
    arrived = lax.all_to_all(outgoing, "ep", split_axis=0, concat_axis=0, tiled=True)
    expert_input = arrived.reshape(ep_count * capacity, model_width)
    gate_value = jnp.dot(expert_input, expert_gate[0], preferred_element_type=jnp.float32)
    up_value = jnp.dot(expert_input, expert_up[0], preferred_element_type=jnp.float32)
    expert_hidden = (jax.nn.silu(gate_value) * up_value).astype(jnp.bfloat16)
    expert_partial = jnp.dot(expert_hidden, expert_down[0], preferred_element_type=jnp.float32)
    expert_cols = sum_at_owner_2(expert_partial.astype(jnp.bfloat16), "tp", 1)
    returned = lax.all_to_all(
        expert_cols.reshape(ep_count, capacity, col_width).astype(jnp.bfloat16),
        "ep",
        split_axis=0,
        concat_axis=0,
        tiled=True,
    ).astype(jnp.float32)
    quarter_sum = jnp.sum(returned.reshape(expert_count, 4, capacity, col_width), axis=1).reshape(
        expert_count * capacity, col_width
    )
    routed = jnp.dot(combiner, quarter_sum, precision=PRECISE, preferred_element_type=jnp.float32)
    hidden_here = dense_gate.shape[1]
    dense_input = jnp.concatenate([dense_gate, dense_up], axis=1)
    partial_dense = jnp.dot(
        collect(normed_cols, "ep", 0), dense_input, preferred_element_type=jnp.float32
    )
    whole_dense = over_pieces(partial_dense, "tp")
    dense_hidden = (
        jax.nn.silu(whole_dense[:, :hidden_here]) * whole_dense[:, hidden_here:]
    ).astype(jnp.bfloat16)
    dense_result = sum_at_owner(
        jnp.dot(dense_hidden, dense_down, preferred_element_type=jnp.float32), "ep", 0
    )
    layer_out = (mixed + routed + branch_weight * dense_result).astype(jnp.bfloat16)
    return (layer_out, new_state)


def solution(mesh):
    return jax.shard_map(
        local,
        mesh=mesh,
        in_specs=(
            P("ep", None),
            P("ep"),
            P("ep", "tp", None, None),
            P(),
            P(None, "tp"),
            P(None, "tp"),
            P(None, "tp"),
            P("tp", None),
            P(),
            P(),
            P("ep", None),
            P("ep", None),
            P("ep", None, "tp"),
            P("ep", None, "tp"),
            P("ep", "tp", None),
            P("tp", "ep"),
            P("tp", "ep"),
            P("ep", "tp"),
        ),
        out_specs=(P("ep", "tp"), P("ep", "tp", None, None)),
        check_vma=False,
    )
```

profile of v0, /device:TPU:1, one launch (start us, length us, event | category | flops | bytes accessed | tf_op | source)
XLA Modules:
  0.0 196.0 jit_solution(4150879327566227816)
XLA Ops:
  7.3 1.0 multiply_reduce_fusion
  8.2 1.3 convolution_bitcast_fusion.2
  9.5 1.3 convolution_bitcast_fusion.3
  10.9 0.7 convert_element_type.55
  11.5 1.1 fusion.48
  13.0 1.4 multiply_add_fusion
  14.4 0.6 fusion.4
  15.4 1.5 copy.82
  16.9 1.0 convolution_bitcast_fusion.1
  17.9 17.4 %all-to-all-start = ((f32[16,8,128]{2,1,0:T(8,128)}), f32[16,8,128]{2,1,0:T(8,128)S(1)}, u32[]{:S(2)}, u32[]{:S(2)}) async-start(f32[16,8,128]{2,1,0:T(8,128)} %convolution_bitcast_fusion.1), calls=%async_computation | async-start | bytes 131072 | tf_op jit(solution)/shard_map/all_to_all | solution.py:19
  35.3 0.8 dynamic_slice.10
  36.1 0.8 dynamic_slice.11
  36.9 6.2 %all-to-all-done = f32[16,8,128]{2,1,0:T(8,128)S(1)} async-done(((f32[16,8,128]{2,1,0:T(8,128)}), f32[16,8,128]{2,1,0:T(8,128)S(1)}, u32[]{:S(2)}, u32[]{:S(2)}) %all-to-all-start) | async-done | bytes 65568 | tf_op jit(solution)/shard_map/all_to_all | solution.py:19
  43.3 9.6 %all_to_all.36 = f32[16,1,16]{2,1,0:T(1,128)S(1)} all-to-all(f32[16,1,16]{2,1,0:T(1,128)S(1)} %broadcast_in_dim.6), channel_id=1, replica_groups=mesh['ep'=64,'tp'=16] {'tp'}, dimensions={0} | all-to-all | bytes 2048 | tf_op jit(solution)/shard_map/all_to_all | solution.py:25
  53.2 25.2 %all_to_all.37 = bf16[64,8,128]{2,1,0:T(8,128)(2,1)S(1)} all-to-all(bf16[64,8,128]{2,1,0:T(8,128)(2,1)S(1)} %broadcast_in_dim.8), channel_id=1, replica_groups=mesh['ep'=64,'tp'=16] {'ep'}, dimensions={0} | all-to-all | bytes 262144 | tf_op jit(solution)/shard_map/all_to_all | solution.py:25
  78.4 0.9 fusion.12
  80.1 16.9 %all_gather.9 = bf16[8,2048]{1,0:T(8,128)(2,1)S(1)} all-gather(bf16[8,128]{1,0:T(8,128)(2,1)S(1)} %multiply_convert_fusion.2), channel_id=1, replica_groups=mesh['ep'=64,'tp'=16] {'tp'}, dimensions={1}, use_global_device_ids=true | all-gather | bytes 34816 | tf_op jit(solution)/shard_map/all_gather | solution.py:181
  97.0 0.2 convolution_convert_fusion.1
  97.3 0.3 broadcast_in_dim.7
  97.7 21.8 %all_to_all.38 = bf16[64,2,2048]{2,1,0:T(2,128)(2,1)S(1)} all-to-all(bf16[64,2,2048]{2,1,0:T(2,128)(2,1)S(1)} %bitcast.80), channel_id=1, replica_groups=mesh['ep'=64,'tp'=16] {'ep'}, dimensions={0} | all-to-all | bytes 1048576 | tf_op jit(solution)/shard_map/all_to_all | solution.py:184
  119.7 1.3 fusion.9
  121.0 2.0 %fusion = bf16[16,16,8,128]{3,2,1,0:T(8,128)(2,1)S(1)} fusion(bf16[128,2048]{1,0:T(8,128)(2,1)S(1)} %reshape.255, bf16[1,112,2048]{2,1,0:T(8,128)(2,1)} %param.32, bf16[1,2048,112]{1,2,0:T(8,128)(2,1)} %param.31, f32[128,112]{0,1:T(8,128)S(1)} %fusion.9), kind=kOutput, calls=%fused_computation.3 | convolution fusion | flops 117788672 | bytes 2023424 | tf_op jit(solution)/shard_map/dot_general | solution.py:189
  123.2 22.6 %all_to_all.39 = bf16[16,128,128]{2,1,0:T(8,128)(2,1)S(1)} all-to-all(bf16[16,128,128]{2,1,0:T(8,128)(2,1)S(1)} %bitcast.81), channel_id=1, replica_groups=mesh['ep'=64,'tp'=16] {'tp'}, dimensions={0} | all-to-all | bytes 1048576 | tf_op jit(solution)/shard_map/all_to_all | solution.py:43
  145.8 0.7 reduce_sum.142
  146.5 6.0 %all-to-all-start.4 = ((bf16[64,2,128]{2,1,0:T(2,128)(2,1)}), bf16[64,2,128]{2,1,0:T(2,128)(2,1)S(1)}, u32[]{:S(2)}, u32[]{:S(2)}) async-start(bf16[64,2,128]{2,1,0:T(2,128)(2,1)} %bitcast.19), calls=%async_computation.4 | async-start | bytes 65536 | tf_op jit(solution)/shard_map/all_to_all | solution.py:191
  152.5 7.5 %copy.85 = f32[22,8,16,512]{3,2,1,0:T(8,128)S(1)} copy(f32[22,8,16,512]{3,1,2,0:T(8,128)} %bitcast.78) | data formatting | bytes 11534336
  160.0 1.3 bitcast_reduce_fusion
  161.3 0.9 convolution_bitcast_fusion
  162.3 0.9 all-to-all-done.4
  163.2 11.1 %all-to-all-start.6 = ((f32[64,8,128]{2,1,0:T(8,128)}), f32[64,8,128]{2,1,0:T(8,128)S(1)}, u32[]{:S(2)}, u32[]{:S(2)}) async-start(f32[64,8,128]{2,1,0:T(8,128)} %convolution_bitcast_fusion), calls=%async_computation.6 | async-start | bytes 524288 | tf_op jit(solution)/shard_map/all_to_all | solution.py:19
  174.3 14.0 %all-to-all-done.6 = f32[64,8,128]{2,1,0:T(8,128)S(1)} async-done(((f32[64,8,128]{2,1,0:T(8,128)}), f32[64,8,128]{2,1,0:T(8,128)S(1)}, u32[]{:S(2)}, u32[]{:S(2)}) %all-to-all-start.6) | async-done | bytes 262176 | tf_op jit(solution)/shard_map/all_to_all | solution.py:19
  188.4 0.7 fusion.3
  (53 shorter events, 2.4 us)
Async XLA Ops:
  7.2 4.4 %copy-start = (bf16[2048,256]{1,0:T(8,128)(2,1)S(1)}, bf16[2048,256]{1,0:T(8,128)(2,1)}, u32[]{:S(2)}) copy-start(bf16[2048,256]{1,0:T(8,128)(2,1)} %param.24) | copy-start | bytes 3145732
  7.2 28.1 %copy-start.2 = (bf16[8,2048]{1,0:T(8,128)(2,1)S(1)}, bf16[8,2048]{1,0:T(8,128)(2,1)}, u32[]{:S(2)}) copy-start(bf16[8,2048]{1,0:T(8,128)(2,1)} %param.18) | copy-start | bytes 98308
  7.2 71.2 %copy-start.4 = (bf16[128,88]{0,1:T(8,128)(2,1)S(1)}, bf16[128,88]{0,1:T(8,128)(2,1)}, u32[]{:S(2)}) copy-start(bf16[128,88]{0,1:T(8,128)(2,1)} %param.33) | copy-start | bytes 67588
  7.2 71.2 %copy-start.3 = (bf16[128,88]{0,1:T(8,128)(2,1)S(1)}, bf16[128,88]{0,1:T(8,128)(2,1)}, u32[]{:S(2)}) copy-start(bf16[128,88]{0,1:T(8,128)(2,1)} %param.34) | copy-start | bytes 67588
  7.2 72.2 %copy-start.5 = (s32[8,2]{0,1:T(2,128)S(1)}, s32[8,2]{0,1:T(2,128)}, u32[]{:S(2)}) copy-start(s32[8,2]{0,1:T(2,128)} %param.28) | copy-start | bytes 196
  7.2 72.8 %copy-start.6 = (f32[8,2]{0,1:T(2,128)S(1)}, f32[8,2]{0,1:T(2,128)}, u32[]{:S(2)}) copy-start(f32[8,2]{0,1:T(2,128)} %param.29) | copy-start | bytes 196
  14.4 108.6 %copy-start.1 = (f32[8,1,128,256]{3,2,1,0:T(8,128)}, f32[8,1,128,256]{3,2,1,0:T(8,128)S(1)}, u32[]{:S(2)}) copy-start(f32[8,1,128,256]{3,2,1,0:T(8,128)S(1)} %multiply_add_fusion) | copy-start | bytes 3145732
  17.9 25.2 %all-to-all-start = ((f32[16,8,128]{2,1,0:T(8,128)}), f32[16,8,128]{2,1,0:T(8,128)S(1)}, u32[]{:S(2)}, u32[]{:S(2)}) async-start(f32[16,8,128]{2,1,0:T(8,128)} %convolution_bitcast_fusion.1), calls=%async_computation | async-start | bytes 131072 | tf_op jit(solution)/shard_map/all_to_all | solution.py:19
  35.3 117.2 %all-gather.3.cloned.1.call-start = ((), (), s32[]{:S(2)}) async-start(), calls=%async_computation.7 | async-start | bytes 6127616 | tf_op jit(solution)/shard_map/all_gather | solution.py:58
  146.5 16.7 %all-to-all-start.4 = ((bf16[64,2,128]{2,1,0:T(2,128)(2,1)}), bf16[64,2,128]{2,1,0:T(2,128)(2,1)S(1)}, u32[]{:S(2)}, u32[]{:S(2)}) async-start(bf16[64,2,128]{2,1,0:T(2,128)(2,1)} %bitcast.19), calls=%async_computation.4 | async-start | bytes 65536 | tf_op jit(solution)/shard_map/all_to_all | solution.py:191
  160.0 1.3 copy-start.7
  163.2 25.2 %all-to-all-start.6 = ((f32[64,8,128]{2,1,0:T(8,128)}), f32[64,8,128]{2,1,0:T(8,128)S(1)}, u32[]{:S(2)}, u32[]{:S(2)}) async-start(f32[64,8,128]{2,1,0:T(8,128)} %convolution_bitcast_fusion), calls=%async_computation.6 | async-start | bytes 524288 | tf_op jit(solution)/shard_map/all_to_all | solution.py:19
Sparse Core Ops, SparseCore 0:
  79.5 37.7 all-gather.2
where the time goes:
time: 197 us; the launch traced here: 196 us
  blocking collectives  96.2 us (49%)
  starting transfers between devices  34.5 us (18%)
  waiting for transfers between devices  21.2 us (11%)
  between operations  14.4 us (7%)
  local copies, waits for them, and re-layouts  11.7 us (6%)
  matrix products  11.4 us (6%)
  other arithmetic  6.54 us (3%)
    all_to_all x2, blocking collectives, sent_to_all(): lax.all_to_all(jnp.broadcast_to(x[None], (size, *x.shape)), axis, 0, 0, t...  34.9 us
    all_to_all x2, starting transfers between devices, sum_at_owner(): tiles = lax.all_to_all(in_blocks(x, dim, size), axis, 0, 0, tiled=True)  28.5 us
    all_to_all x1, blocking collectives, sum_at_owner_2(): tiles = lax.all_to_all(in_blocks(x, dim, size), axis, 0, 0, tiled=True)  22.6 us
    all_to_all x1, blocking collectives, local(): lax.all_to_all(outgoing, 'ep', split_axis=0, concat_axis=0, tiled=True)  21.8 us
    all_to_all x2, waiting for transfers between devices, sum_at_owner(): tiles = lax.all_to_all(in_blocks(x, dim, size), axis, 0, 0, tiled=True)  20.2 us
    all_gather x1, blocking collectives, local(): full = lax.all_gather(normed_cols, 'tp', axis=1, tiled=True)  16.9 us
    unnamed x18, local copies, waits for them, and re-layouts  7.63 us
    all_to_all x1, starting transfers between devices, local(): lax.all_to_all(expert_cols.reshape(ep_count, capacity, col_width).astype(...  6.02 us
  transfers between devices with their start and end apart: 4, of which 3 were waited for; matrix products, arithmetic and copies ran while one was open for 9% of the time, Pallas kernels for 0%

commit v1 on v0

v1 whole, which is shorter than its diff:
```python
import jax
import jax.numpy as jnp
from jax import lax
from jax.sharding import Mesh
from jax.sharding import PartitionSpec as P

RMS_EPSILON = 1e-06
GROUP_EPSILON = 1e-05
PRECISE = lax.Precision.HIGHEST
BF = jnp.bfloat16
F32 = jnp.float32
EP = ("z", "y")
TP = ("x", "c")


def head_decay(head_index, head_total):
    return jnp.exp(
        jnp.log1p(-jnp.exp2(-5.0 - 7.0 * head_index.astype(jnp.float32) / (head_total - 1)))
    )


def rotate_heads(features, positions):
    half_size = features.shape[-1] // 2
    inverse = 10000.0 ** (-jnp.arange(half_size, dtype=jnp.float32) / half_size)
    angles = positions.astype(jnp.float32)[:, None] * inverse[None, :]
    cosine = jnp.cos(angles)[:, None, :]
    sine_part = jnp.sin(angles)[:, None, :]
    first_half = features[..., :half_size]
    second_half = features[..., half_size:]
    return jnp.concatenate(
        [
            first_half * cosine - second_half * sine_part,
            first_half * sine_part + second_half * cosine,
        ],
        axis=-1,
    )


def retention_step(
    normed_in, positions, state, query_weight, key_weight, value_weight, head_index, head_total
):
    row_count, head_count, key_size, value_size = state.shape
    query = jnp.dot(normed_in, query_weight, preferred_element_type=jnp.float32).reshape(
        row_count, head_count, key_size
    )
    keys = jnp.dot(normed_in, key_weight, preferred_element_type=jnp.float32).reshape(
        row_count, head_count, key_size
    )
    values = jnp.dot(normed_in, value_weight, preferred_element_type=jnp.float32).reshape(
        row_count, head_count, value_size
    )
    query = rotate_heads(query, positions)
    keys = rotate_heads(keys, positions) * key_size ** (-0.5)
    decay = head_decay(head_index, head_total)
    new_state = state * decay[None, :, None, None] + keys[:, :, :, None] * values[:, :, None, :]
    retained = jnp.einsum("shk,shkv->shv", query, new_state, precision=PRECISE)
    centered = retained - jnp.mean(retained, axis=-1, keepdims=True)
    normed = centered * lax.rsqrt(
        jnp.mean(centered * centered, axis=-1, keepdims=True) + GROUP_EPSILON
    )
    return (normed.astype(jnp.bfloat16).reshape(row_count, head_count * value_size), new_state)


def padded_halves(w, size):
    return jnp.pad(w, ((0, 2 * size - w.shape[0]), (0, 0))).reshape(2, size, w.shape[1])


def local(
    tokens,
    past_lengths,
    state,
    norm1_gain,
    query_weight,
    key_weight,
    value_weight,
    out_weight,
    norm2_gain,
    branch_gate,
    route_ids,
    route_weights,
    expert_gate,
    expert_up,
    expert_down,
    dense_gate,
    dense_up,
    dense_down,
):
    rows, width = tokens.shape
    x_count = lax.axis_size("x")
    tp_count = 2 * x_count
    ep_count = lax.axis_size(EP)
    tp_index = lax.axis_index(TP)
    blocks = width // 128
    heads_here = state.shape[1]
    head_index = tp_index * heads_here + jnp.arange(heads_here)

    half = -(-dense_gate.shape[1] // 2 // 16) * 16
    part = jnp.concatenate(
        [padded_halves(dense_gate.T, half), padded_halves(dense_up.T, half), padded_halves(dense_down, half)],
        axis=1,
    )
    sent = jnp.broadcast_to(part[None], (x_count, *part.shape)).reshape(tp_count, 3 * half, 128)
    dense_parts = lax.all_to_all(sent, TP, 0, 0, tiled=True)

    inputs = tokens.astype(F32)
    normed_in = (
        inputs
        * lax.rsqrt(jnp.mean(inputs * inputs, axis=-1, keepdims=True) + RMS_EPSILON)
        * norm1_gain
    ).astype(BF)
    normed, new_state = retention_step(
        normed_in,
        past_lengths,
        state,
        query_weight,
        key_weight,
        value_weight,
        head_index,
        heads_here * tp_count,
    )
    partial_mix = jnp.dot(normed, out_weight, preferred_element_type=F32)
    other = lax.ppermute(partial_mix, "c", [(0, 1), (1, 0)])
    pair = (partial_mix + other).astype(BF)
    pair = pair.reshape(rows, blocks, 128).transpose(1, 0, 2).reshape(blocks * rows, 128)
    pairs = lax.all_to_all(
        jnp.broadcast_to(pair[None], (x_count, *pair.shape)), "x", 0, 0, tiled=True
    )
    mix = jnp.sum(pairs.astype(F32), axis=0).reshape(blocks, rows, 128)
    mixed = inputs.reshape(rows, blocks, 128).transpose(1, 0, 2) + mix
    scale = lax.rsqrt(jnp.sum(mixed * mixed, axis=(0, 2), keepdims=True) / width + RMS_EPSILON)
    scaled = mixed * scale * norm2_gain.reshape(blocks, 1, 128)
    branch = jax.nn.sigmoid(jnp.sum(scaled * branch_gate.reshape(blocks, 1, 128), axis=(0, 2)))
    normed_out = scaled.astype(BF).transpose(1, 0, 2).reshape(rows, width)

    expert_count = ep_count // 4
    route_count = route_ids.shape[1]
    route_flat = route_ids.reshape(-1)
    onehot = (route_flat[:, None] == jnp.arange(expert_count, dtype=jnp.int32)[None, :]).astype(
        jnp.int32
    )
    earlier = jnp.cumsum(onehot, axis=0) - onehot
    slot_index = jnp.sum(earlier * onehot, axis=1)
    row_number = jnp.arange(3 * ep_count, dtype=jnp.int32)
    row_expert = row_number // 3 // 4
    row_slot = row_number % 3
    hit = (route_flat[:, None] == row_expert[None, :]) & (slot_index[:, None] == row_slot[None, :])
    hit = hit.astype(F32).reshape(rows, route_count, 3 * ep_count)
    dense_row = (
        (jnp.arange(rows, dtype=jnp.int32)[:, None] == tp_index // 2) & (row_slot[None, :] == 2)
    ).astype(F32)
    selector = (jnp.sum(hit, axis=1) + dense_row).T.astype(BF)
    combiner = jnp.sum(hit * route_weights[:, :, None], axis=1) + dense_row * branch[:, None]

    outgoing = jnp.dot(selector, normed_out, preferred_element_type=F32).astype(BF)
    arrived = lax.all_to_all(
        outgoing.reshape(ep_count, 3 * blocks, 128), EP, 0, 0, tiled=True
    ).reshape(3 * ep_count, width)
    gate_value = jnp.dot(arrived, expert_gate[0], preferred_element_type=F32)
    up_value = jnp.dot(arrived, expert_up[0], preferred_element_type=F32)
    is_dense = (row_slot == 2)[:, None]
    hidden = jnp.where(is_dense, 0.0, jax.nn.silu(gate_value) * up_value).astype(BF)
    gate_t = dense_parts[:, :half].transpose(1, 0, 2).reshape(half, width)
    up_t = dense_parts[:, half : 2 * half].transpose(1, 0, 2).reshape(half, width)
    down = dense_parts[:, 2 * half :].transpose(1, 0, 2).reshape(half, width)
    across = (((1,), (1,)), ((), ()))
    dense_gate_value = lax.dot_general(arrived, gate_t, across, preferred_element_type=F32)
    dense_up_value = lax.dot_general(arrived, up_t, across, preferred_element_type=F32)
    dense_hidden = jnp.where(
        is_dense, jax.nn.silu(dense_gate_value) * dense_up_value, 0.0
    ).astype(BF)
    result = jnp.dot(hidden, expert_down[0], preferred_element_type=F32) + jnp.dot(
        dense_hidden, down, preferred_element_type=F32
    )
    returned = lax.all_to_all(
        result.astype(BF).reshape(ep_count, 3 * blocks, 128), EP, 0, 0, tiled=True
    ).reshape(3 * ep_count, width)
    total = jnp.dot(combiner, returned.astype(F32), precision=PRECISE, preferred_element_type=F32)
    total = total.reshape(rows, blocks, 128).transpose(1, 0, 2).astype(BF)
    sums = lax.all_to_all(total, TP, 0, 0, tiled=True)
    own = lax.dynamic_index_in_dim(mixed, tp_index, 0, keepdims=False)
    layer_out = (own + jnp.sum(sums.astype(F32), axis=0)).astype(BF)
    return (layer_out, new_state)


def solution(mesh):
    split = Mesh(mesh.devices.reshape(8, 8, 8, 2), ("z", "y", "x", "c"))
    return jax.shard_map(
        local,
        mesh=split,
        in_specs=(
            P(EP, None),
            P(EP),
            P(EP, TP, None, None),
            P(),
            P(None, TP),
            P(None, TP),
            P(None, TP),
            P(TP, None),
            P(),
            P(),
            P(EP, None),
            P(EP, None),
            P(EP, None, TP),
            P(EP, None, TP),
            P(EP, TP, None),
            P(TP, EP),
            P(TP, EP),
            P(EP, TP),
        ),
        out_specs=(P(EP, TP), P(EP, TP, None, None)),
        check_vma=False,
    )
```

time: 197 us -> 158 us (0.80)
  blocking collectives: 96.2 us -> 0 us
  waiting for transfers between devices: 21.2 us -> 81.8 us
  starting transfers between devices: 34.5 us -> 49 us
  between operations: 14.4 us -> 1.04 us
  local copies, waits for them, and re-layouts: 11.7 us -> 7.86 us
  other arithmetic: 6.54 us -> 3.94 us
    all_to_all x4 -> x0, blocking collectives: 79.3 us -> none  [the longest x2 34.9 us: sent_to_all(): lax.all_to_all(jnp.broadcast_to(x[None], (size, *x.shape)), axis, 0, 0, t...]
    all_to_all x3 -> x5, waiting for transfers between devices: 21.1 us -> 81.1 us  [the longest x1 22.8 us: local(): lax.all_to_all(outgoing.reshape(ep_count, 3 * blocks, 128), EP, 0, 0, til...]
    all_gather x1 -> x0, blocking collectives: 16.9 us -> none  [local(): full = lax.all_gather(normed_cols, 'tp', axis=1, tiled=True)]
    ppermute x0 -> x1, starting transfers between devices: none -> 16 us  [local(): other = lax.ppermute(partial_mix, 'c', [(0, 1), (1, 0)])]
    unnamed x18 -> x26, local copies, waits for them, and re-layouts: 7.63 us -> 1.87 us
    reshape x3 -> x4, local copies, waits for them, and re-layouts: 0.43 us -> 4.11 us  [the longest x1 2.21 us: local(): result.astype(BF).reshape(ep_count, 3 * blocks, 128)]
    all_to_all x3 -> x5, starting transfers between devices: 34.5 us -> 32.9 us  [the longest x1 13.7 us: local(): lax.all_to_all(outgoing.reshape(ep_count, 3 * blocks, 128), EP, 0, 0, til...]
  transfers between devices with their start and end apart: 4 -> 6, of which waited for: 3 -> 6; matrix products, arithmetic and copies ran while one was open for 9% -> 2% of each run, Pallas kernels for 0% -> 0%
where the time goes in v1:
time: 158 us; the launch traced here: 157 us
  waiting for transfers between devices  81.8 us (52%)
  starting transfers between devices  49 us (31%)
  matrix products  13.2 us (8%)
  local copies, waits for them, and re-layouts  7.86 us (5%)
  other arithmetic  3.94 us (2%)
    all_to_all x1, waiting for transfers between devices, local(): lax.all_to_all(outgoing.reshape(ep_count, 3 * blocks, 128), EP, 0, 0, til...  22.8 us
    all_to_all x1, waiting for transfers between devices, local(): lax.all_to_all(result.astype(BF).reshape(ep_count, 3 * blocks, 128), EP,...  22.4 us
    all_to_all x1, waiting for transfers between devices, local(): dense_parts = lax.all_to_all(sent, TP, 0, 0, tiled=True)  16.5 us
    ppermute x1, starting transfers between devices, local(): other = lax.ppermute(partial_mix, 'c', [(0, 1), (1, 0)])  16 us
    all_to_all x1, starting transfers between devices, local(): lax.all_to_all(outgoing.reshape(ep_count, 3 * blocks, 128), EP, 0, 0, til...  13.7 us
    all_to_all x1, waiting for transfers between devices, local(): lax.all_to_all(jnp.broadcast_to(pair[None], (x_count, *pair.shape)), 'x',...  11.9 us
    all_to_all x1, waiting for transfers between devices, local(): sums = lax.all_to_all(total, TP, 0, 0, tiled=True)  7.48 us
    all_to_all x1, starting transfers between devices, local(): lax.all_to_all(result.astype(BF).reshape(ep_count, 3 * blocks, 128), EP,...  6.16 us
  transfers between devices with their start and end apart: 6, of which 6 were waited for; matrix products, arithmetic and copies ran while one was open for 2% of the time, Pallas kernels for 0%

profile of v1, /device:TPU:1, one launch (start us, length us, event | category | flops | bytes accessed | tf_op | source)
XLA Modules:
  0.0 156.8 jit_solution(16640449308507881330)
XLA Ops:
  0.8 0.8 convert_element_type.72
  1.6 0.9 fusion.31
  2.5 1.3 convolution_bitcast_fusion
  3.9 1.3 convolution_bitcast_fusion.1
  5.2 1.6 fusion.89
  7.2 0.9 copy-done.1
  8.2 0.6 fusion.7
  9.4 16.0 %collective-permute-start = (f32[8,2048]{1,0:T(8,128)S(1)}, f32[8,2048]{1,0:T(8,128)S(1)}, u32[]{:S(2)}, u32[]{:S(2)}) collective-permute-start(f32[8,2048]{1,0:T(8,128)S(1)} %fusion.71), channel_id=1, source_target_pairs={{0,1},{1,0},{2,3},{3,2},{4,5},{5,4},{6,7},{7,6},{8,9},{9,8},{10,11... | collective-permute-start | bytes 196616 | tf_op jit(solution)/shard_map/ppermute | solution.py:122
  25.6 0.7 collective-permute-done
  26.3 0.7 broadcast_in_dim.23
  27.1 3.5 %all-to-all-start = ((bf16[8,128,128]{2,1,0:T(8,128)(2,1)}), bf16[8,128,128]{2,1,0:T(8,128)(2,1)S(1)}, u32[]{:S(2)}, u32[]{:S(2)}) async-start(bf16[8,128,128]{2,1,0:T(8,128)(2,1)} %broadcast_in_dim.23), calls=%async_computation | async-start | bytes 524288 | tf_op jit(solution)/shard_map/all_to_all | solution.py:125
  31.0 11.9 %all-to-all-done = bf16[8,128,128]{2,1,0:T(8,128)(2,1)S(1)} async-done(((bf16[8,128,128]{2,1,0:T(8,128)(2,1)}), bf16[8,128,128]{2,1,0:T(8,128)(2,1)S(1)}, u32[]{:S(2)}, u32[]{:S(2)}) %all-to-all-start) | async-done | bytes 262176 | tf_op jit(solution)/shard_map/all_to_all | solution.py:125
  42.9 0.9 broadcast_in_dim.27
  43.8 3.9 %all-to-all-start.2 = ((bf16[16,144,128]{2,1,0:T(8,128)(2,1)}), bf16[16,144,128]{2,1,0:T(8,128)(2,1)S(1)}, u32[]{:S(2)}, u32[]{:S(2)}) async-start(bf16[16,144,128]{2,1,0:T(8,128)(2,1)} %bitcast.30), calls=%async_computation.2 | async-start | bytes 1179648 | tf_op jit(solution)/shard_map/all_to_all | solution.py:103
  48.1 0.5 convolution_convert_fusion
  48.6 1.2 reshape.334
  49.8 16.5 %all-to-all-done.2 = bf16[16,144,128]{2,1,0:T(8,128)(2,1)S(1)} async-done(((bf16[16,144,128]{2,1,0:T(8,128)(2,1)}), bf16[16,144,128]{2,1,0:T(8,128)(2,1)S(1)}, u32[]{:S(2)}, u32[]{:S(2)}) %all-to-all-start.2) | async-done | bytes 589856 | tf_op jit(solution)/shard_map/all_to_all | solution.py:103
  66.3 13.7 %all-to-all-start.1 = ((bf16[64,48,128]{2,1,0:T(8,128)(2,1)}), bf16[64,48,128]{2,1,0:T(8,128)(2,1)S(1)}, u32[]{:S(2)}, u32[]{:S(2)}) async-start(bf16[64,48,128]{2,1,0:T(8,128)(2,1)} %reshape.334), calls=%async_computation.1 | async-start | bytes 1572864 | tf_op jit(solution)/shard_map/all_to_all | solution.py:155
  80.0 0.8 slice_bitcast_fusion.2
  80.8 22.8 %all-to-all-done.1 = bf16[64,48,128]{2,1,0:T(8,128)(2,1)S(1)} async-done(((bf16[64,48,128]{2,1,0:T(8,128)(2,1)}), bf16[64,48,128]{2,1,0:T(8,128)(2,1)S(1)}, u32[]{:S(2)}, u32[]{:S(2)}) %all-to-all-start.1) | async-done | bytes 786464 | tf_op jit(solution)/shard_map/all_to_all | solution.py:155
  103.6 0.3 reshape.335
  103.9 0.4 fusion.22
  104.3 1.0 fusion.14
  105.3 2.2 %fusion.3 = f32[192,2048]{1,0:T(8,128)S(1)} fusion(bf16[192,2048]{1,0:T(8,128)(2,1)S(1)} %reshape.335, bf16[1,112,2048]{2,1,0:T(8,128)(2,1)} %param.32, bf16[1,2048,112]{1,2,0:T(8,128)(2,1)} %param.31, f32[192,112]{1,0:T(8,128)} %fusion.14, pred[192]{0:T(512)(128)(4,1)S(1)} %broadcast_compare_fusion), kind=kOutput, calls=%fused_computation.6 | convolution fusion | flops 176311296 | bytes 3363008 | tf_op jit(solution)/shard_map/dot_general | solution.py:171
  107.6 3.0 %fusion = bf16[192,2048]{1,0:T(8,128)(2,1)} fusion(f32[192,2048]{1,0:T(8,128)S(1)} %fusion.3, bf16[192,2048]{1,0:T(8,128)(2,1)S(1)} %reshape.335, bf16[16,6,8,128]{3,2,1,0:T(8,128)(2,1)} %get-tuple-element.7, bf16[16,6,8,128]{3,2,1,0:T(8,128)(2,1)} %get-tuple-element.8, f32[192,48]{0,1:T(8,128)S(1)} %fusion.22, pred[192]{0:T(512)(128)(4,1)S(1)} %broadcast_compare_fusion), kind=kOutput, calls=%fused_computation.2 | convolution fusion | flops 76348416 | bytes 3576000 | tf_op jit(solution)/shard_map/dot_general | solution.py:171
  110.6 2.2 %reshape.343 = bf16[64,48,128]{2,1,0:T(8,128)(2,1)} reshape(bf16[192,2048]{1,0:T(8,128)(2,1)} %fusion) | data formatting | bytes 1572864 | tf_op jit(solution)/shard_map/reshape | solution.py:175
  112.8 6.2 %all-to-all-start.3 = ((bf16[64,48,128]{2,1,0:T(8,128)(2,1)}), bf16[64,48,128]{2,1,0:T(8,128)(2,1)S(1)}, u32[]{:S(2)}, u32[]{:S(2)}) async-start(bf16[64,48,128]{2,1,0:T(8,128)(2,1)} %reshape.343), calls=%async_computation.3 | async-start | bytes 1572864 | tf_op jit(solution)/shard_map/all_to_all | solution.py:174
  119.2 22.4 %all-to-all-done.3 = bf16[64,48,128]{2,1,0:T(8,128)(2,1)S(1)} async-done(((bf16[64,48,128]{2,1,0:T(8,128)(2,1)}), bf16[64,48,128]{2,1,0:T(8,128)(2,1)S(1)}, u32[]{:S(2)}, u32[]{:S(2)}) %all-to-all-start.3) | async-done | bytes 786464 | tf_op jit(solution)/shard_map/all_to_all | solution.py:174
  141.9 1.1 fusion.6
  142.9 5.7 %all-to-all-start.4 = ((bf16[16,8,128]{2,1,0:T(8,128)(2,1)}), bf16[16,8,128]{2,1,0:T(8,128)(2,1)S(1)}, u32[]{:S(2)}, u32[]{:S(2)}) async-start(bf16[16,8,128]{2,1,0:T(8,128)(2,1)} %fusion.6), calls=%async_computation.4 | async-start | bytes 65536 | tf_op jit(solution)/shard_map/all_to_all | solution.py:179
  148.7 7.5 %all-to-all-done.4 = bf16[16,8,128]{2,1,0:T(8,128)(2,1)S(1)} async-done(((bf16[16,8,128]{2,1,0:T(8,128)(2,1)}), bf16[16,8,128]{2,1,0:T(8,128)(2,1)S(1)}, u32[]{:S(2)}, u32[]{:S(2)}) %all-to-all-start.4) | async-done | bytes 32800 | tf_op jit(solution)/shard_map/all_to_all | solution.py:179
  156.2 0.6 fusion.73
  (57 shorter events, 2.6 us)
Async XLA Ops:
  0.6 8.5 %copy-start = (bf16[256,2048]{1,0:T(8,128)(2,1)S(1)}, bf16[256,2048]{1,0:T(8,128)(2,1)}, u32[]{:S(2)}) copy-start(bf16[256,2048]{1,0:T(8,128)(2,1)} %param.25) | copy-start | bytes 3145732
  0.6 6.3 %copy-start.2 = (f32[8,1,128,256]{3,2,1,0:T(8,128)S(1)}, f32[8,1,128,256]{3,2,1,0:T(8,128)}, u32[]{:S(2)}) copy-start(f32[8,1,128,256]{3,2,1,0:T(8,128)} %param.20) | copy-start | bytes 3145732
  7.2 1.0 copy-start.1
  7.2 18.2 %copy-start.10 = (s32[8,2]{0,1:T(2,128)S(1)}, s32[8,2]{0,1:T(2,128)}, u32[]{:S(2)}) copy-start(s32[8,2]{0,1:T(2,128)} %param.28) | copy-start | bytes 196
  8.2 22.5 %copy-start.6 = (bf16[128,88]{0,1:T(8,128)(2,1)S(1)}, bf16[128,88]{0,1:T(8,128)(2,1)}, u32[]{:S(2)}) copy-start(bf16[128,88]{0,1:T(8,128)(2,1)} %param.33) | copy-start | bytes 67588
  8.2 22.6 %copy-start.7 = (bf16[128,88]{0,1:T(8,128)(2,1)S(1)}, bf16[128,88]{0,1:T(8,128)(2,1)}, u32[]{:S(2)}) copy-start(bf16[128,88]{0,1:T(8,128)(2,1)} %param.34) | copy-start | bytes 67588
  8.2 22.6 %copy-start.8 = (bf16[88,128]{1,0:T(8,128)(2,1)S(1)}, bf16[88,128]{1,0:T(8,128)(2,1)}, u32[]{:S(2)}) copy-start(bf16[88,128]{1,0:T(8,128)(2,1)} %param.35) | copy-start | bytes 67588
  9.4 16.9 %collective-permute-start = (f32[8,2048]{1,0:T(8,128)S(1)}, f32[8,2048]{1,0:T(8,128)S(1)}, u32[]{:S(2)}, u32[]{:S(2)}) collective-permute-start(f32[8,2048]{1,0:T(8,128)S(1)} %fusion.71), channel_id=1, source_target_pairs={{0,1},{1,0},{2,3},{3,2},{4,5},{5,4},{6,7},{7,6},{8,9},{9,8},{10,11... | collective-permute-start | bytes 196616 | tf_op jit(solution)/shard_map/ppermute | solution.py:122
  25.6 22.2 %copy-start.11 = (f32[8,2]{0,1:T(2,128)S(1)}, f32[8,2]{0,1:T(2,128)}, u32[]{:S(2)}) copy-start(f32[8,2]{0,1:T(2,128)} %param.29) | copy-start | bytes 196
  27.1 20.9 %copy-start.3 = (bf16[8,2048]{1,0:T(8,128)(2,1)S(1)}, bf16[8,2048]{1,0:T(8,128)(2,1)}, u32[]{:S(2)}) copy-start(bf16[8,2048]{1,0:T(8,128)(2,1)} %param.18) | copy-start | bytes 98308
  27.1 21.0 %copy-start.5 = (f32[2048]{0:T(1024)S(1)}, f32[2048]{0:T(1024)}, u32[]{:S(2)}) copy-start(f32[2048]{0:T(1024)} %param.26) | copy-start | bytes 24580
  27.1 15.8 %all-to-all-start = ((bf16[8,128,128]{2,1,0:T(8,128)(2,1)}), bf16[8,128,128]{2,1,0:T(8,128)(2,1)S(1)}, u32[]{:S(2)}, u32[]{:S(2)}) async-start(bf16[8,128,128]{2,1,0:T(8,128)(2,1)} %broadcast_in_dim.23), calls=%async_computation | async-start | bytes 524288 | tf_op jit(solution)/shard_map/all_to_all | solution.py:125
  43.8 22.6 %all-to-all-start.2 = ((bf16[16,144,128]{2,1,0:T(8,128)(2,1)}), bf16[16,144,128]{2,1,0:T(8,128)(2,1)S(1)}, u32[]{:S(2)}, u32[]{:S(2)}) async-start(bf16[16,144,128]{2,1,0:T(8,128)(2,1)} %bitcast.30), calls=%async_computation.2 | async-start | bytes 1179648 | tf_op jit(solution)/shard_map/all_to_all | solution.py:103
  66.3 37.3 %all-to-all-start.1 = ((bf16[64,48,128]{2,1,0:T(8,128)(2,1)}), bf16[64,48,128]{2,1,0:T(8,128)(2,1)S(1)}, u32[]{:S(2)}, u32[]{:S(2)}) async-start(bf16[64,48,128]{2,1,0:T(8,128)(2,1)} %reshape.334), calls=%async_computation.1 | async-start | bytes 1572864 | tf_op jit(solution)/shard_map/all_to_all | solution.py:155
  80.8 23.5 %copy-start.4 = (bf16[1,2048,112]{1,2,0:T(8,128)(2,1)S(1)}, bf16[1,2048,112]{1,2,0:T(8,128)(2,1)}, u32[]{:S(2)}) copy-start(bf16[1,2048,112]{1,2,0:T(8,128)(2,1)} %param.30) | copy-start | bytes 1376260
  110.6 8.4 %copy-start.9 = (f32[2048]{0:T(1024)S(1)}, f32[2048]{0:T(1024)}, u32[]{:S(2)}) copy-start(f32[2048]{0:T(1024)} %param.27) | copy-start | bytes 24580
  112.8 28.8 %all-to-all-start.3 = ((bf16[64,48,128]{2,1,0:T(8,128)(2,1)}), bf16[64,48,128]{2,1,0:T(8,128)(2,1)S(1)}, u32[]{:S(2)}, u32[]{:S(2)}) async-start(bf16[64,48,128]{2,1,0:T(8,128)(2,1)} %reshape.343), calls=%async_computation.3 | async-start | bytes 1572864 | tf_op jit(solution)/shard_map/all_to_all | solution.py:174
  142.9 13.2 %all-to-all-start.4 = ((bf16[16,8,128]{2,1,0:T(8,128)(2,1)}), bf16[16,8,128]{2,1,0:T(8,128)(2,1)S(1)}, u32[]{:S(2)}, u32[]{:S(2)}) async-start(bf16[16,8,128]{2,1,0:T(8,128)(2,1)} %fusion.6), calls=%async_computation.4 | async-start | bytes 65536 | tf_op jit(solution)/shard_map/all_to_all | solution.py:179

commit v2 on v1

v2 whole, which is shorter than its diff:
```python
import jax
import jax.numpy as jnp
from jax import lax
from jax.experimental import pallas as pl
from jax.experimental.pallas import tpu as pltpu
from jax.sharding import Mesh
from jax.sharding import PartitionSpec as P

RMS_EPSILON = 1e-06
GROUP_EPSILON = 1e-05
BF = jnp.bfloat16
F32 = jnp.float32
EP = ("z", "y")
TP = ("x", "c")
NT = (((1,), (1,)), ((), ()))


def padded_halves(w, size):
    return jnp.pad(w, ((0, 2 * size - w.shape[0]), (0, 0))).reshape(2, size, w.shape[1])


def call(kernel, out_shape, args, flops, scratch=(), specs=None, out_specs=None, vmem=None):
    full = pl.BlockSpec(memory_space=pltpu.VMEM)
    size = sum(a.size * a.dtype.itemsize for a in args)
    return pl.pallas_call(
        kernel,
        out_shape=out_shape,
        in_specs=specs or [full] * len(args),
        out_specs=out_specs or jax.tree.map(lambda _: full, out_shape),
        scratch_shapes=list(scratch),
        compiler_params=pltpu.CompilerParams(vmem_limit_bytes=vmem or 16 << 20),
        cost_estimate=pl.CostEstimate(flops=flops, bytes_accessed=size, transcendentals=0),
    )(*args)


def retention_kernel(
    core_ref,
    tokens_ref,
    gain_ref,
    cos_ref,
    sin_ref,
    decay_ref,
    q_hbm,
    k_hbm,
    v_hbm,
    state_hbm,
    out_hbm,
    keep_ref,
    give_ref,
    new_hbm,
    q_w,
    k_w,
    v_w,
    state,
    out_w,
    fresh,
    sems,
):
    rows, width = tokens_ref.shape
    copies = [
        pltpu.make_async_copy(s, d, sems.at[n])
        for n, (s, d) in enumerate(
            ((q_hbm, q_w), (k_hbm, k_w), (v_hbm, v_w), (state_hbm, state), (out_hbm, out_w))
        )
    ]
    for c in copies:
        c.start()
    x = tokens_ref[...].astype(F32)
    inv = lax.rsqrt(jnp.sum(x * x, axis=1, keepdims=True) / width + RMS_EPSILON)
    normed_in = (x * inv * gain_ref[...]).astype(BF)

    def project(n, w):
        copies[n].wait()
        return jnp.dot(normed_in, w[...], preferred_element_type=F32)

    def rotated(v):
        return v * cos_ref[...] + pltpu.roll(v, v.shape[1] // 2, 1) * sin_ref[...]

    query = rotated(project(0, q_w))
    keys = rotated(project(1, k_w)) * q_w.shape[1] ** (-0.5)
    values = project(2, v_w)
    query_t = query.T
    keys_t = keys.T
    copies[3].wait()
    decay = decay_ref[0]
    retained = []
    for i in range(rows):
        new = state[i] * decay + keys_t[:, i : i + 1] * values[i : i + 1, :]
        fresh[i] = new
        retained.append(jnp.sum(query_t[:, i : i + 1] * new, axis=0, keepdims=True))
    back = pltpu.make_async_copy(fresh, new_hbm, sems.at[5])
    back.start()
    retained = jnp.concatenate(retained, axis=0)
    centered = retained - jnp.mean(retained, axis=1, keepdims=True)
    normed = centered * lax.rsqrt(
        jnp.mean(centered * centered, axis=1, keepdims=True) + GROUP_EPSILON
    )
    normed = normed.astype(BF)
    copies[4].wait()
    mix = jnp.dot(normed, out_w[...], preferred_element_type=F32)
    for j in range(width // 128):
        keep_ref[j] = mix[:, 128 * j : 128 * j + 128]
        give_ref[j] = mix[:, 128 * j : 128 * j + 128].astype(BF)
    back.wait()


def dispatch_kernel(
    core_ref, pairs_ref, tokens_ref, gain_ref, gate_ref, select_ref, sent_ref, own_ref, branch_ref, held
):
    rows, width = tokens_ref.shape
    blocks = width // 128
    square = jnp.zeros((rows, 128), F32)
    for j in range(blocks):
        m = tokens_ref[:, 128 * j : 128 * j + 128].astype(F32)
        for p in range(pairs_ref.shape[0]):
            m = m + pairs_ref[p, j].astype(F32)
        held[j] = m
        square = square + m * m
    scale = lax.rsqrt(jnp.sum(square, axis=1, keepdims=True) / width + RMS_EPSILON)
    along = jnp.zeros((rows, 128), F32)
    for j in range(blocks):
        along = along + held[j] * scale * gain_ref[j : j + 1, :] * gate_ref[j : j + 1, :]
    branch_ref[...] = jax.nn.sigmoid(
        jnp.broadcast_to(jnp.sum(along, axis=1, keepdims=True), (rows, 128))
    )
    core = core_ref[1]
    own_ref[...] = held[core_ref[0]]
    mine = [
        held[2 * k + core] * scale * gain_ref[pl.ds(2 * k + core, 1), :] for k in range(blocks // 2)
    ]
    mine = jnp.concatenate(mine, axis=0).astype(BF)
    sent_ref[...] = jnp.dot(select_ref[...], mine, preferred_element_type=F32).astype(BF)


def expert_kernel(
    core_ref,
    mine_ref,
    other_ref,
    gate_ref,
    up_ref,
    down_ref,
    dense_ref,
    keep_ref,
    give_ref,
):
    count, half_width = mine_ref.shape
    half = dense_ref.shape[1] // 3
    core = core_ref[1]
    wide = gate_ref.shape[0]
    gate = jnp.zeros((count, wide), F32)
    up = jnp.zeros((count, wide), F32)
    dense = jnp.zeros((count, 2 * half), F32)
    for ref, parity in ((mine_ref, core), (other_ref, 1 - core)):
        for k in range(half_width // 128):
            x = ref[:, 128 * k : 128 * k + 128]
            at = pl.ds(pl.multiple_of((2 * k + parity) * 128, 128), 128)
            gate = gate + lax.dot_general(x, gate_ref[:, at], NT, preferred_element_type=F32)
            up = up + lax.dot_general(x, up_ref[:, at], NT, preferred_element_type=F32)
            dense = dense + lax.dot_general(
                x, dense_ref[2 * k + parity, : 2 * half, :], NT, preferred_element_type=F32
            )
    is_dense = lax.broadcasted_iota(jnp.int32, (count, 1), 0) % 3 == 2
    hidden = (gate / (1.0 + jnp.exp(-gate))) * up
    hidden = jnp.where(is_dense, 0.0, hidden).astype(BF)
    dgate = dense[:, :half]
    dense_hidden = (dgate / (1.0 + jnp.exp(-dgate))) * dense[:, half:]
    dense_hidden = jnp.where(is_dense, dense_hidden, 0.0).astype(BF)
    for out, parity in ((keep_ref, core), (give_ref, 1 - core)):
        for k in range(half_width // 128):
            at = pl.ds(pl.multiple_of((2 * k + parity) * 128, 128), 128)
            r = jnp.dot(hidden, down_ref[:, at], preferred_element_type=F32)
            r = r + jnp.dot(
                dense_hidden, dense_ref[2 * k + parity, 2 * half :, :], preferred_element_type=F32
            )
            out[:, 128 * k : 128 * k + 128] = r.astype(out.dtype)


def combine_kernel(high_ref, low_ref, back_ref, out_ref):
    back = back_ref[...]
    out_ref[...] = (
        jnp.dot(high_ref[...], back, preferred_element_type=F32)
        + jnp.dot(low_ref[...], back, preferred_element_type=F32)
    ).astype(BF)


def swap(x):
    return lax.ppermute(x, "c", [(0, 1), (1, 0)])


def local(
    tokens,
    past_lengths,
    state,
    norm1_gain,
    query_weight,
    key_weight,
    value_weight,
    out_weight,
    norm2_gain,
    branch_gate,
    route_ids,
    route_weights,
    expert_gate,
    expert_up,
    expert_down,
    dense_gate,
    dense_up,
    dense_down,
):
    rows, width = tokens.shape
    x_count = lax.axis_size("x")
    tp_count = 2 * x_count
    ep_count = lax.axis_size(EP)
    x_index = lax.axis_index("x")
    tp_index = lax.axis_index(TP)
    blocks = width // 128
    key_size = query_weight.shape[1]
    value_size = value_weight.shape[1]
    place = jnp.stack([tp_index, lax.axis_index("c")]).astype(jnp.int32)
    smem = pl.BlockSpec(memory_space=pltpu.SMEM)
    vmem = pl.BlockSpec(memory_space=pltpu.VMEM)
    hbm = pl.BlockSpec(memory_space=pltpu.HBM)

    half = -(-dense_gate.shape[1] // 2 // 16) * 16
    part = jnp.concatenate(
        [
            padded_halves(dense_gate.T, half),
            padded_halves(dense_up.T, half),
            padded_halves(dense_down, half),
        ],
        axis=1,
    )
    sent = jnp.broadcast_to(part[None], (x_count, *part.shape)).reshape(tp_count, 3 * half, 128)
    dense_parts = lax.all_to_all(sent, TP, 0, 0, tiled=True)

    inverse = 10000.0 ** (-jnp.arange(key_size // 2, dtype=F32) / (key_size // 2))
    angles = past_lengths.astype(F32)[:, None] * inverse[None, :]
    cosine, sine = jnp.cos(angles), jnp.sin(angles)
    cosine = jnp.concatenate([cosine, cosine], axis=1)
    sine = jnp.concatenate([-sine, sine], axis=1)
    decay = jnp.exp(jnp.log1p(-jnp.exp2(-5.0 - 7.0 * tp_index.astype(F32) / (tp_count - 1))))
    args = (
        place,
        tokens,
        norm1_gain.reshape(1, width),
        cosine,
        sine,
        decay.reshape(1),
        query_weight,
        key_weight,
        value_weight,
        state.reshape(rows, key_size, value_size),
        out_weight,
    )
    keep, give, new_state = call(
        retention_kernel,
        (
            jax.ShapeDtypeStruct((blocks, rows, 128), F32),
            jax.ShapeDtypeStruct((blocks, rows, 128), BF),
            jax.ShapeDtypeStruct((rows, key_size, value_size), F32),
        ),
        args,
        10_000_000_000,
        scratch=(
            pltpu.VMEM(query_weight.shape, BF),
            pltpu.VMEM(key_weight.shape, BF),
            pltpu.VMEM(value_weight.shape, BF),
            pltpu.VMEM((rows, key_size, value_size), F32),
            pltpu.VMEM(out_weight.shape, BF),
            pltpu.VMEM((rows, key_size, value_size), F32),
            pltpu.SemaphoreType.DMA((6,)),
        ),
        specs=[smem, vmem, vmem, vmem, vmem, smem, hbm, hbm, hbm, hbm, hbm],
        out_specs=(vmem, vmem, hbm),
        vmem=61 << 20,
    )
    pair = (keep + swap(give).astype(F32)).astype(BF)
    pairs = lax.all_to_all(
        jnp.broadcast_to(pair[None], (x_count, *pair.shape)), "x", 0, 0, tiled=True
    )

    route_count = route_ids.shape[1]
    route_flat = route_ids.reshape(-1)
    same = (route_flat[:, None] == route_flat[None, :]).astype(jnp.int32)
    number = jnp.arange(rows * route_count, dtype=jnp.int32)
    slot_index = jnp.sum(same * (number[None, :] < number[:, None]), axis=1)
    place_of = jnp.where(slot_index < 2, route_flat * 3 + slot_index, -1)
    in_row = lax.broadcasted_iota(jnp.int32, (3 * ep_count, 1), 0)
    row_kind = (in_row // 12) * 3 + in_row % 3
    hit = (row_kind == place_of[None, :]).astype(F32).reshape(3 * ep_count, rows, route_count)
    dense_row = (
        (jnp.arange(rows, dtype=jnp.int32)[None, :] == x_index) & (in_row % 3 == 2)
    ).astype(F32)
    chosen = jnp.sum(hit, axis=2) + dense_row
    weighted = jnp.sum(hit * route_weights[None], axis=2)
    ones = jnp.eye(blocks // 2, dtype=F32)
    select = (chosen[:, None, None, :] * ones[None, :, :, None]).astype(BF)
    select = select.reshape(3 * ep_count * blocks // 2, blocks // 2 * rows)

    args = (
        place,
        pairs,
        tokens,
        norm2_gain.reshape(blocks, 128),
        branch_gate.reshape(blocks, 128),
        select,
    )
    outgoing, own, branch = call(
        dispatch_kernel,
        (
            jax.ShapeDtypeStruct((select.shape[0], 128), BF),
            jax.ShapeDtypeStruct((rows, 128), F32),
            jax.ShapeDtypeStruct((rows, 128), F32),
        ),
        args,
        1_000_000_000,
        specs=[smem] + [vmem] * 5,
        scratch=(pltpu.VMEM((blocks, rows, 128), F32),),
    )
    arrived = lax.all_to_all(outgoing.reshape(ep_count, 3 * blocks // 2, 128), EP, 0, 0, tiled=True)
    mine = arrived.reshape(3 * ep_count, width // 2)
    other = swap(mine)
    args = (
        place,
        mine,
        other,
        expert_gate[0].T,
        expert_up[0].T,
        expert_down[0],
        dense_parts,
    )
    shape = (3 * ep_count, width // 2)
    stay, leave = call(
        expert_kernel,
        (jax.ShapeDtypeStruct(shape, F32), jax.ShapeDtypeStruct(shape, BF)),
        args,
        2_000_000_000,
        specs=[smem] + [vmem] * 6,
    )
    result = (stay + swap(leave).astype(F32)).astype(BF)
    returned = lax.all_to_all(result.reshape(ep_count, 3 * blocks // 2, 128), EP, 0, 0, tiled=True)
    combiner = weighted + dense_row * branch[:, 0][None, :]
    spread = combiner.T[None, :, :, None] * ones[:, None, None, :]
    spread = spread.reshape(blocks // 2 * rows, 3 * ep_count * blocks // 2)
    high = lax.reduce_precision(spread, 8, 7)
    low = (spread - high).astype(BF)
    total = call(
        combine_kernel,
        jax.ShapeDtypeStruct((blocks // 2 * rows, 128), BF),
        (high.astype(BF), low, returned.reshape(3 * ep_count * blocks // 2, 128)),
        100_000_000,
    )
    sums = lax.all_to_all(total.reshape(x_count, rows, 128), "x", 0, 0, tiled=True)
    layer_out = (own + jnp.sum(sums.astype(F32), axis=0)).astype(BF)
    return (layer_out, new_state.reshape(state.shape))


def solution(mesh):
    split = Mesh(mesh.devices.reshape(8, 8, 8, 2), ("z", "y", "x", "c"))
    return jax.shard_map(
        local,
        mesh=split,
        in_specs=(
            P(EP, None),
            P(EP),
            P(EP, TP, None, None),
            P(),
            P(None, TP),
            P(None, TP),
            P(None, TP),
            P(TP, None),
            P(),
            P(),
            P(EP, None),
            P(EP, None),
            P(EP, None, TP),
            P(EP, None, TP),
            P(EP, TP, None),
            P(TP, EP),
            P(TP, EP),
            P(EP, TP),
        ),
        out_specs=(P(EP, TP), P(EP, TP, None, None)),
        check_vma=False,
    )
```

time: 158 us -> 138 us (0.87)
  waiting for transfers between devices: 81.8 us -> 43 us
  matrix products: 13.2 us -> 0 us
  Pallas kernels: 0 us -> 9.15 us
  blocking collectives: 0 us -> 8.98 us
  local copies, waits for them, and re-layouts: 7.86 us -> 14.1 us
  other arithmetic: 3.94 us -> 10.1 us
    all_to_all x3 -> x2, waiting for transfers between devices: 52.7 us -> 20.8 us  [the longest x1 13.9 us: local(): lax.all_to_all(outgoing.reshape(ep_count, 3 * blocks // 2, 128), EP, 0, 0...]
    dot_general x11 -> x0, matrix products: 13.2 us -> none  [the longest x1 3.01 us: local(): jnp.dot(dense_hidden, down, preferred_element_type=F32)]
    pallas_call x0 -> x4, Pallas kernels: none -> 9.15 us  [call(): pl.pallas_call(kernel, out_shape=out_shape, in_specs=specs or [full] * le...]
    all_to_all x0 -> x1, blocking collectives: none -> 8.98 us  [local(): lax.all_to_all(total.reshape(x_count, rows, 128), 'x', 0, 0, tiled=True)]
    all_to_all x3 -> x2, starting transfers between devices: 25.5 us -> 17.3 us  [the longest x1 12.5 us: local(): lax.all_to_all(outgoing.reshape(ep_count, 3 * blocks // 2, 128), EP, 0, 0...]
    all_to_all x1, waiting for transfers between devices: 11.9 us -> 4.1 us  [local(): lax.all_to_all(jnp.broadcast_to(pair[None], (x_count, *pair.shape)), 'x',...]
    convert_element_type x0 -> x3, local copies, waits for them, and re-layouts: none -> 5.65 us  [the longest x2 5.58 us: local(): select = (chosen[:, None, None, :] * ones[None, :, :, None]).astype(BF)]
    mul x0 -> x1, local copies, waits for them, and re-layouts: none -> 5.24 us  [local(): spread = combiner.T[None, :, :, None] * ones[:, None, None, :]]
  transfers between devices with their start and end apart: 6 -> 7, of which waited for: 6 -> 6; matrix products, arithmetic and copies ran while one was open for 2% -> 13% of each run, Pallas kernels for 0% -> 0%
where the time goes in v2:
time: 138 us; the launch traced here: 135 us
  starting transfers between devices  48.9 us (35%)
  waiting for transfers between devices  43 us (31%)
  local copies, waits for them, and re-layouts  14.1 us (10%)
  other arithmetic  10.1 us (7%)
  Pallas kernels  9.15 us (7%)
  blocking collectives  8.98 us (7%)
    ppermute x3, starting transfers between devices, swap(): return lax.ppermute(x, 'c', [(0, 1), (1, 0)])  20 us
    all_to_all x1, waiting for transfers between devices, local(): dense_parts = lax.all_to_all(sent, TP, 0, 0, tiled=True)  16.3 us
    all_to_all x1, waiting for transfers between devices, local(): lax.all_to_all(outgoing.reshape(ep_count, 3 * blocks // 2, 128), EP, 0, 0...  13.9 us
    all_to_all x1, starting transfers between devices, local(): lax.all_to_all(outgoing.reshape(ep_count, 3 * blocks // 2, 128), EP, 0, 0...  12.5 us
    pallas_call x4, Pallas kernels, call(): pl.pallas_call(kernel, out_shape=out_shape, in_specs=specs or [full] * le...  9.15 us
    all_to_all x1, blocking collectives, local(): lax.all_to_all(total.reshape(x_count, rows, 128), 'x', 0, 0, tiled=True)  8.98 us
    all_to_all x1, starting transfers between devices, local(): dense_parts = lax.all_to_all(sent, TP, 0, 0, tiled=True)  8.26 us
    all_to_all x1, waiting for transfers between devices, local(): lax.all_to_all(result.reshape(ep_count, 3 * blocks // 2, 128), EP, 0, 0,...  6.89 us
  transfers between devices with their start and end apart: 7, of which 6 were waited for; matrix products, arithmetic and copies ran while one was open for 13% of the time, Pallas kernels for 0%

profile of v2, /device:TPU:1, one launch (start us, length us, event | category | flops | bytes accessed | tf_op | source)
XLA Modules:
  0.0 135.4 jit_solution(7930821284502548797)
XLA Ops:
  0.8 0.7 convert_element_type.69
  1.4 0.6 pad_add_fusion.core_ref
  2.1 0.7 pad_maximum_fusion.1
  2.8 4.8 %shard_map.185 = (f32[16,8,128]{2,1,0:T(8,128)}, bf16[16,8,128]{2,1,0:T(8,128)(2,1)}, f32[8,128,256]{2,1,0:T(8,128)}) custom-call(s32[2]{0:T(128)} %pad_add_fusion.core_ref, bf16[8,2048]{1,0:T(8,128)(2,1)} %tokens_ref.3, f32[1,2048]{1,0:T(1,128)} %bitcast.47, f32[8,128]{1,0:T(8,128)} %get-tuple-element.31.cos_ref, f32[8,128]{1,0:T(8,128)} %get-tuple-element.32.sin_ref, ...), custom_call_target="tpu_custom_call" | custom-call | flops 10000000000 | bytes 4243468 | tf_op jit(solution)/shard_map/pallas_call | solution.py:25
  7.7 16.0 %collective-permute-start = (bf16[16,8,128]{2,1,0:T(8,128)(2,1)}, bf16[16,8,128]{2,1,0:T(8,128)(2,1)S(1)}, u32[]{:S(2)}, u32[]{:S(2)}) collective-permute-start(bf16[16,8,128]{2,1,0:T(8,128)(2,1)} %get-tuple-element.11), channel_id=1, source_target_pairs={{0,1},{1,0},{2,3},{3,2},{4,5},{5,4},{6,7},{7,6},{8,9},{9,8},{10,11... | collective-permute-start | bytes 98312 | tf_op jit(solution)/shard_map/ppermute | solution.py:187
  23.9 0.2 select_reduce_fusion
  24.4 0.3 collective-permute-done
  24.7 0.9 add_convert_fusion.1
  25.6 0.7 broadcast_in_dim.7
  26.4 3.4 %all-to-all-start = ((bf16[8,16,8,128]{3,2,1,0:T(8,128)(2,1)}), bf16[8,16,8,128]{3,2,1,0:T(8,128)(2,1)S(1)}, u32[]{:S(2)}, u32[]{:S(2)}) async-start(bf16[8,16,8,128]{3,2,1,0:T(8,128)(2,1)} %broadcast_in_dim.7), calls=%async_computation | async-start | bytes 524288 | tf_op jit(solution)/shard_map/all_to_all | solution.py:278
  29.9 2.5 %multiply_convert_fusion = bf16[192,8,8,8]{1,0,3,2:T(8,128)(2,1)} fusion(f32[8,8]{0,1:T(8,128)S(1)} %copy.33, f32[192,8]{0,1:T(8,128)S(1)} %convert_add_fusion), kind=kLoop, calls=%fused_computation | loop fusion | flops 196608 | bytes 203008 | tf_op jit(solution)/shard_map/convert_element_type | solution.py:297
  32.3 5.4 %convert_element_type.78 = bf16[1536,64]{0,1:T(8,128)(2,1)S(1)} reshape(bf16[192,8,8,8]{1,0,3,2:T(8,128)(2,1)} %multiply_convert_fusion) | data formatting | bytes 393216 | tf_op jit(solution)/shard_map/convert_element_type | solution.py:297
  37.7 0.2 copy.34.select_ref
  37.9 4.1 %all-to-all-done.pairs_ref = bf16[8,16,8,128]{3,2,1,0:T(8,128)(2,1)S(1)} async-done(((bf16[8,16,8,128]{3,2,1,0:T(8,128)(2,1)}), bf16[8,16,8,128]{3,2,1,0:T(8,128)(2,1)S(1)}, u32[]{:S(2)}, u32[]{:S(2)}) %all-to-all-start) | async-done | bytes 262176 | tf_op jit(solution)/shard_map/all_to_all | solution.py:278
  42.1 1.7 %shard_map.186 = (bf16[1536,128]{1,0:T(8,128)(2,1)}, f32[8,128]{1,0:T(8,128)S(1)}, f32[8,128]{1,0:T(8,128)S(1)}) custom-call(s32[2]{0:T(128)S(1)} %copy-done.6, bf16[8,16,8,128]{3,2,1,0:T(8,128)(2,1)S(1)} %all-to-all-done.pairs_ref, bf16[8,2048]{1,0:T(8,128)(2,1)S(1)} %copy-done.3, f32[16,128]{1,0:T(8,128)S(1)} %bitcast.39, f32[16,128]{1,0:T(8,128)S(1)} %bitcast.40, ...), custom_call_target="tpu_custom_call" | custom-call | flops 1000000000 | bytes 507912 | tf_op jit(solution)/shard_map/pallas_call | solution.py:25
  43.7 12.5 %all-to-all-start.1 = ((bf16[64,24,128]{2,1,0:T(8,128)(2,1)}), bf16[64,24,128]{2,1,0:T(8,128)(2,1)S(1)}, u32[]{:S(2)}, u32[]{:S(2)}) async-start(bf16[64,24,128]{2,1,0:T(8,128)(2,1)} %bitcast.8), calls=%async_computation.1 | async-start | bytes 786432 | tf_op jit(solution)/shard_map/all_to_all | solution.py:320
  56.3 13.9 %all-to-all-done.1 = bf16[64,24,128]{2,1,0:T(8,128)(2,1)S(1)} async-done(((bf16[64,24,128]{2,1,0:T(8,128)(2,1)}), bf16[64,24,128]{2,1,0:T(8,128)(2,1)S(1)}, u32[]{:S(2)}, u32[]{:S(2)}) %all-to-all-start.1) | async-done | bytes 393248 | tf_op jit(solution)/shard_map/all_to_all | solution.py:320
  70.2 0.9 broadcast_in_dim.9
  71.1 8.3 %all-to-all-start.2 = ((bf16[16,144,128]{2,1,0:T(8,128)(2,1)}), bf16[16,144,128]{2,1,0:T(8,128)(2,1)S(1)}, u32[]{:S(2)}, u32[]{:S(2)}) async-start(bf16[16,144,128]{2,1,0:T(8,128)(2,1)} %bitcast.19), calls=%async_computation.2 | async-start | bytes 1179648 | tf_op jit(solution)/shard_map/all_to_all | solution.py:234
  79.5 2.0 %collective-permute-start.1 = (bf16[192,1024]{1,0:T(8,128)(2,1)S(1)}, bf16[192,1024]{1,0:T(8,128)(2,1)S(1)}, u32[]{:S(2)}, u32[]{:S(2)}) collective-permute-start(bf16[192,1024]{1,0:T(8,128)(2,1)S(1)} %reshape.192.mine_ref), channel_id=1, source_target_pairs={{0,1},{1,0},{2,3},{3,2},{4,5},{5,4},{6,7},{7,6},{8,9},{9,8},{10,11... | collective-permute-start | bytes 1179656 | tf_op jit(solution)/shard_map/ppermute | solution.py:187
  81.6 16.3 %all-to-all-done.2.dense_ref = bf16[16,144,128]{2,1,0:T(8,128)(2,1)S(1)} async-done(((bf16[16,144,128]{2,1,0:T(8,128)(2,1)}), bf16[16,144,128]{2,1,0:T(8,128)(2,1)S(1)}, u32[]{:S(2)}, u32[]{:S(2)}) %all-to-all-start.2) | async-done | bytes 589856 | tf_op jit(solution)/shard_map/all_to_all | solution.py:234
  97.9 2.4 %shard_map.187 = (f32[192,1024]{1,0:T(8,128)S(1)}, bf16[192,1024]{1,0:T(8,128)(2,1)S(1)}) custom-call(s32[2]{0:T(128)S(1)} %copy-done.6, bf16[192,1024]{1,0:T(8,128)(2,1)S(1)} %reshape.192.mine_ref, bf16[192,1024]{1,0:T(8,128)(2,1)S(1)} %collective-permute-done.1.other_ref, bf16[112,2048]{1,0:T(8,128)(2,1)S(1)} %bitcast.36, bf16[112,2048]{1,0:T(8,128)(2,1)S(1)} %bitcast.37, ...), custom_call_target="tpu_custom_call" | custom-call | flops 2000000000 | bytes 2752520 | tf_op jit(solution)/shard_map/pallas_call | solution.py:25
  100.4 1.9 %collective-permute-start.2 = (bf16[192,1024]{1,0:T(8,128)(2,1)S(1)}, bf16[192,1024]{1,0:T(8,128)(2,1)S(1)}, u32[]{:S(2)}, u32[]{:S(2)}) collective-permute-start(bf16[192,1024]{1,0:T(8,128)(2,1)S(1)} %get-tuple-element.16), channel_id=1, source_target_pairs={{0,1},{1,0},{2,3},{3,2},{4,5},{5,4},{6,7},{7,6},{8,9},{9,8},{10,11... | collective-permute-start | bytes 1179656 | tf_op jit(solution)/shard_map/ppermute | solution.py:187
  102.5 1.5 %collective-permute-done.2 = bf16[192,1024]{1,0:T(8,128)(2,1)S(1)} collective-permute-done((bf16[192,1024]{1,0:T(8,128)(2,1)S(1)}, bf16[192,1024]{1,0:T(8,128)(2,1)S(1)}, u32[]{:S(2)}, u32[]{:S(2)}) %collective-permute-start.2) | collective-permute-done | bytes 393248 | tf_op jit(solution)/shard_map/ppermute | solution.py:187
  104.1 0.9 reshape.197
  105.0 4.8 %all-to-all-start.3 = ((bf16[64,24,128]{2,1,0:T(8,128)(2,1)}), bf16[64,24,128]{2,1,0:T(8,128)(2,1)S(1)}, u32[]{:S(2)}, u32[]{:S(2)}) async-start(bf16[64,24,128]{2,1,0:T(8,128)(2,1)} %reshape.197), calls=%async_computation.3 | async-start | bytes 786432 | tf_op jit(solution)/shard_map/all_to_all | solution.py:341
  109.8 3.5 %broadcast_multiply_fusion = f32[8,8,192,8]{3,2,1,0:T(8,128)} fusion(f32[8,8]{1,0:T(8,128)S(1)} %fusion.3, f32[8,192]{1,0:T(8,128)S(1)} %bitcast_add_fusion), kind=kLoop, calls=%fused_computation.1 | loop fusion | flops 98304 | bytes 399616 | tf_op jit(solution)/shard_map/mul | solution.py:343
  113.3 5.2 %mul.106 = f32[64,1536]{1,0:T(8,128)S(1)} reshape(f32[8,8,192,8]{3,2,1,0:T(8,128)} %broadcast_multiply_fusion) | data formatting | bytes 786432 | tf_op jit(solution)/shard_map/mul | solution.py:343
  118.6 6.9 %all-to-all-done.3 = bf16[64,24,128]{2,1,0:T(8,128)(2,1)S(1)} async-done(((bf16[64,24,128]{2,1,0:T(8,128)(2,1)}), bf16[64,24,128]{2,1,0:T(8,128)(2,1)S(1)}, u32[]{:S(2)}, u32[]{:S(2)}) %all-to-all-start.3) | async-done | bytes 393248 | tf_op jit(solution)/shard_map/all_to_all | solution.py:341
  125.5 0.3 shard_map.188
  125.8 9.0 %all_to_all.25 = bf16[8,8,128]{2,1,0:T(8,128)(2,1)S(1)} all-to-all(bf16[8,8,128]{2,1,0:T(8,128)(2,1)S(1)} %bitcast.35), channel_id=1, replica_groups=mesh['z'=8,'y'=8,'x'=8,'c'=2] {'x'}, dimensions={0} | all-to-all | bytes 32768 | tf_op jit(solution)/shard_map/all_to_all | solution.py:353
  134.8 0.6 add_convert_fusion.2
  (49 shorter events, 1.3 us)
Async XLA Ops:
  2.8 20.9 %copy-start.10 = (s32[8,2]{0,1:T(2,128)S(1)}, s32[8,2]{0,1:T(2,128)}, u32[]{:S(2)}) copy-start(s32[8,2]{0,1:T(2,128)} %param.28) | copy-start | bytes 196
  2.8 21.5 %copy-start.11 = (f32[8,2]{0,1:T(2,128)S(1)}, f32[8,2]{0,1:T(2,128)}, u32[]{:S(2)}) copy-start(f32[8,2]{0,1:T(2,128)} %param.29) | copy-start | bytes 196
  7.6 34.4 %copy-start.3 = (bf16[8,2048]{1,0:T(8,128)(2,1)S(1)}, bf16[8,2048]{1,0:T(8,128)(2,1)}, u32[]{:S(2)}) copy-start(bf16[8,2048]{1,0:T(8,128)(2,1)} %tokens_ref.3) | copy-start | bytes 98308
  7.6 34.4 %copy-start.4 = (f32[2048]{0:T(1024)S(1)}, f32[2048]{0:T(1024)}, u32[]{:S(2)}) copy-start(f32[2048]{0:T(1024)} %param.26) | copy-start | bytes 24580
  7.6 34.4 %copy-start.5 = (f32[2048]{0:T(1024)S(1)}, f32[2048]{0:T(1024)}, u32[]{:S(2)}) copy-start(f32[2048]{0:T(1024)} %param.27) | copy-start | bytes 24580
  7.7 34.4 %copy-start.6 = (s32[2]{0:T(128)S(1)}, s32[2]{0:T(128)}, u32[]{:S(2)}) copy-start(s32[2]{0:T(128)} %pad_add_fusion.core_ref) | copy-start | bytes 28
  7.7 17.1 %collective-permute-start = (bf16[16,8,128]{2,1,0:T(8,128)(2,1)}, bf16[16,8,128]{2,1,0:T(8,128)(2,1)S(1)}, u32[]{:S(2)}, u32[]{:S(2)}) collective-permute-start(bf16[16,8,128]{2,1,0:T(8,128)(2,1)} %get-tuple-element.11), channel_id=1, source_target_pairs={{0,1},{1,0},{2,3},{3,2},{4,5},{5,4},{6,7},{7,6},{8,9},{9,8},{10,11... | collective-permute-start | bytes 98312 | tf_op jit(solution)/shard_map/ppermute | solution.py:187
  24.3 32.0 %copy-start.7 = (bf16[128,88]{0,1:T(8,128)(2,1)S(1)}, bf16[128,88]{0,1:T(8,128)(2,1)}, u32[]{:S(2)}) copy-start(bf16[128,88]{0,1:T(8,128)(2,1)} %param.33) | copy-start | bytes 67588
  24.7 31.5 %copy-start.8 = (bf16[128,88]{0,1:T(8,128)(2,1)S(1)}, bf16[128,88]{0,1:T(8,128)(2,1)}, u32[]{:S(2)}) copy-start(bf16[128,88]{0,1:T(8,128)(2,1)} %param.34) | copy-start | bytes 67588
  25.6 30.7 %copy-start.9 = (bf16[88,128]{1,0:T(8,128)(2,1)S(1)}, bf16[88,128]{1,0:T(8,128)(2,1)}, u32[]{:S(2)}) copy-start(bf16[88,128]{1,0:T(8,128)(2,1)} %param.35) | copy-start | bytes 67588
  26.4 15.7 %all-to-all-start = ((bf16[8,16,8,128]{3,2,1,0:T(8,128)(2,1)}), bf16[8,16,8,128]{3,2,1,0:T(8,128)(2,1)S(1)}, u32[]{:S(2)}, u32[]{:S(2)}) async-start(bf16[8,16,8,128]{3,2,1,0:T(8,128)(2,1)} %broadcast_in_dim.7), calls=%async_computation | async-start | bytes 524288 | tf_op jit(solution)/shard_map/all_to_all | solution.py:278
  32.3 65.6 %copy-start = (bf16[1,2048,112]{1,2,0:T(8,128)(2,1)S(1)}, bf16[1,2048,112]{1,2,0:T(8,128)(2,1)}, u32[]{:S(2)}) copy-start(bf16[1,2048,112]{1,2,0:T(8,128)(2,1)} %param.30) | copy-start | bytes 1376260
  32.3 65.6 %copy-start.1 = (bf16[1,2048,112]{1,2,0:T(8,128)(2,1)S(1)}, bf16[1,2048,112]{1,2,0:T(8,128)(2,1)}, u32[]{:S(2)}) copy-start(bf16[1,2048,112]{1,2,0:T(8,128)(2,1)} %param.31) | copy-start | bytes 1376260
  32.3 65.6 %copy-start.2 = (bf16[1,112,2048]{2,1,0:T(8,128)(2,1)S(1)}, bf16[1,112,2048]{2,1,0:T(8,128)(2,1)}, u32[]{:S(2)}) copy-start(bf16[1,112,2048]{2,1,0:T(8,128)(2,1)} %param.32) | copy-start | bytes 1376260
  43.7 26.5 %all-to-all-start.1 = ((bf16[64,24,128]{2,1,0:T(8,128)(2,1)}), bf16[64,24,128]{2,1,0:T(8,128)(2,1)S(1)}, u32[]{:S(2)}, u32[]{:S(2)}) async-start(bf16[64,24,128]{2,1,0:T(8,128)(2,1)} %bitcast.8), calls=%async_computation.1 | async-start | bytes 786432 | tf_op jit(solution)/shard_map/all_to_all | solution.py:320
  71.1 26.8 %all-to-all-start.2 = ((bf16[16,144,128]{2,1,0:T(8,128)(2,1)}), bf16[16,144,128]{2,1,0:T(8,128)(2,1)S(1)}, u32[]{:S(2)}, u32[]{:S(2)}) async-start(bf16[16,144,128]{2,1,0:T(8,128)(2,1)} %bitcast.19), calls=%async_computation.2 | async-start | bytes 1179648 | tf_op jit(solution)/shard_map/all_to_all | solution.py:234
  79.5 18.4 %collective-permute-start.1 = (bf16[192,1024]{1,0:T(8,128)(2,1)S(1)}, bf16[192,1024]{1,0:T(8,128)(2,1)S(1)}, u32[]{:S(2)}, u32[]{:S(2)}) collective-permute-start(bf16[192,1024]{1,0:T(8,128)(2,1)S(1)} %reshape.192.mine_ref), channel_id=1, source_target_pairs={{0,1},{1,0},{2,3},{3,2},{4,5},{5,4},{6,7},{7,6},{8,9},{9,8},{10,11... | collective-permute-start | bytes 1179656 | tf_op jit(solution)/shard_map/ppermute | solution.py:187
  100.4 3.6 %collective-permute-start.2 = (bf16[192,1024]{1,0:T(8,128)(2,1)S(1)}, bf16[192,1024]{1,0:T(8,128)(2,1)S(1)}, u32[]{:S(2)}, u32[]{:S(2)}) collective-permute-start(bf16[192,1024]{1,0:T(8,128)(2,1)S(1)} %get-tuple-element.16), channel_id=1, source_target_pairs={{0,1},{1,0},{2,3},{3,2},{4,5},{5,4},{6,7},{7,6},{8,9},{9,8},{10,11... | collective-permute-start | bytes 1179656 | tf_op jit(solution)/shard_map/ppermute | solution.py:187
  105.0 20.5 %all-to-all-start.3 = ((bf16[64,24,128]{2,1,0:T(8,128)(2,1)}), bf16[64,24,128]{2,1,0:T(8,128)(2,1)S(1)}, u32[]{:S(2)}, u32[]{:S(2)}) async-start(bf16[64,24,128]{2,1,0:T(8,128)(2,1)} %reshape.197), calls=%async_computation.3 | async-start | bytes 786432 | tf_op jit(solution)/shard_map/all_to_all | solution.py:341

commit v3 on v2

v3 whole, which is shorter than its diff:
```python
import jax
import jax.numpy as jnp
from jax import lax
from jax.experimental import pallas as pl
from jax.experimental.pallas import tpu as pltpu
from jax.sharding import Mesh
from jax.sharding import PartitionSpec as P

RMS_EPSILON = 1e-06
GROUP_EPSILON = 1e-05
BF = jnp.bfloat16
F32 = jnp.float32
EP = ("z", "y")
TP = ("x", "c")
NT = (((1,), (1,)), ((), ()))
FULL = 61 << 20


def call(kernel, out_shape, args, flops, scratch=(), specs=None, out_specs=None, vmem=None):
    full = pl.BlockSpec(memory_space=pltpu.VMEM)
    size = sum(a.size * a.dtype.itemsize for a in args)
    return pl.pallas_call(
        kernel,
        out_shape=out_shape,
        in_specs=specs or [full] * len(args),
        out_specs=out_specs or jax.tree.map(lambda _: full, out_shape),
        scratch_shapes=list(scratch),
        compiler_params=pltpu.CompilerParams(vmem_limit_bytes=vmem or 16 << 20),
        cost_estimate=pl.CostEstimate(flops=flops, bytes_accessed=size, transcendentals=0),
    )(*args)


def regroup_kernel(gate_hbm, up_hbm, down_hbm, sent_hbm, parts, packed, sems):
    half = packed.shape[1] // 3
    size = gate_hbm.shape[0]
    count = sent_hbm.shape[0]
    copies = [
        pltpu.make_async_copy(ref, parts.at[n], sems.at[count + n])
        for n, ref in enumerate((gate_hbm, up_hbm, down_hbm))
    ]
    for c in copies:
        c.start()
    for n in range(3):
        packed[1, half * n + size - half : half * n + half, :] = jnp.zeros(
            (2 * half - size, packed.shape[2]), BF
        )
    for n, c in enumerate(copies):
        c.wait()
        packed[0, half * n : half * n + half, :] = parts[n, :half, :]
        packed[1, half * n : half * n + size - half, :] = parts[n, half:, :]
    copies = [pltpu.make_async_copy(packed, sent_hbm.at[n], sems.at[n]) for n in range(count)]
    for c in copies:
        c.start()
    for c in copies:
        c.wait()


def retention_kernel(
    tokens_ref,
    gain_ref,
    cos_ref,
    sin_ref,
    decay_ref,
    q_hbm,
    k_hbm,
    v_hbm,
    state_hbm,
    out_hbm,
    keep_ref,
    give_ref,
    new_hbm,
    q_w,
    k_w,
    v_w,
    state,
    out_w,
    fresh,
    held,
    sems,
):
    rows, width = tokens_ref.shape
    core = lax.axis_index("c")
    copies = [
        pltpu.make_async_copy(s, d, sems.at[n])
        for n, (s, d) in enumerate(
            ((q_hbm, q_w), (k_hbm, k_w), (v_hbm, v_w), (state_hbm, state), (out_hbm, out_w))
        )
    ]
    for c in copies:
        c.start()
    x = tokens_ref[...].astype(F32)
    inv = lax.rsqrt(jnp.sum(x * x, axis=1, keepdims=True) / width + RMS_EPSILON)
    normed_in = (x * inv * gain_ref[...]).astype(BF)

    def project(n, w):
        copies[n].wait()
        return jnp.dot(normed_in, w[...], preferred_element_type=F32)

    def rotated(v):
        return v * cos_ref[...] + pltpu.roll(v, v.shape[1] // 2, 1) * sin_ref[...]

    query = rotated(project(0, q_w))
    keys = rotated(project(1, k_w)) * q_w.shape[1] ** (-0.5)
    values = project(2, v_w)
    query_t = query.T
    keys_t = keys.T
    copies[3].wait()
    decay = decay_ref[0]
    retained = []
    for i in range(rows):
        new = state[i] * decay + keys_t[:, i : i + 1] * values[i : i + 1, :]
        fresh[i] = new
        retained.append(jnp.sum(query_t[:, i : i + 1] * new, axis=0, keepdims=True))
    back = pltpu.make_async_copy(fresh, new_hbm, sems.at[5])
    back.start()
    retained = jnp.concatenate(retained, axis=0)
    centered = retained - jnp.mean(retained, axis=1, keepdims=True)
    normed = centered * lax.rsqrt(
        jnp.mean(centered * centered, axis=1, keepdims=True) + GROUP_EPSILON
    )
    normed = normed.astype(BF)
    copies[4].wait()
    mix = jnp.dot(normed, out_w[...], preferred_element_type=F32)
    for j in range(width // 128):
        held[j] = mix[:, 128 * j : 128 * j + 128]
    for k in range(width // 256):
        keep_ref[k] = held[2 * k + core]
        give_ref[k] = held[2 * k + 1 - core].astype(BF)
    back.wait()


def pair_kernel(keep_ref, got_ref, sent_hbm, pair, sems):
    pair[...] = (keep_ref[...] + got_ref[...].astype(F32)).astype(BF)
    copies = [
        pltpu.make_async_copy(pair, sent_hbm.at[n], sems.at[n]) for n in range(sent_hbm.shape[0])
    ]
    for c in copies:
        c.start()
    for c in copies:
        c.wait()


def dispatch_kernel(
    pairs_ref, tokens_ref, gain_ref, gate_ref, select_ref, sent_ref, own_ref, stat_ref, held
):
    rows = tokens_ref.shape[0]
    blocks = pairs_ref.shape[1]
    core = lax.axis_index("c")
    square = jnp.zeros((rows, 128), F32)
    along = jnp.zeros((rows, 128), F32)
    mine = []
    for k in range(blocks):
        j = 2 * k + core
        m = tokens_ref[:, pl.ds(pl.multiple_of(j * 128, 128), 128)].astype(F32)
        for p in range(pairs_ref.shape[0]):
            m = m + pairs_ref[p, k].astype(F32)
        held[k] = m
        square = square + m * m
        along = along + m * gain_ref[pl.ds(j, 1), :] * gate_ref[pl.ds(j, 1), :]
        mine.append(m)
    own_ref[...] = held[lax.axis_index("x")]
    lane = lax.broadcasted_iota(jnp.int32, (rows, 128), 1)
    stat_ref[...] = jnp.where(
        lane < 64, jnp.sum(square, axis=1, keepdims=True), jnp.sum(along, axis=1, keepdims=True)
    )
    mine = jnp.concatenate(mine, axis=0).astype(BF)
    count, _, wide = select_ref.shape
    same = lax.broadcasted_iota(jnp.int32, (blocks, wide), 0) == (
        lax.broadcasted_iota(jnp.int32, (blocks, wide), 1) // rows
    )
    spread = jnp.broadcast_to(select_ref[...], (count, blocks, wide)) * same.astype(F32)[None]
    spread = spread.reshape(count * blocks, wide).astype(BF)
    sent_ref[...] = jnp.dot(spread, mine, preferred_element_type=F32).astype(BF)


def expert_kernel(
    mine_ref, other_ref, gain_ref, gate_ref, up_ref, down_ref, dense_ref, keep_ref, give_ref
):
    count, half_width = mine_ref.shape
    blocks = half_width // 128
    half = dense_ref.shape[1] // 3
    core = lax.axis_index("c")
    sides = ((mine_ref, core), (other_ref, 1 - core))

    def columns(ref, parity):
        return jnp.concatenate(
            [
                ref[:, pl.ds(pl.multiple_of((2 * k + parity) * 128, 128), 128)]
                for k in range(blocks)
            ],
            axis=1,
        )

    def dense_columns(parity, low, high):
        return jnp.concatenate(
            [dense_ref[2 * k + parity, low:high, :] for k in range(blocks)], axis=1
        )

    square = jnp.zeros((count, 128), F32)
    for ref, _ in sides:
        for k in range(blocks):
            x = ref[:, 128 * k : 128 * k + 128].astype(F32)
            square = square + x * x
    scale = lax.rsqrt(
        jnp.sum(square, axis=1, keepdims=True) / (2 * half_width) + RMS_EPSILON
    )
    gate = up = dense = 0.0
    for ref, parity in sides:
        x = jnp.concatenate(
            [
                (
                    ref[:, 128 * k : 128 * k + 128].astype(F32)
                    * scale
                    * gain_ref[pl.ds(2 * k + parity, 1), :]
                ).astype(BF)
                for k in range(blocks)
            ],
            axis=1,
        )

        def along(w):
            return lax.dot_general(x, w, NT, preferred_element_type=F32)

        gate = gate + along(columns(gate_ref, parity))
        up = up + along(columns(up_ref, parity))
        dense = dense + along(dense_columns(parity, 0, 2 * half))
    is_dense = lax.broadcasted_iota(jnp.int32, (count, 1), 0) % 3 == 2
    hidden = (gate / (1.0 + jnp.exp(-gate))) * up
    hidden = jnp.where(is_dense, 0.0, hidden).astype(BF)
    dense_gate = dense[:, :half]
    dense_hidden = (dense_gate / (1.0 + jnp.exp(-dense_gate))) * dense[:, half:]
    dense_hidden = jnp.where(is_dense, dense_hidden, 0.0).astype(BF)
    for out, parity in ((give_ref, 1 - core), (keep_ref, core)):
        r = jnp.dot(hidden, columns(down_ref, parity), preferred_element_type=F32)
        r = r + jnp.dot(
            dense_hidden, dense_columns(parity, 2 * half, 3 * half), preferred_element_type=F32
        )
        out[...] = r.astype(out.dtype)


def combine_kernel(weight_ref, mine_ref, other_ref, back_ref, out_ref):
    rows, count = weight_ref.shape
    blocks = out_ref.shape[0]
    stat = mine_ref[...] + other_ref[...]
    scale = lax.rsqrt(stat[:, :1] / (2 * blocks * 128) + RMS_EPSILON)
    branch = jax.nn.sigmoid(scale * stat[:, 64:65])
    row = lax.broadcasted_iota(jnp.int32, (rows, count), 0)
    place = lax.broadcasted_iota(jnp.int32, (rows, count), 1)
    dense = (row == lax.axis_index("x")) & (place % 3 == 2)
    weight = jnp.where(dense, branch, weight_ref[...])
    high = weight.astype(BF)
    low = (weight - high.astype(F32)).astype(BF)
    back = back_ref[...]
    total = jnp.dot(high, back, preferred_element_type=F32) + jnp.dot(
        low, back, preferred_element_type=F32
    )
    for k in range(blocks):
        out_ref[k] = total[:, 128 * k : 128 * k + 128]


def swap(x):
    return lax.ppermute(x, "c", [(0, 1), (1, 0)])


def local(
    tokens,
    past_lengths,
    state,
    norm1_gain,
    query_weight,
    key_weight,
    value_weight,
    out_weight,
    norm2_gain,
    branch_gate,
    route_ids,
    route_weights,
    expert_gate,
    expert_up,
    expert_down,
    dense_gate,
    dense_up,
    dense_down,
):
    rows, width = tokens.shape
    x_count = lax.axis_size("x")
    tp_count = 2 * x_count
    ep_count = lax.axis_size(EP)
    x_index = lax.axis_index("x")
    tp_index = lax.axis_index(TP)
    blocks = width // 128
    own_blocks = blocks // 2
    key_size = query_weight.shape[1]
    value_size = value_weight.shape[1]
    smem = pl.BlockSpec(memory_space=pltpu.SMEM)
    vmem = pl.BlockSpec(memory_space=pltpu.VMEM)
    hbm = pl.BlockSpec(memory_space=pltpu.HBM)
    shaped = jax.ShapeDtypeStruct

    half = -(-dense_gate.shape[1] // 2 // 16) * 16
    sent = call(
        regroup_kernel,
        shaped((x_count, 2, 3 * half, 128), BF),
        (dense_gate.T, dense_up.T, dense_down),
        1_000_000,
        scratch=(
            pltpu.VMEM((3, *dense_down.shape), BF),
            pltpu.VMEM((2, 3 * half, 128), BF),
            pltpu.SemaphoreType.DMA((x_count + 3,)),
        ),
        specs=[hbm, hbm, hbm],
        out_specs=hbm,
        vmem=FULL,
    )
    dense_parts = lax.all_to_all(
        sent.reshape(tp_count, 3 * half, 128), TP, 0, 0, tiled=True
    )

    lane = jnp.arange(key_size, dtype=jnp.int32)
    inverse = 10000.0 ** (-(lane % (key_size // 2)).astype(F32) / (key_size // 2))
    angles = past_lengths.astype(F32)[:, None] * inverse[None, :]
    cosine = jnp.cos(angles)
    sine = jnp.sin(angles) * jnp.where(lane < key_size // 2, -1.0, 1.0)[None, :]
    decay = jnp.exp(jnp.log1p(-jnp.exp2(-5.0 - 7.0 * tp_index.astype(F32) / (tp_count - 1))))
    keep, give, new_state = call(
        retention_kernel,
        (
            shaped((own_blocks, rows, 128), F32),
            shaped((own_blocks, rows, 128), BF),
            shaped((rows, key_size, value_size), F32),
        ),
        (
            tokens,
            norm1_gain.reshape(1, width),
            cosine,
            sine,
            decay.reshape(1),
            query_weight,
            key_weight,
            value_weight,
            state.reshape(rows, key_size, value_size),
            out_weight,
        ),
        10_000_000_000,
        scratch=(
            pltpu.VMEM(query_weight.shape, BF),
            pltpu.VMEM(key_weight.shape, BF),
            pltpu.VMEM(value_weight.shape, BF),
            pltpu.VMEM((rows, key_size, value_size), F32),
            pltpu.VMEM(out_weight.shape, BF),
            pltpu.VMEM((rows, key_size, value_size), F32),
            pltpu.VMEM((blocks, rows, 128), F32),
            pltpu.SemaphoreType.DMA((6,)),
        ),
        specs=[vmem, vmem, vmem, vmem, smem, hbm, hbm, hbm, hbm, hbm],
        out_specs=(vmem, vmem, hbm),
        vmem=FULL,
    )
    sent = call(
        pair_kernel,
        shaped((x_count, own_blocks, rows, 128), BF),
        (keep, swap(give)),
        1_000_000,
        scratch=(
            pltpu.VMEM((own_blocks, rows, 128), BF),
            pltpu.SemaphoreType.DMA((x_count,)),
        ),
        out_specs=hbm,
    )
    pairs = lax.all_to_all(sent, "x", 0, 0, tiled=True)

    route_count = route_ids.shape[1]
    route_flat = route_ids.reshape(-1)
    same = (route_flat[:, None] == route_flat[None, :]).astype(jnp.int32)
    number = jnp.arange(rows * route_count, dtype=jnp.int32)
    slot_index = jnp.sum(same * (number[None, :] < number[:, None]), axis=1)
    place_of = jnp.where(slot_index < 2, route_flat * 3 + slot_index, -1)
    place_of = place_of.reshape(rows, route_count)
    in_row = jnp.arange(3 * ep_count, dtype=jnp.int32)
    row_kind = (in_row // 12) * 3 + in_row % 3
    weighted = jnp.sum(
        jnp.where(place_of[:, :, None] == row_kind, route_weights[:, :, None], 0.0), axis=1
    )
    token = jnp.arange(own_blocks * rows, dtype=jnp.int32) % rows
    tiled = jnp.tile(place_of, (own_blocks, 1))
    chosen = jnp.any(tiled[None] == row_kind[:, None, None], axis=2) | (
        (in_row[:, None] % 3 == 2) & (token[None, :] == x_index)
    )
    select = chosen.astype(F32)[:, None, :]

    outgoing, own, stat = call(
        dispatch_kernel,
        (
            shaped((3 * ep_count * own_blocks, 128), BF),
            shaped((rows, 128), F32),
            shaped((rows, 128), F32),
        ),
        (pairs, tokens, norm2_gain.reshape(blocks, 128), branch_gate.reshape(blocks, 128), select),
        1_000_000_000,
        scratch=(pltpu.VMEM((own_blocks, rows, 128), F32),),
    )
    arrived = lax.all_to_all(outgoing.reshape(ep_count, 3 * own_blocks, 128), EP, 0, 0, tiled=True)
    other_stat = swap(stat)
    mine = arrived.reshape(3 * ep_count, width // 2)
    other = swap(mine)
    shape = (3 * ep_count, width // 2)
    stay, leave = call(
        expert_kernel,
        (shaped(shape, F32), shaped(shape, BF)),
        (
            mine,
            other,
            norm2_gain.reshape(blocks, 128),
            expert_gate[0].T,
            expert_up[0].T,
            expert_down[0],
            dense_parts,
        ),
        2_000_000_000,
    )
    result = (stay + swap(leave).astype(F32)).astype(BF)
    returned = lax.all_to_all(result.reshape(ep_count, 3 * own_blocks, 128), EP, 0, 0, tiled=True)
    total = call(
        combine_kernel,
        shaped((own_blocks, rows, 128), F32),
        (weighted, stat, other_stat, returned.reshape(3 * ep_count, width // 2)),
        100_000_000,
    )
    sums = lax.all_to_all(total, "x", 0, 0, tiled=True)
    layer_out = (own + jnp.sum(sums, axis=0)).astype(BF)
    return (layer_out, new_state.reshape(state.shape))


def solution(mesh):
    split = Mesh(mesh.devices.reshape(8, 8, 8, 2), ("z", "y", "x", "c"))
    return jax.shard_map(
        local,
        mesh=split,
        in_specs=(
            P(EP, None),
            P(EP),
            P(EP, TP, None, None),
            P(),
            P(None, TP),
            P(None, TP),
            P(None, TP),
            P(TP, None),
            P(),
            P(),
            P(EP, None),
            P(EP, None),
            P(EP, None, TP),
            P(EP, None, TP),
            P(EP, TP, None),
            P(TP, EP),
            P(TP, EP),
            P(EP, TP),
        ),
        out_specs=(P(EP, TP), P(EP, TP, None, None)),
        check_vma=False,
    )
```

time: 138 us -> 131 us (0.949)
  local copies, waits for them, and re-layouts: 14.1 us -> 2.59 us
  waiting for transfers between devices: 43 us -> 51.7 us
  other arithmetic: 10.1 us -> 2.08 us
  starting transfers between devices: 48.9 us -> 51.5 us
    all_to_all x4, waiting for transfers between devices: 41.2 us -> 49.7 us  [the longest x1 16.4 us: local(): lax.all_to_all(sent.reshape(tp_count, 3 * half, 128), TP, 0, 0, tiled=True)]
    convert_element_type x3 -> x0, local copies, waits for them, and re-layouts: 5.65 us -> none  [the longest x2 5.58 us: local(): select = (chosen[:, None, None, :] * ones[None, :, :, None]).astype(BF)]
    mul x1 -> x0, local copies, waits for them, and re-layouts: 5.24 us -> none  [local(): spread = combiner.T[None, :, :, None] * ones[:, None, None, :]]
    convert_element_type x5 -> x2, other arithmetic: 3.98 us -> 0.85 us  [the longest x1 0.58 us: local(): layer_out = (own + jnp.sum(sums, axis=0)).astype(BF)]
    mul x1, other arithmetic: 3.48 us -> 0.72 us  [local(): sine = jnp.sin(angles) * jnp.where(lane < key_size // 2, -1.0, 1.0)[None, :]]
    ppermute x3 -> x4, starting transfers between devices: 20 us -> 22.1 us  [swap(): return lax.ppermute(x, 'c', [(0, 1), (1, 0)])]
    broadcast_in_dim x2 -> x0, local copies, waits for them, and re-layouts: 1.64 us -> none  [the longest x1 0.89 us: local(): jnp.broadcast_to(part[None], (x_count, *part.shape))]
    pallas_call x4 -> x6, Pallas kernels: 9.15 us -> 10.4 us  [call(): pl.pallas_call(kernel, out_shape=out_shape, in_specs=specs or [full] * le...]
  transfers between devices with their start and end apart: 7 -> 8, of which waited for: 6 -> 6; matrix products, arithmetic and copies ran while one was open for 13% -> 1% of each run, Pallas kernels for 0% -> 1%
where the time goes in v3:
time: 131 us; the launch traced here: 129 us
  waiting for transfers between devices  51.7 us (39%)
  starting transfers between devices  51.5 us (39%)
  Pallas kernels  10.4 us (8%)
  blocking collectives  9.24 us (7%)
  local copies, waits for them, and re-layouts  2.59 us (2%)
  other arithmetic  2.08 us (2%)
    ppermute x4, starting transfers between devices, swap(): return lax.ppermute(x, 'c', [(0, 1), (1, 0)])  22.1 us
    all_to_all x1, waiting for transfers between devices, local(): lax.all_to_all(sent.reshape(tp_count, 3 * half, 128), TP, 0, 0, tiled=True)  16.4 us
    all_to_all x1, waiting for transfers between devices, local(): lax.all_to_all(result.reshape(ep_count, 3 * own_blocks, 128), EP, 0, 0, t...  13.7 us
    all_to_all x1, starting transfers between devices, local(): lax.all_to_all(outgoing.reshape(ep_count, 3 * own_blocks, 128), EP, 0, 0,...  13.3 us
    all_to_all x1, waiting for transfers between devices, local(): lax.all_to_all(outgoing.reshape(ep_count, 3 * own_blocks, 128), EP, 0, 0,...  11.9 us
    pallas_call x6, Pallas kernels, call(): pl.pallas_call(kernel, out_shape=out_shape, in_specs=specs or [full] * le...  10.4 us
    all_to_all x1, blocking collectives, local(): sums = lax.all_to_all(total, 'x', 0, 0, tiled=True)  9.24 us
    all_to_all x1, starting transfers between devices, local(): lax.all_to_all(sent.reshape(tp_count, 3 * half, 128), TP, 0, 0, tiled=True)  8.15 us
  transfers between devices with their start and end apart: 8, of which 6 were waited for; matrix products, arithmetic and copies ran while one was open for 1% of the time, Pallas kernels for 1%

profile of v3, /device:TPU:1, one launch (start us, length us, event | category | flops | bytes accessed | tf_op | source)
XLA Modules:
  0.0 128.6 jit_solution(12789776788199237467)
XLA Ops:
  0.7 0.6 copy-done.9
  1.4 0.7 fusion
  2.2 4.7 %shard_map.185 = (f32[8,8,128]{2,1,0:T(8,128)}, bf16[8,8,128]{2,1,0:T(8,128)(2,1)}, f32[8,128,256]{2,1,0:T(8,128)}) custom-call(bf16[8,2048]{1,0:T(8,128)(2,1)} %tokens_ref.3, f32[1,2048]{1,0:T(1,128)} %bitcast.33, f32[8,128]{1,0:T(8,128)} %get-tuple-element.27.cos_ref, f32[8,128]{1,0:T(8,128)} %get-tuple-element.26.sin_ref, f32[1]{0:T(128)} %bitcast.1.decay_ref, ...), custom_call_target="tpu_custom_call" | custom-call | flops 10000000000 | bytes 4243460 | tf_op jit(solution)/shard_map/pallas_call | solution.py:22
  6.9 16.0 %collective-permute-start = (bf16[8,8,128]{2,1,0:T(8,128)(2,1)}, bf16[8,8,128]{2,1,0:T(8,128)(2,1)S(1)}, u32[]{:S(2)}, u32[]{:S(2)}) collective-permute-start(bf16[8,8,128]{2,1,0:T(8,128)(2,1)} %get-tuple-element.11), channel_id=1, source_target_pairs={{0,1},{1,0},{2,3},{3,2},{4,5},{5,4},{6,7},{7,6},{8,9},{9,8},{10,11... | collective-permute-start | bytes 49160 | tf_op jit(solution)/shard_map/ppermute | solution.py:262
  23.1 0.2 select_reduce_fusion.1
  23.4 0.1 copy.41
  23.6 0.1 compare_reduce_fusion
  23.7 0.3 collective-permute-done.got_ref
  24.0 0.7 shard_map.186
  24.7 3.4 %all-to-all-start = ((bf16[8,8,8,128]{3,2,1,0:T(8,128)(2,1)}), bf16[8,8,8,128]{3,2,1,0:T(8,128)(2,1)S(1)}, u32[]{:S(2)}, u32[]{:S(2)}) async-start(bf16[8,8,8,128]{3,2,1,0:T(8,128)(2,1)} %shard_map.186), calls=%async_computation | async-start | bytes 262144 | tf_op jit(solution)/shard_map/all_to_all | solution.py:370
  28.1 0.2 copy.43
  28.4 0.3 or_convert_fusion.select_ref
  28.7 7.7 %all-to-all-done.pairs_ref = bf16[8,8,8,128]{3,2,1,0:T(8,128)(2,1)S(1)} async-done(((bf16[8,8,8,128]{3,2,1,0:T(8,128)(2,1)}), bf16[8,8,8,128]{3,2,1,0:T(8,128)(2,1)S(1)}, u32[]{:S(2)}, u32[]{:S(2)}) %all-to-all-start) | async-done | bytes 131104 | tf_op jit(solution)/shard_map/all_to_all | solution.py:370
  36.4 1.0 shard_map.187
  37.4 13.3 %all-to-all-start.1 = ((bf16[64,24,128]{2,1,0:T(8,128)(2,1)}), bf16[64,24,128]{2,1,0:T(8,128)(2,1)S(1)}, u32[]{:S(2)}, u32[]{:S(2)}) async-start(bf16[64,24,128]{2,1,0:T(8,128)(2,1)} %bitcast.6), calls=%async_computation.1 | async-start | bytes 786432 | tf_op jit(solution)/shard_map/all_to_all | solution.py:402
  50.7 1.7 %shard_map.188 = bf16[8,2,144,128]{3,2,1,0:T(8,128)(2,1)} custom-call(bf16[88,128]{1,0:T(8,128)(2,1)} %bitcast.30, bf16[88,128]{1,0:T(8,128)(2,1)} %bitcast.31, bf16[88,128]{1,0:T(8,128)(2,1)} %down_hbm.1), custom_call_target="tpu_custom_call" | custom-call | flops 1000000 | bytes 67584 | tf_op jit(solution)/shard_map/pallas_call | solution.py:22
  52.4 11.9 %all-to-all-done.1 = bf16[64,24,128]{2,1,0:T(8,128)(2,1)S(1)} async-done(((bf16[64,24,128]{2,1,0:T(8,128)(2,1)}), bf16[64,24,128]{2,1,0:T(8,128)(2,1)S(1)}, u32[]{:S(2)}, u32[]{:S(2)}) %all-to-all-start.1) | async-done | bytes 393248 | tf_op jit(solution)/shard_map/all_to_all | solution.py:402
  64.3 8.1 %all-to-all-start.2 = ((bf16[16,144,128]{2,1,0:T(8,128)(2,1)}), bf16[16,144,128]{2,1,0:T(8,128)(2,1)S(1)}, u32[]{:S(2)}, u32[]{:S(2)}) async-start(bf16[16,144,128]{2,1,0:T(8,128)(2,1)} %bitcast.28), calls=%async_computation.2 | async-start | bytes 1179648 | tf_op jit(solution)/shard_map/all_to_all | solution.py:315
  72.5 0.2 reshape.211.mine_ref
  72.6 2.1 %collective-permute-start.2 = (bf16[192,1024]{1,0:T(8,128)(2,1)S(1)}, bf16[192,1024]{1,0:T(8,128)(2,1)S(1)}, u32[]{:S(2)}, u32[]{:S(2)}) collective-permute-start(bf16[192,1024]{1,0:T(8,128)(2,1)S(1)} %reshape.211.mine_ref), channel_id=1, source_target_pairs={{0,1},{1,0},{2,3},{3,2},{4,5},{5,4},{6,7},{7,6},{8,9},{9,8},{10,11... | collective-permute-start | bytes 1179656 | tf_op jit(solution)/shard_map/ppermute | solution.py:262
  74.8 16.4 %all-to-all-done.2.dense_ref = bf16[16,144,128]{2,1,0:T(8,128)(2,1)S(1)} async-done(((bf16[16,144,128]{2,1,0:T(8,128)(2,1)}), bf16[16,144,128]{2,1,0:T(8,128)(2,1)S(1)}, u32[]{:S(2)}, u32[]{:S(2)}) %all-to-all-start.2) | async-done | bytes 589856 | tf_op jit(solution)/shard_map/all_to_all | solution.py:315
  91.2 1.9 %shard_map.189 = (f32[192,1024]{1,0:T(8,128)S(1)}, bf16[192,1024]{1,0:T(8,128)(2,1)S(1)}) custom-call(bf16[192,1024]{1,0:T(8,128)(2,1)S(1)} %reshape.211.mine_ref, bf16[192,1024]{1,0:T(8,128)(2,1)S(1)} %collective-permute-done.2.other_ref, f32[16,128]{1,0:T(8,128)S(1)} %bitcast.27, bf16[112,2048]{1,0:T(8,128)(2,1)S(1)} %bitcast.22, ...), custom_call_target="tpu_custom_call" | custom-call | flops 2000000000 | bytes 2760704 | tf_op jit(solution)/shard_map/pallas_call | solution.py:22
  93.1 1.9 %collective-permute-start.3 = (bf16[192,1024]{1,0:T(8,128)(2,1)S(1)}, bf16[192,1024]{1,0:T(8,128)(2,1)S(1)}, u32[]{:S(2)}, u32[]{:S(2)}) collective-permute-start(bf16[192,1024]{1,0:T(8,128)(2,1)S(1)} %get-tuple-element.16), channel_id=1, source_target_pairs={{0,1},{1,0},{2,3},{3,2},{4,5},{5,4},{6,7},{7,6},{8,9},{9,8},{10,11... | collective-permute-start | bytes 1179656 | tf_op jit(solution)/shard_map/ppermute | solution.py:262
  95.1 1.7 %collective-permute-done.3 = bf16[192,1024]{1,0:T(8,128)(2,1)S(1)} collective-permute-done((bf16[192,1024]{1,0:T(8,128)(2,1)S(1)}, bf16[192,1024]{1,0:T(8,128)(2,1)S(1)}, u32[]{:S(2)}, u32[]{:S(2)}) %collective-permute-start.3) | collective-permute-done | bytes 393248 | tf_op jit(solution)/shard_map/ppermute | solution.py:262
  96.8 0.9 reshape.213
  97.8 4.6 %all-to-all-start.3 = ((bf16[64,24,128]{2,1,0:T(8,128)(2,1)}), bf16[64,24,128]{2,1,0:T(8,128)(2,1)S(1)}, u32[]{:S(2)}, u32[]{:S(2)}) async-start(bf16[64,24,128]{2,1,0:T(8,128)(2,1)} %reshape.213), calls=%async_computation.3 | async-start | bytes 786432 | tf_op jit(solution)/shard_map/all_to_all | solution.py:422
  102.4 2.0 %collective-permute-start.1 = (f32[8,128]{1,0:T(8,128)S(1)}, f32[8,128]{1,0:T(8,128)S(1)}, u32[]{:S(2)}, u32[]{:S(2)}) collective-permute-start(f32[8,128]{1,0:T(8,128)S(1)} %get-tuple-element.13.mine_ref), channel_id=1, source_target_pairs={{0,1},{1,0},{2,3},{3,2},{4,5},{5,4},{6,7},{7,6},{8,9},{9,8},{10,11... | collective-permute-start | bytes 12296 | tf_op jit(solution)/shard_map/ppermute | solution.py:262
  104.5 13.7 %all-to-all-done.3 = bf16[64,24,128]{2,1,0:T(8,128)(2,1)S(1)} async-done(((bf16[64,24,128]{2,1,0:T(8,128)(2,1)}), bf16[64,24,128]{2,1,0:T(8,128)(2,1)S(1)}, u32[]{:S(2)}, u32[]{:S(2)}) %all-to-all-start.3) | async-done | bytes 393248 | tf_op jit(solution)/shard_map/all_to_all | solution.py:422
  118.3 0.2 reshape.214.back_ref
  118.4 0.3 shard_map.190
  118.8 9.2 %all_to_all.25 = f32[8,8,128]{2,1,0:T(8,128)S(1)} all-to-all(f32[8,8,128]{2,1,0:T(8,128)S(1)} %shard_map.190), channel_id=1, replica_groups=mesh['z'=8,'y'=8,'x'=8,'c'=2] {'x'}, dimensions={0} | all-to-all | bytes 65536 | tf_op jit(solution)/shard_map/all_to_all | solution.py:429
  128.0 0.6 add_convert_fusion.1
  (35 shorter events, 0.6 us)
Async XLA Ops:
  0.6 0.7 copy-start.9
  6.9 16.1 %copy-start.7 = (s32[8,2]{0,1:T(2,128)S(1)}, s32[8,2]{0,1:T(2,128)}, u32[]{:S(2)}) copy-start(s32[8,2]{0,1:T(2,128)} %param.28) | copy-start | bytes 196
  6.9 17.1 %collective-permute-start = (bf16[8,8,128]{2,1,0:T(8,128)(2,1)}, bf16[8,8,128]{2,1,0:T(8,128)(2,1)S(1)}, u32[]{:S(2)}, u32[]{:S(2)}) collective-permute-start(bf16[8,8,128]{2,1,0:T(8,128)(2,1)} %get-tuple-element.11), channel_id=1, source_target_pairs={{0,1},{1,0},{2,3},{3,2},{4,5},{5,4},{6,7},{7,6},{8,9},{9,8},{10,11... | collective-permute-start | bytes 49160 | tf_op jit(solution)/shard_map/ppermute | solution.py:262
  23.1 0.8 copy-start
  24.7 11.7 %all-to-all-start = ((bf16[8,8,8,128]{3,2,1,0:T(8,128)(2,1)}), bf16[8,8,8,128]{3,2,1,0:T(8,128)(2,1)S(1)}, u32[]{:S(2)}, u32[]{:S(2)}) async-start(bf16[8,8,8,128]{3,2,1,0:T(8,128)(2,1)} %shard_map.186), calls=%async_computation | async-start | bytes 262144 | tf_op jit(solution)/shard_map/all_to_all | solution.py:370
  28.4 8.1 %copy-start.4 = (bf16[8,2048]{1,0:T(8,128)(2,1)S(1)}, bf16[8,2048]{1,0:T(8,128)(2,1)}, u32[]{:S(2)}) copy-start(bf16[8,2048]{1,0:T(8,128)(2,1)} %tokens_ref.3) | copy-start | bytes 98308
  28.4 8.0 %copy-start.5 = (f32[2048]{0:T(1024)S(1)}, f32[2048]{0:T(1024)}, u32[]{:S(2)}) copy-start(f32[2048]{0:T(1024)} %param.27) | copy-start | bytes 24580
  28.4 8.0 %copy-start.6 = (f32[2048]{0:T(1024)S(1)}, f32[2048]{0:T(1024)}, u32[]{:S(2)}) copy-start(f32[2048]{0:T(1024)} %param.26) | copy-start | bytes 24580
  37.4 26.9 %all-to-all-start.1 = ((bf16[64,24,128]{2,1,0:T(8,128)(2,1)}), bf16[64,24,128]{2,1,0:T(8,128)(2,1)S(1)}, u32[]{:S(2)}, u32[]{:S(2)}) async-start(bf16[64,24,128]{2,1,0:T(8,128)(2,1)} %bitcast.6), calls=%async_computation.1 | async-start | bytes 786432 | tf_op jit(solution)/shard_map/all_to_all | solution.py:402
  64.3 26.9 %copy-start.2 = (bf16[1,2048,112]{1,2,0:T(8,128)(2,1)S(1)}, bf16[1,2048,112]{1,2,0:T(8,128)(2,1)}, u32[]{:S(2)}) copy-start(bf16[1,2048,112]{1,2,0:T(8,128)(2,1)} %param.31) | copy-start | bytes 1376260
  64.3 26.9 %copy-start.3 = (bf16[1,112,2048]{2,1,0:T(8,128)(2,1)S(1)}, bf16[1,112,2048]{2,1,0:T(8,128)(2,1)}, u32[]{:S(2)}) copy-start(bf16[1,112,2048]{2,1,0:T(8,128)(2,1)} %param.32) | copy-start | bytes 1376260
  64.3 26.9 %all-to-all-start.2 = ((bf16[16,144,128]{2,1,0:T(8,128)(2,1)}), bf16[16,144,128]{2,1,0:T(8,128)(2,1)S(1)}, u32[]{:S(2)}, u32[]{:S(2)}) async-start(bf16[16,144,128]{2,1,0:T(8,128)(2,1)} %bitcast.28), calls=%async_computation.2 | async-start | bytes 1179648 | tf_op jit(solution)/shard_map/all_to_all | solution.py:315
  72.5 18.7 %copy-start.1 = (bf16[1,2048,112]{1,2,0:T(8,128)(2,1)S(1)}, bf16[1,2048,112]{1,2,0:T(8,128)(2,1)}, u32[]{:S(2)}) copy-start(bf16[1,2048,112]{1,2,0:T(8,128)(2,1)} %param.30) | copy-start | bytes 1376260
  72.6 18.5 %collective-permute-start.2 = (bf16[192,1024]{1,0:T(8,128)(2,1)S(1)}, bf16[192,1024]{1,0:T(8,128)(2,1)S(1)}, u32[]{:S(2)}, u32[]{:S(2)}) collective-permute-start(bf16[192,1024]{1,0:T(8,128)(2,1)S(1)} %reshape.211.mine_ref), channel_id=1, source_target_pairs={{0,1},{1,0},{2,3},{3,2},{4,5},{5,4},{6,7},{7,6},{8,9},{9,8},{10,11... | collective-permute-start | bytes 1179656 | tf_op jit(solution)/shard_map/ppermute | solution.py:262
  93.1 3.6 %collective-permute-start.3 = (bf16[192,1024]{1,0:T(8,128)(2,1)S(1)}, bf16[192,1024]{1,0:T(8,128)(2,1)S(1)}, u32[]{:S(2)}, u32[]{:S(2)}) collective-permute-start(bf16[192,1024]{1,0:T(8,128)(2,1)S(1)} %get-tuple-element.16), channel_id=1, source_target_pairs={{0,1},{1,0},{2,3},{3,2},{4,5},{5,4},{6,7},{7,6},{8,9},{9,8},{10,11... | collective-permute-start | bytes 1179656 | tf_op jit(solution)/shard_map/ppermute | solution.py:262
  97.8 20.5 %all-to-all-start.3 = ((bf16[64,24,128]{2,1,0:T(8,128)(2,1)}), bf16[64,24,128]{2,1,0:T(8,128)(2,1)S(1)}, u32[]{:S(2)}, u32[]{:S(2)}) async-start(bf16[64,24,128]{2,1,0:T(8,128)(2,1)} %reshape.213), calls=%async_computation.3 | async-start | bytes 786432 | tf_op jit(solution)/shard_map/all_to_all | solution.py:422
  102.4 2.1 %copy-start.8 = (f32[8,2]{0,1:T(2,128)S(1)}, f32[8,2]{0,1:T(2,128)}, u32[]{:S(2)}) copy-start(f32[8,2]{0,1:T(2,128)} %param.29) | copy-start | bytes 196
  102.4 16.0 %collective-permute-start.1 = (f32[8,128]{1,0:T(8,128)S(1)}, f32[8,128]{1,0:T(8,128)S(1)}, u32[]{:S(2)}, u32[]{:S(2)}) collective-permute-start(f32[8,128]{1,0:T(8,128)S(1)} %get-tuple-element.13.mine_ref), channel_id=1, source_target_pairs={{0,1},{1,0},{2,3},{3,2},{4,5},{5,4},{6,7},{7,6},{8,9},{9,8},{10,11... | collective-permute-start | bytes 12296 | tf_op jit(solution)/shard_map/ppermute | solution.py:262

commit v4 on v3

--- a/solution.py
+++ b/solution.py
@@ -31,8 +31,7 @@
 
 
 def regroup_kernel(gate_hbm, up_hbm, down_hbm, sent_hbm, parts, packed, sems):
-    half = packed.shape[1] // 3
-    size = gate_hbm.shape[0]
+    half = gate_hbm.shape[0] // 2
     count = sent_hbm.shape[0]
     copies = [
         pltpu.make_async_copy(ref, parts.at[n], sems.at[count + n])
@@ -40,14 +39,13 @@
     ]
     for c in copies:
         c.start()
-    for n in range(3):
-        packed[1, half * n + size - half : half * n + half, :] = jnp.zeros(
-            (2 * half - size, packed.shape[2]), BF
-        )
+    spare = packed.shape[1] - 3 * half
+    for p in range(2):
+        packed[p, 3 * half :, :] = jnp.zeros((spare, packed.shape[2]), BF)
     for n, c in enumerate(copies):
         c.wait()
-        packed[0, half * n : half * n + half, :] = parts[n, :half, :]
-        packed[1, half * n : half * n + size - half, :] = parts[n, half:, :]
+        for p in range(2):
+            packed[p, half * n : half * n + half, :] = parts[n, half * p : half * p + half, :]
     copies = [pltpu.make_async_copy(packed, sent_hbm.at[n], sems.at[n]) for n in range(count)]
     for c in copies:
         c.start()
@@ -129,40 +127,25 @@
     back.wait()
 
 
-def pair_kernel(keep_ref, got_ref, sent_hbm, pair, sems):
-    pair[...] = (keep_ref[...] + got_ref[...].astype(F32)).astype(BF)
-    copies = [
-        pltpu.make_async_copy(pair, sent_hbm.at[n], sems.at[n]) for n in range(sent_hbm.shape[0])
-    ]
-    for c in copies:
-        c.start()
-    for c in copies:
-        c.wait()
-
-
-def dispatch_kernel(
-    pairs_ref, tokens_ref, gain_ref, gate_ref, select_ref, sent_ref, own_ref, stat_ref, held
-):
+def pair_kernel(keep_ref, got_ref, sent_ref):
+    pair = (keep_ref[...] + got_ref[...].astype(F32)).astype(BF)
+    for n in range(sent_ref.shape[0]):
+        sent_ref[n] = pair
+
+
+def dispatch_kernel(pairs_ref, tokens_ref, select_ref, sent_ref, own_ref, held):
     rows = tokens_ref.shape[0]
     blocks = pairs_ref.shape[1]
     core = lax.axis_index("c")
-    square = jnp.zeros((rows, 128), F32)
-    along = jnp.zeros((rows, 128), F32)
     mine = []
     for k in range(blocks):
-        j = 2 * k + core
-        m = tokens_ref[:, pl.ds(pl.multiple_of(j * 128, 128), 128)].astype(F32)
+        at = pl.multiple_of((2 * k + core) * 128, 128)
+        m = tokens_ref[:, pl.ds(at, 128)].astype(F32)
         for p in range(pairs_ref.shape[0]):
             m = m + pairs_ref[p, k].astype(F32)
         held[k] = m
-        square = square + m * m
-        along = along + m * gain_ref[pl.ds(j, 1), :] * gate_ref[pl.ds(j, 1), :]
         mine.append(m)
     own_ref[...] = held[lax.axis_index("x")]
-    lane = lax.broadcasted_iota(jnp.int32, (rows, 128), 1)
-    stat_ref[...] = jnp.where(
-        lane < 64, jnp.sum(square, axis=1, keepdims=True), jnp.sum(along, axis=1, keepdims=True)
-    )
     mine = jnp.concatenate(mine, axis=0).astype(BF)
     count, _, wide = select_ref.shape
     same = lax.broadcasted_iota(jnp.int32, (blocks, wide), 0) == (
@@ -173,88 +156,127 @@
     sent_ref[...] = jnp.dot(spread, mine, preferred_element_type=F32).astype(BF)
 
 
-def expert_kernel(
-    mine_ref, other_ref, gain_ref, gate_ref, up_ref, down_ref, dense_ref, keep_ref, give_ref
-):
-    count, half_width = mine_ref.shape
+def columns(ref, parity, blocks):
+    return jnp.concatenate(
+        [ref[:, pl.ds(pl.multiple_of((2 * k + parity) * 128, 128), 128)] for k in range(blocks)],
+        axis=1,
+    )
+
+
+def gains(ref, k, parity):
+    return ref[pl.ds(2 * k + parity, 1), :]
+
+
+def project(x_ref, parity, gain_ref, bias_ref, gate_ref, up_ref, dense_ref):
+    count, half_width = x_ref.shape
     blocks = half_width // 128
     half = dense_ref.shape[1] // 3
+    half = half - half % 4
+    square = jnp.zeros((count, 128), F32)
+    along = jnp.zeros((count, 128), F32)
+    parts = []
+    for k in range(blocks):
+        x = x_ref[:, 128 * k : 128 * k + 128].astype(F32)
+        square = square + x * x
+        x = x * gains(gain_ref, k, parity)
+        along = along + x * gains(bias_ref, k, parity)
+        parts.append(x.astype(BF))
+    x = jnp.concatenate(parts, axis=1)
+    dense = jnp.concatenate(
+        [dense_ref[2 * k + parity, : 2 * half, :] for k in range(blocks)], axis=1
+    )
+    sums = [
+        lax.dot_general(x, w, NT, preferred_element_type=F32)
+        for w in (columns(gate_ref, parity, blocks), columns(up_ref, parity, blocks), dense)
+    ]
+    return (*sums, square, along)
+
+
+def first_kernel(
+    x_ref, gain_ref, bias_ref, gate_ref, up_ref, dense_ref, g_ref, u_ref, d_ref, s_ref, a_ref
+):
     core = lax.axis_index("c")
-    sides = ((mine_ref, core), (other_ref, 1 - core))
-
-    def columns(ref, parity):
-        return jnp.concatenate(
-            [
-                ref[:, pl.ds(pl.multiple_of((2 * k + parity) * 128, 128), 128)]
-                for k in range(blocks)
-            ],
-            axis=1,
-        )
-
-    def dense_columns(parity, low, high):
-        return jnp.concatenate(
-            [dense_ref[2 * k + parity, low:high, :] for k in range(blocks)], axis=1
-        )
-
-    square = jnp.zeros((count, 128), F32)
-    for ref, _ in sides:
-        for k in range(blocks):
-            x = ref[:, 128 * k : 128 * k + 128].astype(F32)
-            square = square + x * x
-    scale = lax.rsqrt(
-        jnp.sum(square, axis=1, keepdims=True) / (2 * half_width) + RMS_EPSILON
-    )
-    gate = up = dense = 0.0
-    for ref, parity in sides:
-        x = jnp.concatenate(
-            [
-                (
-                    ref[:, 128 * k : 128 * k + 128].astype(F32)
-                    * scale
-                    * gain_ref[pl.ds(2 * k + parity, 1), :]
-                ).astype(BF)
-                for k in range(blocks)
-            ],
-            axis=1,
-        )
-
-        def along(w):
-            return lax.dot_general(x, w, NT, preferred_element_type=F32)
-
-        gate = gate + along(columns(gate_ref, parity))
-        up = up + along(columns(up_ref, parity))
-        dense = dense + along(dense_columns(parity, 0, 2 * half))
+    results = project(x_ref, core, gain_ref, bias_ref, gate_ref, up_ref, dense_ref)
+    for ref, value in zip((g_ref, u_ref, d_ref, s_ref, a_ref), results):
+        ref[...] = value
+
+
+def expand(hidden, dense_hidden, branch, parity, down_ref, dense_ref, blocks):
+    half = dense_hidden.shape[1]
+    down = jnp.concatenate(
+        [dense_ref[2 * k + parity, 2 * half : 3 * half, :] for k in range(blocks)], axis=1
+    )
+    r = jnp.dot(hidden, columns(down_ref, parity, blocks), preferred_element_type=F32)
+    return r + branch * jnp.dot(dense_hidden, down, preferred_element_type=F32)
+
+
+def second_kernel(
+    x_ref,
+    gain_ref,
+    bias_ref,
+    gate_ref,
+    up_ref,
+    dense_ref,
+    down_ref,
+    g_ref,
+    u_ref,
+    d_ref,
+    s_ref,
+    a_ref,
+    give_ref,
+    hidden_ref,
+    dense_hidden_ref,
+    branch_ref,
+):
+    count, half_width = x_ref.shape
+    other = 1 - lax.axis_index("c")
+    results = project(x_ref, other, gain_ref, bias_ref, gate_ref, up_ref, dense_ref)
+    gate, up, dense, square, along = [
+        ref[...] + value for ref, value in zip((g_ref, u_ref, d_ref, s_ref, a_ref), results)
+    ]
+    half = dense.shape[1] // 2
+    scale = lax.rsqrt(jnp.sum(square, axis=1, keepdims=True) / (2 * half_width) + RMS_EPSILON)
+    branch = jax.nn.sigmoid(jnp.sum(along, axis=1, keepdims=True) * scale)
     is_dense = lax.broadcasted_iota(jnp.int32, (count, 1), 0) % 3 == 2
-    hidden = (gate / (1.0 + jnp.exp(-gate))) * up
-    hidden = jnp.where(is_dense, 0.0, hidden).astype(BF)
-    dense_gate = dense[:, :half]
-    dense_hidden = (dense_gate / (1.0 + jnp.exp(-dense_gate))) * dense[:, half:]
-    dense_hidden = jnp.where(is_dense, dense_hidden, 0.0).astype(BF)
-    for out, parity in ((give_ref, 1 - core), (keep_ref, core)):
-        r = jnp.dot(hidden, columns(down_ref, parity), preferred_element_type=F32)
-        r = r + jnp.dot(
-            dense_hidden, dense_columns(parity, 2 * half, 3 * half), preferred_element_type=F32
-        )
-        out[...] = r.astype(out.dtype)
-
-
-def combine_kernel(weight_ref, mine_ref, other_ref, back_ref, out_ref):
+
+    def gated(v, w):
+        v = v * scale
+        return (v / (1.0 + jnp.exp(-v))) * (w * scale)
+
+    hidden = jnp.where(is_dense, 0.0, gated(gate, up)).astype(BF)
+    dense_hidden = jnp.where(is_dense, gated(dense[:, :half], dense[:, half:]), 0.0).astype(BF)
+    r = expand(hidden, dense_hidden, branch, other, down_ref, dense_ref, half_width // 128)
+    give_ref[...] = r.astype(BF)
+    hidden_ref[...] = hidden
+    dense_hidden_ref[...] = dense_hidden
+    branch_ref[...] = jnp.broadcast_to(branch, branch_ref.shape)
+
+
+def third_kernel(hidden_ref, dense_hidden_ref, branch_ref, down_ref, dense_ref, keep_ref):
+    keep_ref[...] = expand(
+        hidden_ref[...],
+        dense_hidden_ref[...],
+        branch_ref[:, :1],
+        lax.axis_index("c"),
+        down_ref,
+        dense_ref,
+        keep_ref.shape[1] // 128,
+    )
+
+
+def combine_kernel(weight_ref, back_ref, out_ref):
     rows, count = weight_ref.shape
-    blocks = out_ref.shape[0]
-    stat = mine_ref[...] + other_ref[...]
-    scale = lax.rsqrt(stat[:, :1] / (2 * blocks * 128) + RMS_EPSILON)
-    branch = jax.nn.sigmoid(scale * stat[:, 64:65])
     row = lax.broadcasted_iota(jnp.int32, (rows, count), 0)
     place = lax.broadcasted_iota(jnp.int32, (rows, count), 1)
     dense = (row == lax.axis_index("x")) & (place % 3 == 2)
-    weight = jnp.where(dense, branch, weight_ref[...])
+    weight = jnp.where(dense, 1.0, weight_ref[...])
     high = weight.astype(BF)
     low = (weight - high.astype(F32)).astype(BF)
     back = back_ref[...]
     total = jnp.dot(high, back, preferred_element_type=F32) + jnp.dot(
         low, back, preferred_element_type=F32
     )
-    for k in range(blocks):
+    for k in range(out_ref.shape[0]):
         out_ref[k] = total[:, 128 * k : 128 * k + 128]
 
 
@@ -297,15 +319,16 @@
     hbm = pl.BlockSpec(memory_space=pltpu.HBM)
     shaped = jax.ShapeDtypeStruct
 
-    half = -(-dense_gate.shape[1] // 2 // 16) * 16
+    half = dense_gate.shape[1] // 2
+    packed = -(-3 * half // 8) * 8
     sent = call(
         regroup_kernel,
-        shaped((x_count, 2, 3 * half, 128), BF),
+        shaped((x_count, 2, packed, 128), BF),
         (dense_gate.T, dense_up.T, dense_down),
         1_000_000,
         scratch=(
             pltpu.VMEM((3, *dense_down.shape), BF),
-            pltpu.VMEM((2, 3 * half, 128), BF),
+            pltpu.VMEM((2, packed, 128), BF),
             pltpu.SemaphoreType.DMA((x_count + 3,)),
         ),
         specs=[hbm, hbm, hbm],
@@ -313,7 +336,7 @@
         vmem=FULL,
     )
     dense_parts = lax.all_to_all(
-        sent.reshape(tp_count, 3 * half, 128), TP, 0, 0, tiled=True
+        sent.reshape(tp_count, packed, 128), TP, 0, 0, tiled=True
     )
 
     lane = jnp.arange(key_size, dtype=jnp.int32)
@@ -356,19 +379,6 @@
         out_specs=(vmem, vmem, hbm),
         vmem=FULL,
     )
-    sent = call(
-        pair_kernel,
-        shaped((x_count, own_blocks, rows, 128), BF),
-        (keep, swap(give)),
-        1_000_000,
-        scratch=(
-            pltpu.VMEM((own_blocks, rows, 128), BF),
-            pltpu.SemaphoreType.DMA((x_count,)),
-        ),
-        out_specs=hbm,
-    )
-    pairs = lax.all_to_all(sent, "x", 0, 0, tiled=True)
-
     route_count = route_ids.shape[1]
     route_flat = route_ids.reshape(-1)
     same = (route_flat[:, None] == route_flat[None, :]).astype(jnp.int32)
@@ -388,34 +398,56 @@
     )
     select = chosen.astype(F32)[:, None, :]
 
-    outgoing, own, stat = call(
+    sent = call(
+        pair_kernel,
+        shaped((x_count, own_blocks, rows, 128), BF),
+        (keep, swap(give)),
+        1_000_000,
+    )
+    sent, select, weighted = lax.optimization_barrier((sent, select, weighted))
+    pairs = lax.all_to_all(sent, "x", 0, 0, tiled=True)
+
+    outgoing, own = call(
         dispatch_kernel,
-        (
-            shaped((3 * ep_count * own_blocks, 128), BF),
-            shaped((rows, 128), F32),
-            shaped((rows, 128), F32),
-        ),
-        (pairs, tokens, norm2_gain.reshape(blocks, 128), branch_gate.reshape(blocks, 128), select),
+        (shaped((3 * ep_count * own_blocks, 128), BF), shaped((rows, 128), F32)),
+        (pairs, tokens, select),
         1_000_000_000,
         scratch=(pltpu.VMEM((own_blocks, rows, 128), F32),),
     )
     arrived = lax.all_to_all(outgoing.reshape(ep_count, 3 * own_blocks, 128), EP, 0, 0, tiled=True)
-    other_stat = swap(stat)
-    mine = arrived.reshape(3 * ep_count, width // 2)
+    count = 3 * ep_count
+    shape = (count, width // 2)
+    weights = (
+        norm2_gain.reshape(blocks, 128),
+        branch_gate.reshape(blocks, 128),
+        expert_gate[0].T,
+        expert_up[0].T,
+        dense_parts,
+    )
+    down = expert_down[0]
+    mine = arrived.reshape(shape)
     other = swap(mine)
-    shape = (3 * ep_count, width // 2)
-    stay, leave = call(
-        expert_kernel,
-        (shaped(shape, F32), shaped(shape, BF)),
+    partials = call(
+        first_kernel,
+        tuple(shaped((count, n), F32) for n in (down.shape[0], down.shape[0], 2 * half, 128, 128)),
+        (mine, *weights),
+        2_000_000_000,
+    )
+    leave, hidden, dense_hidden, branch = call(
+        second_kernel,
         (
-            mine,
-            other,
-            norm2_gain.reshape(blocks, 128),
-            expert_gate[0].T,
-            expert_up[0].T,
-            expert_down[0],
-            dense_parts,
-        ),
+            shaped(shape, BF),
+            shaped((count, down.shape[0]), BF),
+            shaped((count, half), BF),
+            shaped((count, 128), F32),
+        ),
+        (other, *weights, down, *partials),
+        2_000_000_000,
+    )
+    stay = call(
+        third_kernel,
+        shaped(shape, F32),
+        (hidden, dense_hidden, branch, down, dense_parts),
         2_000_000_000,
     )
     result = (stay + swap(leave).astype(F32)).astype(BF)
@@ -423,7 +455,7 @@
     total = call(
         combine_kernel,
         shaped((own_blocks, rows, 128), F32),
-        (weighted, stat, other_stat, returned.reshape(3 * ep_count, width // 2)),
+        (weighted, returned.reshape(shape)),
         100_000_000,
     )
     sums = lax.all_to_all(total, "x", 0, 0, tiled=True)

time: 131 us -> 130 us (level)
  the two profiles are of different devices: /device:TPU:1 before, /device:TPU:16 now
where the time goes in v4:
time: 130 us; the launch traced here: 129 us
  blocking collectives  48.7 us (37%)
  starting transfers between devices  34.8 us (27%)
  waiting for transfers between devices  29.4 us (23%)
  Pallas kernels  9.45 us (7%)
  local copies, waits for them, and re-layouts  3.3 us (3%)
  other arithmetic  2.07 us (2%)
    all_to_all x1, starting transfers between devices, local(): lax.all_to_all(outgoing.reshape(ep_count, 3 * own_blocks, 128), EP, 0, 0,...  23.3 us
    all_to_all x1, blocking collectives, local(): lax.all_to_all(result.reshape(ep_count, 3 * own_blocks, 128), EP, 0, 0, t...  22 us
    all_to_all x1, blocking collectives, local(): pairs = lax.all_to_all(sent, 'x', 0, 0, tiled=True)  16.3 us
    all_to_all x1, waiting for transfers between devices, local(): lax.all_to_all(outgoing.reshape(ep_count, 3 * own_blocks, 128), EP, 0, 0,...  14.3 us
    all_to_all x1, waiting for transfers between devices, local(): lax.all_to_all(sent.reshape(tp_count, packed, 128), TP, 0, 0, tiled=True)  14.1 us
    all_to_all x1, blocking collectives, local(): sums = lax.all_to_all(total, 'x', 0, 0, tiled=True)  10.4 us
    pallas_call x8, Pallas kernels, call(): pl.pallas_call(kernel, out_shape=out_shape, in_specs=specs or [full] * le...  9.45 us
    ppermute x3, starting transfers between devices, swap(): return lax.ppermute(x, 'c', [(0, 1), (1, 0)])  7.83 us
  transfers between devices with their start and end apart: 5, of which 3 were waited for; matrix products, arithmetic and copies ran while one was open for 1% of the time, Pallas kernels for 2%

profile of v4, /device:TPU:16, one launch (start us, length us, event | category | flops | bytes accessed | tf_op | source)
XLA Modules:
  0.0 128.7 jit_solution(8120243394370953780)
XLA Ops:
  0.8 0.6 copy-done.9
  1.4 0.7 fusion
  2.1 4.7 %shard_map.185 = (f32[8,8,128]{2,1,0:T(8,128)}, bf16[8,8,128]{2,1,0:T(8,128)(2,1)}, f32[8,128,256]{2,1,0:T(8,128)}) custom-call(bf16[8,2048]{1,0:T(8,128)(2,1)} %tokens_ref.3, f32[1,2048]{1,0:T(1,128)} %bitcast.37, f32[8,128]{1,0:T(8,128)} %get-tuple-element.43.cos_ref, f32[8,128]{1,0:T(8,128)} %get-tuple-element.42.sin_ref, f32[1]{0:T(128)} %bitcast.1.decay_ref, ...), custom_call_target="tpu_custom_call" | custom-call | flops 10000000000 | bytes 4243460 | tf_op jit(solution)/shard_map/pallas_call | solution.py:22
  6.9 1.9 %collective-permute-start = (bf16[8,8,128]{2,1,0:T(8,128)(2,1)}, bf16[8,8,128]{2,1,0:T(8,128)(2,1)S(1)}, u32[]{:S(2)}, u32[]{:S(2)}) collective-permute-start(bf16[8,8,128]{2,1,0:T(8,128)(2,1)} %get-tuple-element.20), channel_id=1, source_target_pairs={{0,1},{1,0},{2,3},{3,2},{4,5},{5,4},{6,7},{7,6},{8,9},{9,8},{10,11... | collective-permute-start | bytes 49160 | tf_op jit(solution)/shard_map/ppermute | solution.py:284
  8.8 0.7 copy-done.7
  9.7 0.2 select_reduce_fusion.1
  9.9 0.1 copy.35
  10.1 0.1 compare_reduce_fusion
  10.2 0.2 copy.36
  10.5 0.3 or_convert_fusion.select_ref
  10.7 0.4 copy-done.8
  11.3 16.3 %all_to_all.25.pairs_ref = bf16[8,8,8,128]{3,2,1,0:T(8,128)(2,1)S(1)} all-to-all(bf16[8,8,8,128]{3,2,1,0:T(8,128)(2,1)S(1)} %shard_map.186), channel_id=1, replica_groups=mesh['z'=8,'y'=8,'x'=8,'c'=2] {'x'}, dimensions={0} | all-to-all | bytes 262144 | tf_op jit(solution)/shard_map/all_to_all | solution.py:408
  27.5 1.0 shard_map.187
  28.5 23.3 %all-to-all-start.1 = ((bf16[64,24,128]{2,1,0:T(8,128)(2,1)}), bf16[64,24,128]{2,1,0:T(8,128)(2,1)S(1)}, u32[]{:S(2)}, u32[]{:S(2)}) async-start(bf16[64,24,128]{2,1,0:T(8,128)(2,1)} %bitcast.4), calls=%async_computation.1 | async-start | bytes 786432 | tf_op jit(solution)/shard_map/all_to_all | solution.py:417
  51.8 1.7 %shard_map.188 = bf16[8,2,136,128]{3,2,1,0:T(8,128)(2,1)} custom-call(bf16[88,128]{1,0:T(8,128)(2,1)} %bitcast.34, bf16[88,128]{1,0:T(8,128)(2,1)} %bitcast.35, bf16[88,128]{1,0:T(8,128)(2,1)} %down_hbm.1), custom_call_target="tpu_custom_call" | custom-call | flops 1000000 | bytes 67584 | tf_op jit(solution)/shard_map/pallas_call | solution.py:22
  53.5 14.3 %all-to-all-done.1 = bf16[64,24,128]{2,1,0:T(8,128)(2,1)S(1)} async-done(((bf16[64,24,128]{2,1,0:T(8,128)(2,1)}), bf16[64,24,128]{2,1,0:T(8,128)(2,1)S(1)}, u32[]{:S(2)}, u32[]{:S(2)}) %all-to-all-start.1) | async-done | bytes 393248 | tf_op jit(solution)/shard_map/all_to_all | solution.py:417
  67.9 3.7 %all-to-all-start.2 = ((bf16[16,136,128]{2,1,0:T(8,128)(2,1)}), bf16[16,136,128]{2,1,0:T(8,128)(2,1)S(1)}, u32[]{:S(2)}, u32[]{:S(2)}) async-start(bf16[16,136,128]{2,1,0:T(8,128)(2,1)} %bitcast.32), calls=%async_computation.2 | async-start | bytes 1114112 | tf_op jit(solution)/shard_map/all_to_all | solution.py:338
  71.6 0.2 reshape.208.x_ref
  71.8 2.2 %collective-permute-start.1 = (bf16[192,1024]{1,0:T(8,128)(2,1)S(1)}, bf16[192,1024]{1,0:T(8,128)(2,1)S(1)}, u32[]{:S(2)}, u32[]{:S(2)}) collective-permute-start(bf16[192,1024]{1,0:T(8,128)(2,1)S(1)} %reshape.208.x_ref), channel_id=1, source_target_pairs={{0,1},{1,0},{2,3},{3,2},{4,5},{5,4},{6,7},{7,6},{8,9},{9,8},{10,11... | collective-permute-start | bytes 1179656 | tf_op jit(solution)/shard_map/ppermute | solution.py:284
  74.0 14.1 %all-to-all-done.2.dense_ref = bf16[16,136,128]{2,1,0:T(8,128)(2,1)S(1)} async-done(((bf16[16,136,128]{2,1,0:T(8,128)(2,1)}), bf16[16,136,128]{2,1,0:T(8,128)(2,1)S(1)}, u32[]{:S(2)}, u32[]{:S(2)}) %all-to-all-start.2) | async-done | bytes 557088 | tf_op jit(solution)/shard_map/all_to_all | solution.py:338
  88.1 0.5 shard_map.189
  88.7 0.4 copy-done.3
  89.1 0.9 shard_map.190
  90.0 3.7 %collective-permute-start.2 = (bf16[192,1024]{1,0:T(8,128)(2,1)S(1)}, bf16[192,1024]{1,0:T(8,128)(2,1)S(1)}, u32[]{:S(2)}, u32[]{:S(2)}) collective-permute-start(bf16[192,1024]{1,0:T(8,128)(2,1)S(1)} %get-tuple-element.34), channel_id=1, source_target_pairs={{0,1},{1,0},{2,3},{3,2},{4,5},{5,4},{6,7},{7,6},{8,9},{9,8},{10,11... | collective-permute-start | bytes 1179656 | tf_op jit(solution)/shard_map/ppermute | solution.py:284
  93.8 0.4 shard_map.191
  94.1 1.0 collective-permute-done.2
  95.2 0.2 reshape.212
  95.3 22.0 %all_to_all.26 = bf16[64,24,128]{2,1,0:T(8,128)(2,1)S(1)} all-to-all(bf16[64,24,128]{2,1,0:T(8,128)(2,1)S(1)} %reshape.212), channel_id=1, replica_groups=mesh['z'=8,'y'=8,'x'=8,'c'=2] {'z','y'}, dimensions={0} | all-to-all | bytes 786432 | tf_op jit(solution)/shard_map/all_to_all | solution.py:454
  117.3 0.2 reshape.213.back_ref
  117.5 0.2 shard_map.192
  117.7 10.4 %all_to_all.27 = f32[8,8,128]{2,1,0:T(8,128)S(1)} all-to-all(f32[8,8,128]{2,1,0:T(8,128)S(1)} %shard_map.192), channel_id=1, replica_groups=mesh['z'=8,'y'=8,'x'=8,'c'=2] {'x'}, dimensions={0} | all-to-all | bytes 65536 | tf_op jit(solution)/shard_map/all_to_all | solution.py:461
  128.2 0.6 add_convert_fusion.1
  (33 shorter events, 0.6 us)
Async XLA Ops:
  0.7 0.7 copy-start.9
  6.9 4.4 %collective-permute-start = (bf16[8,8,128]{2,1,0:T(8,128)(2,1)}, bf16[8,8,128]{2,1,0:T(8,128)(2,1)S(1)}, u32[]{:S(2)}, u32[]{:S(2)}) collective-permute-start(bf16[8,8,128]{2,1,0:T(8,128)(2,1)} %get-tuple-element.20), channel_id=1, source_target_pairs={{0,1},{1,0},{2,3},{3,2},{4,5},{5,4},{6,7},{7,6},{8,9},{9,8},{10,11... | collective-permute-start | bytes 49160 | tf_op jit(solution)/shard_map/ppermute | solution.py:284
  8.8 0.7 copy-start.7
  10.4 0.7 copy-start.8
  10.5 0.8 copy-start
  11.2 16.3 %copy-start.4 = (bf16[8,2048]{1,0:T(8,128)(2,1)S(1)}, bf16[8,2048]{1,0:T(8,128)(2,1)}, u32[]{:S(2)}) copy-start(bf16[8,2048]{1,0:T(8,128)(2,1)} %tokens_ref.3) | copy-start | bytes 98308
  28.5 39.3 %all-to-all-start.1 = ((bf16[64,24,128]{2,1,0:T(8,128)(2,1)}), bf16[64,24,128]{2,1,0:T(8,128)(2,1)S(1)}, u32[]{:S(2)}, u32[]{:S(2)}) async-start(bf16[64,24,128]{2,1,0:T(8,128)(2,1)} %bitcast.4), calls=%async_computation.1 | async-start | bytes 786432 | tf_op jit(solution)/shard_map/all_to_all | solution.py:417
  67.9 20.2 %copy-start.2 = (bf16[1,2048,112]{1,2,0:T(8,128)(2,1)S(1)}, bf16[1,2048,112]{1,2,0:T(8,128)(2,1)}, u32[]{:S(2)}) copy-start(bf16[1,2048,112]{1,2,0:T(8,128)(2,1)} %param.31) | copy-start | bytes 1376260
  67.9 20.2 %all-to-all-start.2 = ((bf16[16,136,128]{2,1,0:T(8,128)(2,1)}), bf16[16,136,128]{2,1,0:T(8,128)(2,1)S(1)}, u32[]{:S(2)}, u32[]{:S(2)}) async-start(bf16[16,136,128]{2,1,0:T(8,128)(2,1)} %bitcast.32), calls=%async_computation.2 | async-start | bytes 1114112 | tf_op jit(solution)/shard_map/all_to_all | solution.py:338
  71.6 16.5 %copy-start.1 = (bf16[1,2048,112]{1,2,0:T(8,128)(2,1)S(1)}, bf16[1,2048,112]{1,2,0:T(8,128)(2,1)}, u32[]{:S(2)}) copy-start(bf16[1,2048,112]{1,2,0:T(8,128)(2,1)} %param.30) | copy-start | bytes 1376260
  71.6 16.5 %copy-start.5 = (f32[2048]{0:T(1024)S(1)}, f32[2048]{0:T(1024)}, u32[]{:S(2)}) copy-start(f32[2048]{0:T(1024)} %param.26) | copy-start | bytes 24580
  71.6 16.5 %copy-start.6 = (f32[2048]{0:T(1024)S(1)}, f32[2048]{0:T(1024)}, u32[]{:S(2)}) copy-start(f32[2048]{0:T(1024)} %param.27) | copy-start | bytes 24580
  71.8 16.9 %collective-permute-start.1 = (bf16[192,1024]{1,0:T(8,128)(2,1)S(1)}, bf16[192,1024]{1,0:T(8,128)(2,1)S(1)}, u32[]{:S(2)}, u32[]{:S(2)}) collective-permute-start(bf16[192,1024]{1,0:T(8,128)(2,1)S(1)} %reshape.208.x_ref), channel_id=1, source_target_pairs={{0,1},{1,0},{2,3},{3,2},{4,5},{5,4},{6,7},{7,6},{8,9},{9,8},{10,11... | collective-permute-start | bytes 1179656 | tf_op jit(solution)/shard_map/ppermute | solution.py:284
  88.1 1.0 copy-start.3
  90.0 5.1 %collective-permute-start.2 = (bf16[192,1024]{1,0:T(8,128)(2,1)S(1)}, bf16[192,1024]{1,0:T(8,128)(2,1)S(1)}, u32[]{:S(2)}, u32[]{:S(2)}) collective-permute-start(bf16[192,1024]{1,0:T(8,128)(2,1)S(1)} %get-tuple-element.34), channel_id=1, source_target_pairs={{0,1},{1,0},{2,3},{3,2},{4,5},{5,4},{6,7},{7,6},{8,9},{9,8},{10,11... | collective-permute-start | bytes 1179656 | tf_op jit(solution)/shard_map/ppermute | solution.py:284

commit v5 on v4

--- a/solution.py
+++ b/solution.py
@@ -13,7 +13,7 @@
 EP = ("z", "y")
 TP = ("x", "c")
 NT = (((1,), (1,)), ((), ()))
-FULL = 61 << 20
+FULL = 58 << 20
 
 
 def call(kernel, out_shape, args, flops, scratch=(), specs=None, out_specs=None, vmem=None):
@@ -30,23 +30,39 @@
     )(*args)
 
 
-def regroup_kernel(gate_hbm, up_hbm, down_hbm, sent_hbm, parts, packed, sems):
-    half = gate_hbm.shape[0] // 2
+def regroup_kernel(gate_hbm, up_hbm, down_hbm, sent_hbm, packed, sems):
+    size = gate_hbm.shape[0]
     count = sent_hbm.shape[0]
     copies = [
-        pltpu.make_async_copy(ref, parts.at[n], sems.at[count + n])
+        pltpu.make_async_copy(ref, packed.at[pl.ds(size * n, size)], sems.at[count + n])
         for n, ref in enumerate((gate_hbm, up_hbm, down_hbm))
     ]
     for c in copies:
         c.start()
-    spare = packed.shape[1] - 3 * half
-    for p in range(2):
-        packed[p, 3 * half :, :] = jnp.zeros((spare, packed.shape[2]), BF)
-    for n, c in enumerate(copies):
+    for c in copies:
         c.wait()
-        for p in range(2):
-            packed[p, half * n : half * n + half, :] = parts[n, half * p : half * p + half, :]
     copies = [pltpu.make_async_copy(packed, sent_hbm.at[n], sems.at[n]) for n in range(count)]
+    for c in copies:
+        c.start()
+    for c in copies:
+        c.wait()
+
+
+def trade_kernel(gate_hbm, up_hbm, down_hbm, out_ref, sems):
+    size, width = down_hbm.shape
+    blocks = width // 256
+    other = 1 - lax.axis_index("c")
+    copies = []
+    for n, ref in enumerate((gate_hbm, up_hbm)):
+        for k in range(blocks):
+            at = pl.ds(pl.multiple_of((2 * k + other) * 128, 128), 128)
+            copies.append((ref.at[:, at], (n, pl.ds(128 * k, 128))))
+    for n in range(2):
+        copies.append((down_hbm.at[:, pl.ds(n * width // 2, width // 2)], (2 + n, slice(None))))
+    copies = [
+        pltpu.make_async_copy(src, out_ref.at[pl.ds(size * n, size), lanes], sems.at[i])
+        for i, (src, (n, lanes)) in enumerate(copies)
+    ]
     for c in copies:
         c.start()
     for c in copies:
@@ -167,117 +183,113 @@
     return ref[pl.ds(2 * k + parity, 1), :]
 
 
-def project(x_ref, parity, gain_ref, bias_ref, gate_ref, up_ref, dense_ref):
+def first_kernel(
+    x_ref, gain_ref, bias_ref, gate_ref, up_ref, got_ref, dense_ref, keep_ref, give_ref, sums
+):
     count, half_width = x_ref.shape
+    third = count // 3
     blocks = half_width // 128
-    half = dense_ref.shape[1] // 3
-    half = half - half % 4
+    wide = gate_ref.shape[0]
+    size = dense_ref.shape[1] // 3
+    core = lax.axis_index("c")
     square = jnp.zeros((count, 128), F32)
-    along = jnp.zeros((count, 128), F32)
+    along = jnp.zeros((third, 128), F32)
     parts = []
     for k in range(blocks):
         x = x_ref[:, 128 * k : 128 * k + 128].astype(F32)
         square = square + x * x
-        x = x * gains(gain_ref, k, parity)
-        along = along + x * gains(bias_ref, k, parity)
+        x = x * gains(gain_ref, k, core)
+        along = along + x[2 * third :] * gains(bias_ref, k, core)
         parts.append(x.astype(BF))
     x = jnp.concatenate(parts, axis=1)
-    dense = jnp.concatenate(
-        [dense_ref[2 * k + parity, : 2 * half, :] for k in range(blocks)], axis=1
-    )
-    sums = [
-        lax.dot_general(x, w, NT, preferred_element_type=F32)
-        for w in (columns(gate_ref, parity, blocks), columns(up_ref, parity, blocks), dense)
-    ]
-    return (*sums, square, along)
-
-
-def first_kernel(
-    x_ref, gain_ref, bias_ref, gate_ref, up_ref, dense_ref, g_ref, u_ref, d_ref, s_ref, a_ref
-):
+
+    def apply(rows, w):
+        return lax.dot_general(rows, w, NT, preferred_element_type=F32)
+
+    rows = x[: 2 * third]
+    sums[:, :] = jnp.zeros(sums.shape, F32)
+    sums[:, 0:wide] = apply(rows, columns(gate_ref, core, blocks))
+    sums[:, 128 : 128 + wide] = apply(rows, got_ref[:wide, :])
+    sums[:, 256 : 256 + wide] = apply(rows, columns(up_ref, core, blocks))
+    sums[:, 384 : 384 + wide] = apply(rows, got_ref[wide : 2 * wide, :])
+    sums[:, 512:640] = jnp.broadcast_to(
+        jnp.sum(square[: 2 * third], axis=1, keepdims=True), (2 * third, 128)
+    )
+    own = pl.ds(pl.multiple_of(core * third, third), third)
+    other = pl.ds(pl.multiple_of((1 - core) * third, third), third)
+    keep_ref[:, :512] = sums[own, :512]
+    for p, q in enumerate((1, 0, 3, 2)):
+        give_ref[:, 128 * p : 128 * p + 128] = sums[other, 128 * q : 128 * q + 128]
+    rows = x[2 * third :]
+    lane = lax.broadcasted_iota(jnp.int32, (third, 128), 1)
+    both = jnp.where(
+        lane < 64,
+        jnp.sum(square[2 * third :], axis=1, keepdims=True),
+        jnp.sum(along, axis=1, keepdims=True),
+    )
+    for ref, at in ((keep_ref, own), (give_ref, other)):
+        ref[:, 768:896] = jnp.where(lane < 32, sums[at, 512:640], both)
+    for n in range(2):
+        w = jnp.concatenate(
+            [dense_ref[k, size * n : size * n + size, :] for k in range(blocks)], axis=1
+        )
+        part = jnp.concatenate(
+            [apply(rows, w), jnp.zeros((third, 128 - size), F32)], axis=1
+        )
+        keep_ref[:, 512 + 128 * n : 640 + 128 * n] = part
+        give_ref[:, 512 + 128 * n : 640 + 128 * n] = part
+
+
+def second_kernel(keep_ref, got_ref, down_ref, traded_ref, dense_ref, out_ref):
+    wide, width = down_ref.shape
+    blocks, size = dense_ref.shape[0], dense_ref.shape[1] // 3
+    stats = keep_ref[:, 768:896] + got_ref[:, 768:896]
+
+    def scale(value):
+        return lax.rsqrt(value / width + RMS_EPSILON)
+
+    def gated(at, to, count, factor):
+        v = (keep_ref[:, at : at + count] + got_ref[:, at : at + count]) * factor
+        w = (keep_ref[:, to : to + count] + got_ref[:, to : to + count]) * factor
+        return ((v / (1.0 + jnp.exp(-v))) * w).astype(BF)
+
+    factor = scale(stats[:, 0:1])
+    own = gated(0, 256, wide, factor)
+    other = gated(128, 384, wide, factor)
+    for n in range(2):
+        at = slice(n * width // 2, (n + 1) * width // 2)
+        r = jnp.dot(own, down_ref[:, at], preferred_element_type=F32)
+        r = r + jnp.dot(
+            other, traded_ref[(2 + n) * wide : (3 + n) * wide, :], preferred_element_type=F32
+        )
+        out_ref[:, at] = r.astype(BF)
+    factor = scale(stats[:, 32:33])
+    branch = jax.nn.sigmoid(stats[:, 64:65] * factor)
+    hidden = gated(512, 640, size, factor)
+    w = jnp.concatenate([dense_ref[k, 2 * size :, :] for k in range(blocks)], axis=1)
+    r = branch * jnp.dot(hidden, w, preferred_element_type=F32)
+    out_ref[:, width:] = r.astype(BF)
+
+
+def combine_kernel(weight_ref, back_ref, out_ref):
+    rows = weight_ref.shape[0]
+    blocks = out_ref.shape[0]
+    width = 128 * blocks
     core = lax.axis_index("c")
-    results = project(x_ref, core, gain_ref, bias_ref, gate_ref, up_ref, dense_ref)
-    for ref, value in zip((g_ref, u_ref, d_ref, s_ref, a_ref), results):
-        ref[...] = value
-
-
-def expand(hidden, dense_hidden, branch, parity, down_ref, dense_ref, blocks):
-    half = dense_hidden.shape[1]
-    down = jnp.concatenate(
-        [dense_ref[2 * k + parity, 2 * half : 3 * half, :] for k in range(blocks)], axis=1
-    )
-    r = jnp.dot(hidden, columns(down_ref, parity, blocks), preferred_element_type=F32)
-    return r + branch * jnp.dot(dense_hidden, down, preferred_element_type=F32)
-
-
-def second_kernel(
-    x_ref,
-    gain_ref,
-    bias_ref,
-    gate_ref,
-    up_ref,
-    dense_ref,
-    down_ref,
-    g_ref,
-    u_ref,
-    d_ref,
-    s_ref,
-    a_ref,
-    give_ref,
-    hidden_ref,
-    dense_hidden_ref,
-    branch_ref,
-):
-    count, half_width = x_ref.shape
-    other = 1 - lax.axis_index("c")
-    results = project(x_ref, other, gain_ref, bias_ref, gate_ref, up_ref, dense_ref)
-    gate, up, dense, square, along = [
-        ref[...] + value for ref, value in zip((g_ref, u_ref, d_ref, s_ref, a_ref), results)
-    ]
-    half = dense.shape[1] // 2
-    scale = lax.rsqrt(jnp.sum(square, axis=1, keepdims=True) / (2 * half_width) + RMS_EPSILON)
-    branch = jax.nn.sigmoid(jnp.sum(along, axis=1, keepdims=True) * scale)
-    is_dense = lax.broadcasted_iota(jnp.int32, (count, 1), 0) % 3 == 2
-
-    def gated(v, w):
-        v = v * scale
-        return (v / (1.0 + jnp.exp(-v))) * (w * scale)
-
-    hidden = jnp.where(is_dense, 0.0, gated(gate, up)).astype(BF)
-    dense_hidden = jnp.where(is_dense, gated(dense[:, :half], dense[:, half:]), 0.0).astype(BF)
-    r = expand(hidden, dense_hidden, branch, other, down_ref, dense_ref, half_width // 128)
-    give_ref[...] = r.astype(BF)
-    hidden_ref[...] = hidden
-    dense_hidden_ref[...] = dense_hidden
-    branch_ref[...] = jnp.broadcast_to(branch, branch_ref.shape)
-
-
-def third_kernel(hidden_ref, dense_hidden_ref, branch_ref, down_ref, dense_ref, keep_ref):
-    keep_ref[...] = expand(
-        hidden_ref[...],
-        dense_hidden_ref[...],
-        branch_ref[:, :1],
-        lax.axis_index("c"),
-        down_ref,
-        dense_ref,
-        keep_ref.shape[1] // 128,
-    )
-
-
-def combine_kernel(weight_ref, back_ref, out_ref):
-    rows, count = weight_ref.shape
-    row = lax.broadcasted_iota(jnp.int32, (rows, count), 0)
-    place = lax.broadcasted_iota(jnp.int32, (rows, count), 1)
-    dense = (row == lax.axis_index("x")) & (place % 3 == 2)
-    weight = jnp.where(dense, 1.0, weight_ref[...])
+    weight = weight_ref[...]
     high = weight.astype(BF)
     low = (weight - high.astype(F32)).astype(BF)
-    back = back_ref[...]
+    back = back_ref[:, :width]
     total = jnp.dot(high, back, preferred_element_type=F32) + jnp.dot(
         low, back, preferred_element_type=F32
     )
-    for k in range(out_ref.shape[0]):
-        out_ref[k] = total[:, 128 * k : 128 * k + 128]
+    for j in range(blocks):
+        out_ref[j] = total[:, 128 * j : 128 * j + 128]
+    here = lax.broadcasted_iota(jnp.int32, (rows, 128), 0) == lax.axis_index("x")
+    for k in range(blocks // 2):
+        dense = back_ref[:, width + 128 * k : width + 128 * k + 128].astype(F32)
+        dense = jnp.sum(dense, axis=0, keepdims=True)
+        out_ref[2 * k + core] = out_ref[2 * k + core] + jnp.where(here, dense, 0.0)
 
 
 def swap(x):
@@ -319,24 +331,33 @@
     hbm = pl.BlockSpec(memory_space=pltpu.HBM)
     shaped = jax.ShapeDtypeStruct
 
-    half = dense_gate.shape[1] // 2
-    packed = -(-3 * half // 8) * 8
+    size = dense_down.shape[0]
     sent = call(
         regroup_kernel,
-        shaped((x_count, 2, packed, 128), BF),
+        shaped((x_count, 3 * size, 128), BF),
         (dense_gate.T, dense_up.T, dense_down),
         1_000_000,
         scratch=(
-            pltpu.VMEM((3, *dense_down.shape), BF),
-            pltpu.VMEM((2, packed, 128), BF),
+            pltpu.VMEM((3 * size, 128), BF),
             pltpu.SemaphoreType.DMA((x_count + 3,)),
         ),
         specs=[hbm, hbm, hbm],
         out_specs=hbm,
         vmem=FULL,
     )
-    dense_parts = lax.all_to_all(
-        sent.reshape(tp_count, packed, 128), TP, 0, 0, tiled=True
+    dense_parts = lax.all_to_all(sent, "x", 0, 0, tiled=True)
+
+    gate_rows, up_rows, down = expert_gate[0].T, expert_up[0].T, expert_down[0]
+    traded = swap(
+        call(
+            trade_kernel,
+            shaped((4 * down.shape[0], width // 2), BF),
+            (gate_rows, up_rows, down),
+            1_000_000,
+            scratch=(pltpu.SemaphoreType.DMA((blocks + 2,)),),
+            specs=[hbm, hbm, hbm],
+            vmem=FULL,
+        )
     )
 
     lane = jnp.arange(key_size, dtype=jnp.int32)
@@ -388,8 +409,9 @@
     place_of = place_of.reshape(rows, route_count)
     in_row = jnp.arange(3 * ep_count, dtype=jnp.int32)
     row_kind = (in_row // 12) * 3 + in_row % 3
+    slot_kind = (jnp.arange(ep_count, dtype=jnp.int32) // 4) * 3 + lax.axis_index("c")
     weighted = jnp.sum(
-        jnp.where(place_of[:, :, None] == row_kind, route_weights[:, :, None], 0.0), axis=1
+        jnp.where(place_of[:, :, None] == slot_kind, route_weights[:, :, None], 0.0), axis=1
     )
     token = jnp.arange(own_blocks * rows, dtype=jnp.int32) % rows
     tiled = jnp.tile(place_of, (own_blocks, 1))
@@ -415,50 +437,38 @@
         scratch=(pltpu.VMEM((own_blocks, rows, 128), F32),),
     )
     arrived = lax.all_to_all(outgoing.reshape(ep_count, 3 * own_blocks, 128), EP, 0, 0, tiled=True)
-    count = 3 * ep_count
-    shape = (count, width // 2)
-    weights = (
-        norm2_gain.reshape(blocks, 128),
-        branch_gate.reshape(blocks, 128),
-        expert_gate[0].T,
-        expert_up[0].T,
-        dense_parts,
-    )
-    down = expert_down[0]
-    mine = arrived.reshape(shape)
-    other = swap(mine)
-    partials = call(
+    mine = arrived.reshape(ep_count, 3, own_blocks, 128).transpose(1, 0, 2, 3)
+    mine = mine.reshape(3 * ep_count, width // 2)
+    message = shaped((ep_count, 7 * 128), F32)
+    kept, given = call(
         first_kernel,
-        tuple(shaped((count, n), F32) for n in (down.shape[0], down.shape[0], 2 * half, 128, 128)),
-        (mine, *weights),
+        (message, message),
+        (
+            mine,
+            norm2_gain.reshape(blocks, 128),
+            branch_gate.reshape(blocks, 128),
+            gate_rows,
+            up_rows,
+            traded,
+            dense_parts,
+        ),
         2_000_000_000,
-    )
-    leave, hidden, dense_hidden, branch = call(
+        scratch=(pltpu.VMEM((2 * ep_count, 640), F32),),
+    )
+    result = call(
         second_kernel,
-        (
-            shaped(shape, BF),
-            shaped((count, down.shape[0]), BF),
-            shaped((count, half), BF),
-            shaped((count, 128), F32),
-        ),
-        (other, *weights, down, *partials),
+        shaped((ep_count, 3 * width // 2), BF),
+        (kept, swap(given), down, traded, dense_parts),
         2_000_000_000,
     )
-    stay = call(
-        third_kernel,
-        shaped(shape, F32),
-        (hidden, dense_hidden, branch, down, dense_parts),
-        2_000_000_000,
-    )
-    result = (stay + swap(leave).astype(F32)).astype(BF)
     returned = lax.all_to_all(result.reshape(ep_count, 3 * own_blocks, 128), EP, 0, 0, tiled=True)
     total = call(
         combine_kernel,
-        shaped((own_blocks, rows, 128), F32),
-        (weighted, returned.reshape(shape)),
+        shaped((blocks, rows, 128), F32),
+        (weighted, returned.reshape(ep_count, 3 * width // 2)),
         100_000_000,
     )
-    sums = lax.all_to_all(total, "x", 0, 0, tiled=True)
+    sums = lax.all_to_all(total, TP, 0, 0, tiled=True)
     layer_out = (own + jnp.sum(sums, axis=0)).astype(BF)
     return (layer_out, new_state.reshape(state.shape))
 

time: 130 us -> 129 us (level)
  the two profiles are of different devices: /device:TPU:16 before, /device:TPU:1 now
where the time goes in v5:
time: 129 us; the launch traced here: 128 us
  blocking collectives  47 us (36%)
  starting transfers between devices  46.7 us (36%)
  waiting for transfers between devices  17.7 us (14%)
  Pallas kernels  11.1 us (9%)
  local copies, waits for them, and re-layouts  2.59 us (2%)
  other arithmetic  2 us (2%)
    ppermute x3, starting transfers between devices, swap(): return lax.ppermute(x, 'c', [(0, 1), (1, 0)])  29.8 us
    all_to_all x1, blocking collectives, local(): lax.all_to_all(result.reshape(ep_count, 3 * own_blocks, 128), EP, 0, 0, t...  22.1 us
    all_to_all x1, starting transfers between devices, local(): lax.all_to_all(outgoing.reshape(ep_count, 3 * own_blocks, 128), EP, 0, 0,...  13.4 us
    all_to_all x1, blocking collectives, local(): sums = lax.all_to_all(total, TP, 0, 0, tiled=True)  13.1 us
    all_to_all x1, waiting for transfers between devices, local(): lax.all_to_all(outgoing.reshape(ep_count, 3 * own_blocks, 128), EP, 0, 0,...  12.3 us
    all_to_all x1, blocking collectives, local(): pairs = lax.all_to_all(sent, 'x', 0, 0, tiled=True)  11.9 us
    pallas_call x8, Pallas kernels, call(): pl.pallas_call(kernel, out_shape=out_shape, in_specs=specs or [full] * le...  11.1 us
    all_to_all x1, starting transfers between devices, local(): dense_parts = lax.all_to_all(sent, 'x', 0, 0, tiled=True)  3.54 us
  transfers between devices with their start and end apart: 5, of which 4 were waited for; matrix products, arithmetic and copies ran while one was open for 1% of the time, Pallas kernels for 3%

profile of v5, /device:TPU:1, one launch (start us, length us, event | category | flops | bytes accessed | tf_op | source)
XLA Modules:
  0.0 128.0 jit_solution(14442663964307227621)
XLA Ops:
  0.8 0.6 copy-done.9
  1.4 0.7 fusion
  2.1 4.7 %shard_map.185 = (f32[8,8,128]{2,1,0:T(8,128)}, bf16[8,8,128]{2,1,0:T(8,128)(2,1)}, f32[8,128,256]{2,1,0:T(8,128)}) custom-call(bf16[8,2048]{1,0:T(8,128)(2,1)} %tokens_ref.3, f32[1,2048]{1,0:T(1,128)} %bitcast.54, f32[8,128]{1,0:T(8,128)} %get-tuple-element.29.cos_ref, f32[8,128]{1,0:T(8,128)} %get-tuple-element.28.sin_ref, f32[1]{0:T(128)} %bitcast.1.decay_ref, ...), custom_call_target="tpu_custom_call" | custom-call | flops 10000000000 | bytes 4243460 | tf_op jit(solution)/shard_map/pallas_call | solution.py:22
  6.9 16.0 %collective-permute-start = (bf16[8,8,128]{2,1,0:T(8,128)(2,1)}, bf16[8,8,128]{2,1,0:T(8,128)(2,1)S(1)}, u32[]{:S(2)}, u32[]{:S(2)}) collective-permute-start(bf16[8,8,128]{2,1,0:T(8,128)(2,1)} %get-tuple-element.13), channel_id=1, source_target_pairs={{0,1},{1,0},{2,3},{3,2},{4,5},{5,4},{6,7},{7,6},{8,9},{9,8},{10,11... | collective-permute-start | bytes 49160 | tf_op jit(solution)/shard_map/ppermute | solution.py:296
  23.0 0.7 copy-done.7
  23.6 0.1 copy.34
  23.7 0.1 eq.71
  23.8 0.2 select_reduce_fusion.1
  24.0 0.1 copy.36
  24.1 0.1 tile.8
  24.2 0.1 compare_reduce_fusion
  24.3 0.2 copy.37
  24.6 0.3 or_convert_fusion.select_ref
  24.9 0.4 copy-done.8
  25.4 11.9 %all_to_all.25.pairs_ref = bf16[8,8,8,128]{3,2,1,0:T(8,128)(2,1)S(1)} all-to-all(bf16[8,8,8,128]{3,2,1,0:T(8,128)(2,1)S(1)} %shard_map.186), channel_id=1, replica_groups=mesh['z'=8,'y'=8,'x'=8,'c'=2] {'x'}, dimensions={0} | all-to-all | bytes 262144 | tf_op jit(solution)/shard_map/all_to_all | solution.py:430
  37.2 1.0 shard_map.187
  38.2 13.4 %all-to-all-start.1 = ((bf16[64,24,128]{2,1,0:T(8,128)(2,1)}), bf16[64,24,128]{2,1,0:T(8,128)(2,1)S(1)}, u32[]{:S(2)}, u32[]{:S(2)}) async-start(bf16[64,24,128]{2,1,0:T(8,128)(2,1)} %bitcast.4), calls=%async_computation.1 | async-start | bytes 786432 | tf_op jit(solution)/shard_map/all_to_all | solution.py:439
  51.6 1.7 %shard_map.189 = bf16[8,264,128]{2,1,0:T(8,128)(2,1)} custom-call(bf16[88,128]{1,0:T(8,128)(2,1)} %bitcast.51, bf16[88,128]{1,0:T(8,128)(2,1)} %bitcast.52, bf16[88,128]{1,0:T(8,128)(2,1)} %down_hbm.1), custom_call_target="tpu_custom_call" | custom-call | flops 1000000 | bytes 67584 | tf_op jit(solution)/shard_map/pallas_call | solution.py:22
  53.3 12.3 %all-to-all-done.1 = bf16[64,24,128]{2,1,0:T(8,128)(2,1)S(1)} async-done(((bf16[64,24,128]{2,1,0:T(8,128)(2,1)}), bf16[64,24,128]{2,1,0:T(8,128)(2,1)S(1)}, u32[]{:S(2)}, u32[]{:S(2)}) %all-to-all-start.1) | async-done | bytes 393248 | tf_op jit(solution)/shard_map/all_to_all | solution.py:439
  65.7 3.5 %all-to-all-start.2 = ((bf16[8,264,128]{2,1,0:T(8,128)(2,1)}), bf16[8,264,128]{2,1,0:T(8,128)(2,1)S(1)}, u32[]{:S(2)}, u32[]{:S(2)}) async-start(bf16[8,264,128]{2,1,0:T(8,128)(2,1)} %shard_map.189), calls=%async_computation.2 | async-start | bytes 1081344 | tf_op jit(solution)/shard_map/all_to_all | solution.py:348
  69.2 2.4 %shard_map.188 = bf16[448,1024]{1,0:T(8,128)(2,1)} custom-call(bf16[112,2048]{1,0:T(8,128)(2,1)} %bitcast.36, bf16[112,2048]{1,0:T(8,128)(2,1)} %bitcast.38, bf16[112,2048]{1,0:T(8,128)(2,1)} %bitcast.40), custom_call_target="tpu_custom_call" | custom-call | flops 1000000 | bytes 1376256 | tf_op jit(solution)/shard_map/pallas_call | solution.py:22
  71.6 6.2 %collective-permute-start.1 = (bf16[448,1024]{1,0:T(8,128)(2,1)}, bf16[448,1024]{1,0:T(8,128)(2,1)S(1)}, u32[]{:S(2)}, u32[]{:S(2)}) collective-permute-start(bf16[448,1024]{1,0:T(8,128)(2,1)} %shard_map.188), channel_id=1, source_target_pairs={{0,1},{1,0},{2,3},{3,2},{4,5},{5,4},{6,7},{7,6},{8,9},{9,8},{10,11... | collective-permute-start | bytes 2752520 | tf_op jit(solution)/shard_map/ppermute | solution.py:296
  78.0 2.1 %collective-permute-done.1.got_ref.traded_ref = bf16[448,1024]{1,0:T(8,128)(2,1)S(1)} collective-permute-done((bf16[448,1024]{1,0:T(8,128)(2,1)}, bf16[448,1024]{1,0:T(8,128)(2,1)S(1)}, u32[]{:S(2)}, u32[]{:S(2)}) %collective-permute-start.1) | collective-permute-done | bytes 917536 | tf_op jit(solution)/shard_map/ppermute | solution.py:296
  80.1 2.1 %all-to-all-done.2.dense_ref = bf16[8,264,128]{2,1,0:T(8,128)(2,1)S(1)} async-done(((bf16[8,264,128]{2,1,0:T(8,128)(2,1)}), bf16[8,264,128]{2,1,0:T(8,128)(2,1)S(1)}, u32[]{:S(2)}, u32[]{:S(2)}) %all-to-all-start.2) | async-done | bytes 540704 | tf_op jit(solution)/shard_map/all_to_all | solution.py:348
  82.3 0.6 shard_map.190
  82.9 7.6 %collective-permute-start.2 = (f32[64,896]{1,0:T(8,128)S(1)}, f32[64,896]{1,0:T(8,128)S(1)}, u32[]{:S(2)}, u32[]{:S(2)}) collective-permute-start(f32[64,896]{1,0:T(8,128)S(1)} %get-tuple-element.20), channel_id=1, source_target_pairs={{0,1},{1,0},{2,3},{3,2},{4,5},{5,4},{6,7},{7,6},{8,9},{9,8},{10,11... | collective-permute-start | bytes 688136 | tf_op jit(solution)/shard_map/ppermute | solution.py:296
  90.5 1.1 collective-permute-done.2.got_ref
  91.6 0.4 shard_map.191
  92.0 22.1 %all_to_all.26 = bf16[64,24,128]{2,1,0:T(8,128)(2,1)S(1)} all-to-all(bf16[64,24,128]{2,1,0:T(8,128)(2,1)S(1)} %bitcast.48), channel_id=1, replica_groups=mesh['z'=8,'y'=8,'x'=8,'c'=2] {'z','y'}, dimensions={0} | all-to-all | bytes 786432 | tf_op jit(solution)/shard_map/all_to_all | solution.py:464
  114.2 0.2 shard_map.192
  114.4 13.1 %all_to_all.27 = f32[16,8,128]{2,1,0:T(8,128)S(1)} all-to-all(f32[16,8,128]{2,1,0:T(8,128)S(1)} %shard_map.192), channel_id=1, replica_groups=mesh['z'=8,'y'=8,'x'=8,'c'=2] {'x','c'}, dimensions={0} | all-to-all | bytes 131072 | tf_op jit(solution)/shard_map/all_to_all | solution.py:471
  127.5 0.6 add_convert_fusion
  (34 shorter events, 0.6 us)
Async XLA Ops:
  0.7 0.7 copy-start.9
  6.9 18.5 %collective-permute-start = (bf16[8,8,128]{2,1,0:T(8,128)(2,1)}, bf16[8,8,128]{2,1,0:T(8,128)(2,1)S(1)}, u32[]{:S(2)}, u32[]{:S(2)}) collective-permute-start(bf16[8,8,128]{2,1,0:T(8,128)(2,1)} %get-tuple-element.13), channel_id=1, source_target_pairs={{0,1},{1,0},{2,3},{3,2},{4,5},{5,4},{6,7},{7,6},{8,9},{9,8},{10,11... | collective-permute-start | bytes 49160 | tf_op jit(solution)/shard_map/ppermute | solution.py:296
  22.9 0.7 copy-start.7
  24.6 0.7 copy-start.8
  24.6 0.8 copy-start.3
  25.4 11.9 %copy-start.4 = (bf16[8,2048]{1,0:T(8,128)(2,1)S(1)}, bf16[8,2048]{1,0:T(8,128)(2,1)}, u32[]{:S(2)}) copy-start(bf16[8,2048]{1,0:T(8,128)(2,1)} %tokens_ref.3) | copy-start | bytes 98308
  38.2 27.4 %all-to-all-start.1 = ((bf16[64,24,128]{2,1,0:T(8,128)(2,1)}), bf16[64,24,128]{2,1,0:T(8,128)(2,1)S(1)}, u32[]{:S(2)}, u32[]{:S(2)}) async-start(bf16[64,24,128]{2,1,0:T(8,128)(2,1)} %bitcast.4), calls=%async_computation.1 | async-start | bytes 786432 | tf_op jit(solution)/shard_map/all_to_all | solution.py:439
  65.7 16.6 %all-to-all-start.2 = ((bf16[8,264,128]{2,1,0:T(8,128)(2,1)}), bf16[8,264,128]{2,1,0:T(8,128)(2,1)S(1)}, u32[]{:S(2)}, u32[]{:S(2)}) async-start(bf16[8,264,128]{2,1,0:T(8,128)(2,1)} %shard_map.189), calls=%async_computation.2 | async-start | bytes 1081344 | tf_op jit(solution)/shard_map/all_to_all | solution.py:348
  71.6 8.5 %collective-permute-start.1 = (bf16[448,1024]{1,0:T(8,128)(2,1)}, bf16[448,1024]{1,0:T(8,128)(2,1)S(1)}, u32[]{:S(2)}, u32[]{:S(2)}) collective-permute-start(bf16[448,1024]{1,0:T(8,128)(2,1)} %shard_map.188), channel_id=1, source_target_pairs={{0,1},{1,0},{2,3},{3,2},{4,5},{5,4},{6,7},{7,6},{8,9},{9,8},{10,11... | collective-permute-start | bytes 2752520 | tf_op jit(solution)/shard_map/ppermute | solution.py:296
  77.8 4.4 %copy-start.1 = (bf16[1,2048,112]{1,2,0:T(8,128)(2,1)S(1)}, bf16[1,2048,112]{1,2,0:T(8,128)(2,1)}, u32[]{:S(2)}) copy-start(bf16[1,2048,112]{1,2,0:T(8,128)(2,1)} %param.31) | copy-start | bytes 1376260
  77.9 4.3 %copy-start = (bf16[1,2048,112]{1,2,0:T(8,128)(2,1)S(1)}, bf16[1,2048,112]{1,2,0:T(8,128)(2,1)}, u32[]{:S(2)}) copy-start(bf16[1,2048,112]{1,2,0:T(8,128)(2,1)} %param.30) | copy-start | bytes 1376260
  77.9 4.3 %copy-start.5 = (f32[2048]{0:T(1024)S(1)}, f32[2048]{0:T(1024)}, u32[]{:S(2)}) copy-start(f32[2048]{0:T(1024)} %param.26) | copy-start | bytes 24580
  77.9 4.3 %copy-start.6 = (f32[2048]{0:T(1024)S(1)}, f32[2048]{0:T(1024)}, u32[]{:S(2)}) copy-start(f32[2048]{0:T(1024)} %param.27) | copy-start | bytes 24580
  82.3 9.3 %copy-start.2 = (bf16[1,112,2048]{2,1,0:T(8,128)(2,1)S(1)}, bf16[1,112,2048]{2,1,0:T(8,128)(2,1)}, u32[]{:S(2)}) copy-start(bf16[1,112,2048]{2,1,0:T(8,128)(2,1)} %param.32) | copy-start | bytes 1376260
  82.9 8.7 %collective-permute-start.2 = (f32[64,896]{1,0:T(8,128)S(1)}, f32[64,896]{1,0:T(8,128)S(1)}, u32[]{:S(2)}, u32[]{:S(2)}) collective-permute-start(f32[64,896]{1,0:T(8,128)S(1)} %get-tuple-element.20), channel_id=1, source_target_pairs={{0,1},{1,0},{2,3},{3,2},{4,5},{5,4},{6,7},{7,6},{8,9},{9,8},{10,11... | collective-permute-start | bytes 688136 | tf_op jit(solution)/shard_map/ppermute | solution.py:296

commit v6 on v5

--- a/solution.py
+++ b/solution.py
@@ -14,6 +14,7 @@
 TP = ("x", "c")
 NT = (((1,), (1,)), ((), ()))
 FULL = 58 << 20
+TRADE = 16 << 20
 
 
 def call(kernel, out_shape, args, flops, scratch=(), specs=None, out_specs=None, vmem=None):
@@ -184,8 +185,21 @@
 
 
 def first_kernel(
-    x_ref, gain_ref, bias_ref, gate_ref, up_ref, got_ref, dense_ref, keep_ref, give_ref, sums
+    x_ref,
+    gain_ref,
+    bias_ref,
+    gate_ref,
+    up_ref,
+    traded_hbm,
+    dense_ref,
+    keep_ref,
+    give_ref,
+    sums,
+    got_ref,
+    sem,
 ):
+    copy = pltpu.make_async_copy(traded_hbm.at[pl.ds(0, got_ref.shape[0])], got_ref, sem)
+    copy.start()
     count, half_width = x_ref.shape
     third = count // 3
     blocks = half_width // 128
@@ -209,8 +223,9 @@
     rows = x[: 2 * third]
     sums[:, :] = jnp.zeros(sums.shape, F32)
     sums[:, 0:wide] = apply(rows, columns(gate_ref, core, blocks))
+    sums[:, 256 : 256 + wide] = apply(rows, columns(up_ref, core, blocks))
+    copy.wait()
     sums[:, 128 : 128 + wide] = apply(rows, got_ref[:wide, :])
-    sums[:, 256 : 256 + wide] = apply(rows, columns(up_ref, core, blocks))
     sums[:, 384 : 384 + wide] = apply(rows, got_ref[wide : 2 * wide, :])
     sums[:, 512:640] = jnp.broadcast_to(
         jnp.sum(square[: 2 * third], axis=1, keepdims=True), (2 * third, 128)
@@ -240,8 +255,10 @@
         give_ref[:, 512 + 128 * n : 640 + 128 * n] = part
 
 
-def second_kernel(keep_ref, got_ref, down_ref, traded_ref, dense_ref, out_ref):
+def second_kernel(keep_ref, got_ref, down_ref, traded_hbm, dense_ref, out_ref, traded_ref, sem):
     wide, width = down_ref.shape
+    copy = pltpu.make_async_copy(traded_hbm.at[pl.ds(2 * wide, 2 * wide)], traded_ref, sem)
+    copy.start()
     blocks, size = dense_ref.shape[0], dense_ref.shape[1] // 3
     stats = keep_ref[:, 768:896] + got_ref[:, 768:896]
 
@@ -253,22 +270,23 @@
         w = (keep_ref[:, to : to + count] + got_ref[:, to : to + count]) * factor
         return ((v / (1.0 + jnp.exp(-v))) * w).astype(BF)
 
-    factor = scale(stats[:, 0:1])
-    own = gated(0, 256, wide, factor)
-    other = gated(128, 384, wide, factor)
-    for n in range(2):
-        at = slice(n * width // 2, (n + 1) * width // 2)
-        r = jnp.dot(own, down_ref[:, at], preferred_element_type=F32)
-        r = r + jnp.dot(
-            other, traded_ref[(2 + n) * wide : (3 + n) * wide, :], preferred_element_type=F32
-        )
-        out_ref[:, at] = r.astype(BF)
     factor = scale(stats[:, 32:33])
     branch = jax.nn.sigmoid(stats[:, 64:65] * factor)
     hidden = gated(512, 640, size, factor)
     w = jnp.concatenate([dense_ref[k, 2 * size :, :] for k in range(blocks)], axis=1)
     r = branch * jnp.dot(hidden, w, preferred_element_type=F32)
     out_ref[:, width:] = r.astype(BF)
+    factor = scale(stats[:, 0:1])
+    own = gated(0, 256, wide, factor)
+    other = gated(128, 384, wide, factor)
+    copy.wait()
+    for n in range(2):
+        at = slice(n * width // 2, (n + 1) * width // 2)
+        r = jnp.dot(own, down_ref[:, at], preferred_element_type=F32)
+        r = r + jnp.dot(
+            other, traded_ref[n * wide : (n + 1) * wide, :], preferred_element_type=F32
+        )
+        out_ref[:, at] = r.astype(BF)
 
 
 def combine_kernel(weight_ref, back_ref, out_ref):
@@ -356,7 +374,7 @@
             1_000_000,
             scratch=(pltpu.SemaphoreType.DMA((blocks + 2,)),),
             specs=[hbm, hbm, hbm],
-            vmem=FULL,
+            vmem=TRADE,
         )
     )
 
@@ -426,7 +444,6 @@
         (keep, swap(give)),
         1_000_000,
     )
-    sent, select, weighted = lax.optimization_barrier((sent, select, weighted))
     pairs = lax.all_to_all(sent, "x", 0, 0, tiled=True)
 
     outgoing, own = call(
@@ -453,13 +470,23 @@
             dense_parts,
         ),
         2_000_000_000,
-        scratch=(pltpu.VMEM((2 * ep_count, 640), F32),),
+        scratch=(
+            pltpu.VMEM((2 * ep_count, 640), F32),
+            pltpu.VMEM((2 * down.shape[0], width // 2), BF),
+            pltpu.SemaphoreType.DMA,
+        ),
+        specs=[vmem] * 5 + [hbm, vmem],
     )
     result = call(
         second_kernel,
         shaped((ep_count, 3 * width // 2), BF),
         (kept, swap(given), down, traded, dense_parts),
         2_000_000_000,
+        scratch=(
+            pltpu.VMEM((2 * down.shape[0], width // 2), BF),
+            pltpu.SemaphoreType.DMA,
+        ),
+        specs=[vmem] * 3 + [hbm, vmem],
     )
     returned = lax.all_to_all(result.reshape(ep_count, 3 * own_blocks, 128), EP, 0, 0, tiled=True)
     total = call(

time: 129 us -> 129 us (level)
  blocking collectives: 47 us -> 13.1 us
  waiting for transfers between devices: 17.7 us -> 40.1 us
  starting transfers between devices: 46.7 us -> 58.2 us
    all_to_all x2 -> x0, blocking collectives: 34 us -> none  [the longest x1 22.1 us: local(): lax.all_to_all(result.reshape(ep_count, 3 * own_blocks, 128), EP, 0, 0, t...]
    all_to_all x0 -> x2, waiting for transfers between devices: none -> 22.3 us  [the longest x1 14.5 us: local(): lax.all_to_all(result.reshape(ep_count, 3 * own_blocks, 128), EP, 0, 0, t...]
    all_to_all x0 -> x2, starting transfers between devices: none -> 9.92 us  [the longest x1 6.55 us: local(): lax.all_to_all(result.reshape(ep_count, 3 * own_blocks, 128), EP, 0, 0, t...]
    ppermute x3, starting transfers between devices: 29.8 us -> 31.5 us  [swap(): return lax.ppermute(x, 'c', [(0, 1), (1, 0)])]
  transfers between devices with their start and end apart: 5 -> 7, of which waited for: 4 -> 7; matrix products, arithmetic and copies ran while one was open for 1% -> 1% of each run, Pallas kernels for 3% -> 2%
where the time goes in v6:
time: 129 us; the launch traced here: 128 us
  starting transfers between devices  58.2 us (45%)
  waiting for transfers between devices  40.1 us (31%)
  blocking collectives  13.1 us (10%)
  Pallas kernels  10.6 us (8%)
  local copies, waits for them, and re-layouts  2.95 us (2%)
  other arithmetic  2 us (2%)
    ppermute x3, starting transfers between devices, swap(): return lax.ppermute(x, 'c', [(0, 1), (1, 0)])  31.5 us
    all_to_all x1, waiting for transfers between devices, local(): lax.all_to_all(result.reshape(ep_count, 3 * own_blocks, 128), EP, 0, 0, t...  14.5 us
    all_to_all x1, starting transfers between devices, local(): lax.all_to_all(outgoing.reshape(ep_count, 3 * own_blocks, 128), EP, 0, 0,...  13.3 us
    all_to_all x1, blocking collectives, local(): sums = lax.all_to_all(total, TP, 0, 0, tiled=True)  13.1 us
    all_to_all x1, waiting for transfers between devices, local(): lax.all_to_all(outgoing.reshape(ep_count, 3 * own_blocks, 128), EP, 0, 0,...  11.8 us
    pallas_call x8, Pallas kernels, call(): pl.pallas_call(kernel, out_shape=out_shape, in_specs=specs or [full] * le...  10.6 us
    all_to_all x1, waiting for transfers between devices, local(): pairs = lax.all_to_all(sent, 'x', 0, 0, tiled=True)  7.77 us
    all_to_all x1, starting transfers between devices, local(): lax.all_to_all(result.reshape(ep_count, 3 * own_blocks, 128), EP, 0, 0, t...  6.55 us
  transfers between devices with their start and end apart: 7, of which 7 were waited for; matrix products, arithmetic and copies ran while one was open for 1% of the time, Pallas kernels for 2%

profile of v6, /device:TPU:1, one launch (start us, length us, event | category | flops | bytes accessed | tf_op | source)
XLA Modules:
  0.0 128.0 jit_solution(6817866226481855746)
XLA Ops:
  0.8 0.6 copy-done.9
  1.4 0.7 fusion
  2.1 4.7 %shard_map.185 = (f32[8,8,128]{2,1,0:T(8,128)}, bf16[8,8,128]{2,1,0:T(8,128)(2,1)}, f32[8,128,256]{2,1,0:T(8,128)}) custom-call(bf16[8,2048]{1,0:T(8,128)(2,1)} %tokens_ref.3, f32[1,2048]{1,0:T(1,128)} %bitcast.53, f32[8,128]{1,0:T(8,128)} %get-tuple-element.25.cos_ref, f32[8,128]{1,0:T(8,128)} %get-tuple-element.24.sin_ref, f32[1]{0:T(128)} %bitcast.1.decay_ref, ...), custom_call_target="tpu_custom_call" | custom-call | flops 10000000000 | bytes 4243460 | tf_op jit(solution)/shard_map/pallas_call | solution.py:23
  6.9 16.0 %collective-permute-start = (bf16[8,8,128]{2,1,0:T(8,128)(2,1)}, bf16[8,8,128]{2,1,0:T(8,128)(2,1)S(1)}, u32[]{:S(2)}, u32[]{:S(2)}) collective-permute-start(bf16[8,8,128]{2,1,0:T(8,128)(2,1)} %get-tuple-element.10), channel_id=1, source_target_pairs={{0,1},{1,0},{2,3},{3,2},{4,5},{5,4},{6,7},{7,6},{8,9},{9,8},{10,11... | collective-permute-start | bytes 49160 | tf_op jit(solution)/shard_map/ppermute | solution.py:314
  23.1 0.2 select_reduce_fusion.1
  23.5 0.1 compare_reduce_fusion
  23.7 0.3 collective-permute-done.got_ref
  23.9 0.7 shard_map.186
  24.6 3.4 %all-to-all-start = ((bf16[8,8,8,128]{3,2,1,0:T(8,128)(2,1)}), bf16[8,8,8,128]{3,2,1,0:T(8,128)(2,1)S(1)}, u32[]{:S(2)}, u32[]{:S(2)}) async-start(bf16[8,8,8,128]{3,2,1,0:T(8,128)(2,1)} %shard_map.186), calls=%async_computation | async-start | bytes 262144 | tf_op jit(solution)/shard_map/all_to_all | solution.py:447
  28.0 0.2 copy.45
  28.2 0.3 or_convert_fusion.select_ref
  28.5 7.8 %all-to-all-done.pairs_ref = bf16[8,8,8,128]{3,2,1,0:T(8,128)(2,1)S(1)} async-done(((bf16[8,8,8,128]{3,2,1,0:T(8,128)(2,1)}), bf16[8,8,8,128]{3,2,1,0:T(8,128)(2,1)S(1)}, u32[]{:S(2)}, u32[]{:S(2)}) %all-to-all-start) | async-done | bytes 131104 | tf_op jit(solution)/shard_map/all_to_all | solution.py:447
  36.3 1.0 shard_map.187
  37.3 13.3 %all-to-all-start.1 = ((bf16[64,24,128]{2,1,0:T(8,128)(2,1)}), bf16[64,24,128]{2,1,0:T(8,128)(2,1)S(1)}, u32[]{:S(2)}, u32[]{:S(2)}) async-start(bf16[64,24,128]{2,1,0:T(8,128)(2,1)} %bitcast.4), calls=%async_computation.1 | async-start | bytes 786432 | tf_op jit(solution)/shard_map/all_to_all | solution.py:456
  50.6 1.7 %shard_map.189 = bf16[8,264,128]{2,1,0:T(8,128)(2,1)} custom-call(bf16[88,128]{1,0:T(8,128)(2,1)} %bitcast.50, bf16[88,128]{1,0:T(8,128)(2,1)} %bitcast.51, bf16[88,128]{1,0:T(8,128)(2,1)} %down_hbm.1), custom_call_target="tpu_custom_call" | custom-call | flops 1000000 | bytes 67584 | tf_op jit(solution)/shard_map/pallas_call | solution.py:23
  52.3 11.8 %all-to-all-done.1 = bf16[64,24,128]{2,1,0:T(8,128)(2,1)S(1)} async-done(((bf16[64,24,128]{2,1,0:T(8,128)(2,1)}), bf16[64,24,128]{2,1,0:T(8,128)(2,1)S(1)}, u32[]{:S(2)}, u32[]{:S(2)}) %all-to-all-start.1) | async-done | bytes 393248 | tf_op jit(solution)/shard_map/all_to_all | solution.py:456
  64.1 3.5 %all-to-all-start.2 = ((bf16[8,264,128]{2,1,0:T(8,128)(2,1)}), bf16[8,264,128]{2,1,0:T(8,128)(2,1)S(1)}, u32[]{:S(2)}, u32[]{:S(2)}) async-start(bf16[8,264,128]{2,1,0:T(8,128)(2,1)} %shard_map.189), calls=%async_computation.2 | async-start | bytes 1081344 | tf_op jit(solution)/shard_map/all_to_all | solution.py:366
  67.7 0.4 shard_map.188
  68.1 6.6 %collective-permute-start.1 = (bf16[448,1024]{1,0:T(8,128)(2,1)S(1)}, bf16[448,1024]{1,0:T(8,128)(2,1)S(1)}, u32[]{:S(2)}, u32[]{:S(2)}) collective-permute-start(bf16[448,1024]{1,0:T(8,128)(2,1)S(1)} %shard_map.188), channel_id=1, source_target_pairs={{0,1},{1,0},{2,3},{3,2},{4,5},{5,4},{6,7},{7,6},{8,9},{9,8},{10,11... | collective-permute-start | bytes 2752520 | tf_op jit(solution)/shard_map/ppermute | solution.py:314
  74.9 1.9 %collective-permute-done.1.traded_hbm = bf16[448,1024]{1,0:T(8,128)(2,1)S(1)} collective-permute-done((bf16[448,1024]{1,0:T(8,128)(2,1)S(1)}, bf16[448,1024]{1,0:T(8,128)(2,1)S(1)}, u32[]{:S(2)}, u32[]{:S(2)}) %collective-permute-start.1) | collective-permute-done | bytes 917536 | tf_op jit(solution)/shard_map/ppermute | solution.py:314
  76.8 2.7 %all-to-all-done.2.dense_ref = bf16[8,264,128]{2,1,0:T(8,128)(2,1)S(1)} async-done(((bf16[8,264,128]{2,1,0:T(8,128)(2,1)}), bf16[8,264,128]{2,1,0:T(8,128)(2,1)S(1)}, u32[]{:S(2)}, u32[]{:S(2)}) %all-to-all-start.2) | async-done | bytes 540704 | tf_op jit(solution)/shard_map/all_to_all | solution.py:366
  79.5 1.1 shard_map.190
  80.5 8.9 %collective-permute-start.2 = (f32[64,896]{1,0:T(8,128)S(1)}, f32[64,896]{1,0:T(8,128)S(1)}, u32[]{:S(2)}, u32[]{:S(2)}) collective-permute-start(f32[64,896]{1,0:T(8,128)S(1)} %get-tuple-element.14), channel_id=1, source_target_pairs={{0,1},{1,0},{2,3},{3,2},{4,5},{5,4},{6,7},{7,6},{8,9},{9,8},{10,11... | collective-permute-start | bytes 688136 | tf_op jit(solution)/shard_map/ppermute | solution.py:314
  89.4 1.1 collective-permute-done.2.got_ref
  90.5 0.8 shard_map.191
  91.4 0.8 copy.50
  92.2 6.5 %all-to-all-start.3 = ((bf16[64,24,128]{2,1,0:T(8,128)(2,1)}), bf16[64,24,128]{2,1,0:T(8,128)(2,1)S(1)}, u32[]{:S(2)}, u32[]{:S(2)}) async-start(bf16[64,24,128]{2,1,0:T(8,128)(2,1)} %bitcast.27), calls=%async_computation.3 | async-start | bytes 786432 | tf_op jit(solution)/shard_map/all_to_all | solution.py:491
  98.8 0.7 copy-done.8
  99.5 14.5 %all-to-all-done.3 = bf16[64,24,128]{2,1,0:T(8,128)(2,1)S(1)} async-done(((bf16[64,24,128]{2,1,0:T(8,128)(2,1)}), bf16[64,24,128]{2,1,0:T(8,128)(2,1)S(1)}, u32[]{:S(2)}, u32[]{:S(2)}) %all-to-all-start.3) | async-done | bytes 393248 | tf_op jit(solution)/shard_map/all_to_all | solution.py:491
  114.1 0.2 shard_map.192
  114.3 13.1 %all_to_all.25 = f32[16,8,128]{2,1,0:T(8,128)S(1)} all-to-all(f32[16,8,128]{2,1,0:T(8,128)S(1)} %shard_map.192), channel_id=1, replica_groups=mesh['z'=8,'y'=8,'x'=8,'c'=2] {'x','c'}, dimensions={0} | all-to-all | bytes 131072 | tf_op jit(solution)/shard_map/all_to_all | solution.py:498
  127.4 0.6 add_convert_fusion
  (36 shorter events, 0.8 us)
Async XLA Ops:
  0.7 0.7 copy-start.9
  6.9 16.1 %copy-start.7 = (s32[8,2]{0,1:T(2,128)S(1)}, s32[8,2]{0,1:T(2,128)}, u32[]{:S(2)}) copy-start(s32[8,2]{0,1:T(2,128)} %param.28) | copy-start | bytes 196
  6.9 17.1 %collective-permute-start = (bf16[8,8,128]{2,1,0:T(8,128)(2,1)}, bf16[8,8,128]{2,1,0:T(8,128)(2,1)S(1)}, u32[]{:S(2)}, u32[]{:S(2)}) collective-permute-start(bf16[8,8,128]{2,1,0:T(8,128)(2,1)} %get-tuple-element.10), channel_id=1, source_target_pairs={{0,1},{1,0},{2,3},{3,2},{4,5},{5,4},{6,7},{7,6},{8,9},{9,8},{10,11... | collective-permute-start | bytes 49160 | tf_op jit(solution)/shard_map/ppermute | solution.py:314
  23.1 0.8 copy-start.3
  24.6 11.7 %all-to-all-start = ((bf16[8,8,8,128]{3,2,1,0:T(8,128)(2,1)}), bf16[8,8,8,128]{3,2,1,0:T(8,128)(2,1)S(1)}, u32[]{:S(2)}, u32[]{:S(2)}) async-start(bf16[8,8,8,128]{3,2,1,0:T(8,128)(2,1)} %shard_map.186), calls=%async_computation | async-start | bytes 262144 | tf_op jit(solution)/shard_map/all_to_all | solution.py:447
  28.2 8.1 %copy-start.4 = (bf16[8,2048]{1,0:T(8,128)(2,1)S(1)}, bf16[8,2048]{1,0:T(8,128)(2,1)}, u32[]{:S(2)}) copy-start(bf16[8,2048]{1,0:T(8,128)(2,1)} %tokens_ref.3) | copy-start | bytes 98308
  37.3 26.9 %all-to-all-start.1 = ((bf16[64,24,128]{2,1,0:T(8,128)(2,1)}), bf16[64,24,128]{2,1,0:T(8,128)(2,1)S(1)}, u32[]{:S(2)}, u32[]{:S(2)}) async-start(bf16[64,24,128]{2,1,0:T(8,128)(2,1)} %bitcast.4), calls=%async_computation.1 | async-start | bytes 786432 | tf_op jit(solution)/shard_map/all_to_all | solution.py:456
  50.5 17.1 %copy-start.2 = (bf16[1,112,2048]{2,1,0:T(8,128)(2,1)S(1)}, bf16[1,112,2048]{2,1,0:T(8,128)(2,1)}, u32[]{:S(2)}) copy-start(bf16[1,112,2048]{2,1,0:T(8,128)(2,1)} %param.32) | copy-start | bytes 1376260
  52.3 15.4 %copy-start = (bf16[1,2048,112]{1,2,0:T(8,128)(2,1)S(1)}, bf16[1,2048,112]{1,2,0:T(8,128)(2,1)}, u32[]{:S(2)}) copy-start(bf16[1,2048,112]{1,2,0:T(8,128)(2,1)} %param.30) | copy-start | bytes 1376260
  52.3 15.4 %copy-start.1 = (bf16[1,2048,112]{1,2,0:T(8,128)(2,1)S(1)}, bf16[1,2048,112]{1,2,0:T(8,128)(2,1)}, u32[]{:S(2)}) copy-start(bf16[1,2048,112]{1,2,0:T(8,128)(2,1)} %param.31) | copy-start | bytes 1376260
  64.1 15.3 %all-to-all-start.2 = ((bf16[8,264,128]{2,1,0:T(8,128)(2,1)}), bf16[8,264,128]{2,1,0:T(8,128)(2,1)S(1)}, u32[]{:S(2)}, u32[]{:S(2)}) async-start(bf16[8,264,128]{2,1,0:T(8,128)(2,1)} %shard_map.189), calls=%async_computation.2 | async-start | bytes 1081344 | tf_op jit(solution)/shard_map/all_to_all | solution.py:366
  68.1 8.6 %collective-permute-start.1 = (bf16[448,1024]{1,0:T(8,128)(2,1)S(1)}, bf16[448,1024]{1,0:T(8,128)(2,1)S(1)}, u32[]{:S(2)}, u32[]{:S(2)}) collective-permute-start(bf16[448,1024]{1,0:T(8,128)(2,1)S(1)} %shard_map.188), channel_id=1, source_target_pairs={{0,1},{1,0},{2,3},{3,2},{4,5},{5,4},{6,7},{7,6},{8,9},{9,8},{10,11... | collective-permute-start | bytes 2752520 | tf_op jit(solution)/shard_map/ppermute | solution.py:314
  74.8 4.7 %copy-start.5 = (f32[2048]{0:T(1024)S(1)}, f32[2048]{0:T(1024)}, u32[]{:S(2)}) copy-start(f32[2048]{0:T(1024)} %param.26) | copy-start | bytes 24580
  74.8 4.7 %copy-start.6 = (f32[2048]{0:T(1024)S(1)}, f32[2048]{0:T(1024)}, u32[]{:S(2)}) copy-start(f32[2048]{0:T(1024)} %param.27) | copy-start | bytes 24580
  80.5 10.0 %collective-permute-start.2 = (f32[64,896]{1,0:T(8,128)S(1)}, f32[64,896]{1,0:T(8,128)S(1)}, u32[]{:S(2)}, u32[]{:S(2)}) collective-permute-start(f32[64,896]{1,0:T(8,128)S(1)} %get-tuple-element.14), channel_id=1, source_target_pairs={{0,1},{1,0},{2,3},{3,2},{4,5},{5,4},{6,7},{7,6},{8,9},{9,8},{10,11... | collective-permute-start | bytes 688136 | tf_op jit(solution)/shard_map/ppermute | solution.py:314
  92.2 21.9 %all-to-all-start.3 = ((bf16[64,24,128]{2,1,0:T(8,128)(2,1)}), bf16[64,24,128]{2,1,0:T(8,128)(2,1)S(1)}, u32[]{:S(2)}, u32[]{:S(2)}) async-start(bf16[64,24,128]{2,1,0:T(8,128)(2,1)} %bitcast.27), calls=%async_computation.3 | async-start | bytes 786432 | tf_op jit(solution)/shard_map/all_to_all | solution.py:491
  98.7 0.7 copy-start.8

commit v7 on v5

--- a/solution.py
+++ b/solution.py
@@ -14,6 +14,7 @@
 TP = ("x", "c")
 NT = (((1,), (1,)), ((), ()))
 FULL = 58 << 20
+TRADE = 16 << 20
 
 
 def call(kernel, out_shape, args, flops, scratch=(), specs=None, out_specs=None, vmem=None):
@@ -48,7 +49,7 @@
         c.wait()
 
 
-def trade_kernel(gate_hbm, up_hbm, down_hbm, out_ref, sems):
+def trade_kernel(gate_hbm, up_hbm, down_hbm, out_hbm, sems):
     size, width = down_hbm.shape
     blocks = width // 256
     other = 1 - lax.axis_index("c")
@@ -60,7 +61,7 @@
     for n in range(2):
         copies.append((down_hbm.at[:, pl.ds(n * width // 2, width // 2)], (2 + n, slice(None))))
     copies = [
-        pltpu.make_async_copy(src, out_ref.at[pl.ds(size * n, size), lanes], sems.at[i])
+        pltpu.make_async_copy(src, out_hbm.at[pl.ds(size * n, size), lanes], sems.at[i])
         for i, (src, (n, lanes)) in enumerate(copies)
     ]
     for c in copies:
@@ -149,8 +150,21 @@
         sent_ref[n] = pair
 
 
-def dispatch_kernel(pairs_ref, tokens_ref, select_ref, sent_ref, own_ref, held):
+def dispatch_kernel(
+    pairs_ref,
+    tokens_ref,
+    select_ref,
+    gain_ref,
+    bias_ref,
+    sent_ref,
+    own_ref,
+    gain_out,
+    bias_out,
+    held,
+):
     rows = tokens_ref.shape[0]
+    gain_out[...] = gain_ref[...]
+    bias_out[...] = bias_ref[...]
     blocks = pairs_ref.shape[1]
     core = lax.axis_index("c")
     mine = []
@@ -351,12 +365,13 @@
     traded = swap(
         call(
             trade_kernel,
-            shaped((4 * down.shape[0], width // 2), BF),
+            pltpu.HBM((4 * down.shape[0], width // 2), BF),
             (gate_rows, up_rows, down),
             1_000_000,
             scratch=(pltpu.SemaphoreType.DMA((blocks + 2,)),),
             specs=[hbm, hbm, hbm],
-            vmem=FULL,
+            out_specs=hbm,
+            vmem=TRADE,
         )
     )
 
@@ -426,13 +441,17 @@
         (keep, swap(give)),
         1_000_000,
     )
-    sent, select, weighted = lax.optimization_barrier((sent, select, weighted))
     pairs = lax.all_to_all(sent, "x", 0, 0, tiled=True)
 
-    outgoing, own = call(
+    outgoing, own, gain, bias = call(
         dispatch_kernel,
-        (shaped((3 * ep_count * own_blocks, 128), BF), shaped((rows, 128), F32)),
-        (pairs, tokens, select),
+        (
+            shaped((3 * ep_count * own_blocks, 128), BF),
+            shaped((rows, 128), F32),
+            shaped((blocks, 128), F32),
+            shaped((blocks, 128), F32),
+        ),
+        (pairs, tokens, select, norm2_gain.reshape(blocks, 128), branch_gate.reshape(blocks, 128)),
         1_000_000_000,
         scratch=(pltpu.VMEM((own_blocks, rows, 128), F32),),
     )
@@ -445,8 +464,8 @@
         (message, message),
         (
             mine,
-            norm2_gain.reshape(blocks, 128),
-            branch_gate.reshape(blocks, 128),
+            gain,
+            bias,
             gate_rows,
             up_rows,
             traded,

time: 129 us -> 128 us (level)
  blocking collectives: 47 us -> 13.1 us
  waiting for transfers between devices: 17.7 us -> 39.4 us
  starting transfers between devices: 46.7 us -> 58.2 us
    all_to_all x2 -> x0, blocking collectives: 34 us -> none  [the longest x1 22.1 us: local(): lax.all_to_all(result.reshape(ep_count, 3 * own_blocks, 128), EP, 0, 0, t...]
    all_to_all x0 -> x2, waiting for transfers between devices: none -> 22.3 us  [the longest x1 14.6 us: local(): lax.all_to_all(result.reshape(ep_count, 3 * own_blocks, 128), EP, 0, 0, t...]
    all_to_all x0 -> x2, starting transfers between devices: none -> 9.93 us  [the longest x1 6.56 us: local(): lax.all_to_all(result.reshape(ep_count, 3 * own_blocks, 128), EP, 0, 0, t...]
    ppermute x3, starting transfers between devices: 29.8 us -> 31.5 us  [swap(): return lax.ppermute(x, 'c', [(0, 1), (1, 0)])]
  transfers between devices with their start and end apart: 5 -> 7, of which waited for: 4 -> 7; matrix products, arithmetic and copies ran while one was open for 1% -> 1% of each run, Pallas kernels for 3% -> 2%
where the time goes in v7:
time: 128 us; the launch traced here: 127 us
  starting transfers between devices  58.2 us (45%)
  waiting for transfers between devices  39.4 us (31%)
  blocking collectives  13.1 us (10%)
  Pallas kernels  10.4 us (8%)
  local copies, waits for them, and re-layouts  2.95 us (2%)
  other arithmetic  2 us (2%)
    ppermute x3, starting transfers between devices, swap(): return lax.ppermute(x, 'c', [(0, 1), (1, 0)])  31.5 us
    all_to_all x1, waiting for transfers between devices, local(): lax.all_to_all(result.reshape(ep_count, 3 * own_blocks, 128), EP, 0, 0, t...  14.6 us
    all_to_all x1, starting transfers between devices, local(): lax.all_to_all(outgoing.reshape(ep_count, 3 * own_blocks, 128), EP, 0, 0,...  13.3 us
    all_to_all x1, blocking collectives, local(): sums = lax.all_to_all(total, TP, 0, 0, tiled=True)  13.1 us
    all_to_all x1, waiting for transfers between devices, local(): lax.all_to_all(outgoing.reshape(ep_count, 3 * own_blocks, 128), EP, 0, 0,...  11.8 us
    pallas_call x8, Pallas kernels, call(): pl.pallas_call(kernel, out_shape=out_shape, in_specs=specs or [full] * le...  10.4 us
    all_to_all x1, waiting for transfers between devices, local(): pairs = lax.all_to_all(sent, 'x', 0, 0, tiled=True)  7.75 us
    all_to_all x1, starting transfers between devices, local(): lax.all_to_all(result.reshape(ep_count, 3 * own_blocks, 128), EP, 0, 0, t...  6.56 us
  transfers between devices with their start and end apart: 7, of which 7 were waited for; matrix products, arithmetic and copies ran while one was open for 1% of the time, Pallas kernels for 2%

profile of v7, /device:TPU:1, one launch (start us, length us, event | category | flops | bytes accessed | tf_op | source)
XLA Modules:
  0.0 127.1 jit_solution(2334957899284002339)
XLA Ops:
  0.8 0.6 copy-done.9
  1.4 0.7 fusion
  2.1 4.7 %shard_map.185 = (f32[8,8,128]{2,1,0:T(8,128)}, bf16[8,8,128]{2,1,0:T(8,128)(2,1)}, f32[8,128,256]{2,1,0:T(8,128)}) custom-call(bf16[8,2048]{1,0:T(8,128)(2,1)} %tokens_ref.3, f32[1,2048]{1,0:T(1,128)} %bitcast.53, f32[8,128]{1,0:T(8,128)} %get-tuple-element.29.cos_ref, f32[8,128]{1,0:T(8,128)} %get-tuple-element.28.sin_ref, f32[1]{0:T(128)} %bitcast.1.decay_ref, ...), custom_call_target="tpu_custom_call" | custom-call | flops 10000000000 | bytes 4243460 | tf_op jit(solution)/shard_map/pallas_call | solution.py:23
  6.9 16.0 %collective-permute-start = (bf16[8,8,128]{2,1,0:T(8,128)(2,1)}, bf16[8,8,128]{2,1,0:T(8,128)(2,1)S(1)}, u32[]{:S(2)}, u32[]{:S(2)}) collective-permute-start(bf16[8,8,128]{2,1,0:T(8,128)(2,1)} %get-tuple-element.12), channel_id=1, source_target_pairs={{0,1},{1,0},{2,3},{3,2},{4,5},{5,4},{6,7},{7,6},{8,9},{9,8},{10,11... | collective-permute-start | bytes 49160 | tf_op jit(solution)/shard_map/ppermute | solution.py:310
  23.1 0.2 select_reduce_fusion.1
  23.5 0.1 compare_reduce_fusion
  23.7 0.3 collective-permute-done.got_ref
  23.9 0.7 shard_map.186
  24.6 3.4 %all-to-all-start = ((bf16[8,8,8,128]{3,2,1,0:T(8,128)(2,1)}), bf16[8,8,8,128]{3,2,1,0:T(8,128)(2,1)S(1)}, u32[]{:S(2)}, u32[]{:S(2)}) async-start(bf16[8,8,8,128]{3,2,1,0:T(8,128)(2,1)} %shard_map.186), calls=%async_computation | async-start | bytes 262144 | tf_op jit(solution)/shard_map/all_to_all | solution.py:444
  28.0 0.2 copy.45
  28.3 0.3 or_convert_fusion.select_ref
  28.5 7.7 %all-to-all-done.pairs_ref = bf16[8,8,8,128]{3,2,1,0:T(8,128)(2,1)S(1)} async-done(((bf16[8,8,8,128]{3,2,1,0:T(8,128)(2,1)}), bf16[8,8,8,128]{3,2,1,0:T(8,128)(2,1)S(1)}, u32[]{:S(2)}, u32[]{:S(2)}) %all-to-all-start) | async-done | bytes 131104 | tf_op jit(solution)/shard_map/all_to_all | solution.py:444
  36.3 1.0 shard_map.187
  37.3 13.3 %all-to-all-start.1 = ((bf16[64,24,128]{2,1,0:T(8,128)(2,1)}), bf16[64,24,128]{2,1,0:T(8,128)(2,1)S(1)}, u32[]{:S(2)}, u32[]{:S(2)}) async-start(bf16[64,24,128]{2,1,0:T(8,128)(2,1)} %bitcast.6), calls=%async_computation.1 | async-start | bytes 786432 | tf_op jit(solution)/shard_map/all_to_all | solution.py:458
  50.6 1.7 %shard_map.189 = bf16[8,264,128]{2,1,0:T(8,128)(2,1)} custom-call(bf16[88,128]{1,0:T(8,128)(2,1)} %bitcast.50, bf16[88,128]{1,0:T(8,128)(2,1)} %bitcast.51, bf16[88,128]{1,0:T(8,128)(2,1)} %down_hbm.1), custom_call_target="tpu_custom_call" | custom-call | flops 1000000 | bytes 67584 | tf_op jit(solution)/shard_map/pallas_call | solution.py:23
  52.3 11.8 %all-to-all-done.1 = bf16[64,24,128]{2,1,0:T(8,128)(2,1)S(1)} async-done(((bf16[64,24,128]{2,1,0:T(8,128)(2,1)}), bf16[64,24,128]{2,1,0:T(8,128)(2,1)S(1)}, u32[]{:S(2)}, u32[]{:S(2)}) %all-to-all-start.1) | async-done | bytes 393248 | tf_op jit(solution)/shard_map/all_to_all | solution.py:458
  64.2 3.5 %all-to-all-start.2 = ((bf16[8,264,128]{2,1,0:T(8,128)(2,1)}), bf16[8,264,128]{2,1,0:T(8,128)(2,1)S(1)}, u32[]{:S(2)}, u32[]{:S(2)}) async-start(bf16[8,264,128]{2,1,0:T(8,128)(2,1)} %shard_map.189), calls=%async_computation.2 | async-start | bytes 1081344 | tf_op jit(solution)/shard_map/all_to_all | solution.py:362
  67.7 1.1 shard_map.188
  68.8 6.6 %collective-permute-start.1 = (bf16[448,1024]{1,0:T(8,128)(2,1)}, bf16[448,1024]{1,0:T(8,128)(2,1)S(1)}, u32[]{:S(2)}, u32[]{:S(2)}) collective-permute-start(bf16[448,1024]{1,0:T(8,128)(2,1)} %shard_map.188), channel_id=1, source_target_pairs={{0,1},{1,0},{2,3},{3,2},{4,5},{5,4},{6,7},{7,6},{8,9},{9,8},{10,11... | collective-permute-start | bytes 2752520 | tf_op jit(solution)/shard_map/ppermute | solution.py:310
  75.6 2.1 %collective-permute-done.1.got_ref.traded_ref = bf16[448,1024]{1,0:T(8,128)(2,1)S(1)} collective-permute-done((bf16[448,1024]{1,0:T(8,128)(2,1)}, bf16[448,1024]{1,0:T(8,128)(2,1)S(1)}, u32[]{:S(2)}, u32[]{:S(2)}) %collective-permute-start.1) | collective-permute-done | bytes 917536 | tf_op jit(solution)/shard_map/ppermute | solution.py:310
  77.7 1.8 %all-to-all-done.2.dense_ref = bf16[8,264,128]{2,1,0:T(8,128)(2,1)S(1)} async-done(((bf16[8,264,128]{2,1,0:T(8,128)(2,1)}), bf16[8,264,128]{2,1,0:T(8,128)(2,1)S(1)}, u32[]{:S(2)}, u32[]{:S(2)}) %all-to-all-start.2) | async-done | bytes 540704 | tf_op jit(solution)/shard_map/all_to_all | solution.py:362
  79.5 0.6 shard_map.190
  80.1 8.9 %collective-permute-start.2 = (f32[64,896]{1,0:T(8,128)S(1)}, f32[64,896]{1,0:T(8,128)S(1)}, u32[]{:S(2)}, u32[]{:S(2)}) collective-permute-start(f32[64,896]{1,0:T(8,128)S(1)} %get-tuple-element.18), channel_id=1, source_target_pairs={{0,1},{1,0},{2,3},{3,2},{4,5},{5,4},{6,7},{7,6},{8,9},{9,8},{10,11... | collective-permute-start | bytes 688136 | tf_op jit(solution)/shard_map/ppermute | solution.py:310
  89.0 1.1 collective-permute-done.2.got_ref
  90.1 0.4 shard_map.191
  90.5 0.8 copy.50
  91.3 6.6 %all-to-all-start.3 = ((bf16[64,24,128]{2,1,0:T(8,128)(2,1)}), bf16[64,24,128]{2,1,0:T(8,128)(2,1)S(1)}, u32[]{:S(2)}, u32[]{:S(2)}) async-start(bf16[64,24,128]{2,1,0:T(8,128)(2,1)} %bitcast.27), calls=%async_computation.3 | async-start | bytes 786432 | tf_op jit(solution)/shard_map/all_to_all | solution.py:483
  97.9 0.7 copy-done.8
  98.6 14.6 %all-to-all-done.3 = bf16[64,24,128]{2,1,0:T(8,128)(2,1)S(1)} async-done(((bf16[64,24,128]{2,1,0:T(8,128)(2,1)}), bf16[64,24,128]{2,1,0:T(8,128)(2,1)S(1)}, u32[]{:S(2)}, u32[]{:S(2)}) %all-to-all-start.3) | async-done | bytes 393248 | tf_op jit(solution)/shard_map/all_to_all | solution.py:483
  113.2 0.2 shard_map.192
  113.4 13.1 %all_to_all.25 = f32[16,8,128]{2,1,0:T(8,128)S(1)} all-to-all(f32[16,8,128]{2,1,0:T(8,128)S(1)} %shard_map.192), channel_id=1, replica_groups=mesh['z'=8,'y'=8,'x'=8,'c'=2] {'x','c'}, dimensions={0} | all-to-all | bytes 131072 | tf_op jit(solution)/shard_map/all_to_all | solution.py:490
  126.5 0.6 add_convert_fusion
  (36 shorter events, 0.8 us)
Async XLA Ops:
  0.7 0.7 copy-start.9
  6.9 16.1 %copy-start.7 = (s32[8,2]{0,1:T(2,128)S(1)}, s32[8,2]{0,1:T(2,128)}, u32[]{:S(2)}) copy-start(s32[8,2]{0,1:T(2,128)} %param.28) | copy-start | bytes 196
  6.9 17.1 %collective-permute-start = (bf16[8,8,128]{2,1,0:T(8,128)(2,1)}, bf16[8,8,128]{2,1,0:T(8,128)(2,1)S(1)}, u32[]{:S(2)}, u32[]{:S(2)}) collective-permute-start(bf16[8,8,128]{2,1,0:T(8,128)(2,1)} %get-tuple-element.12), channel_id=1, source_target_pairs={{0,1},{1,0},{2,3},{3,2},{4,5},{5,4},{6,7},{7,6},{8,9},{9,8},{10,11... | collective-permute-start | bytes 49160 | tf_op jit(solution)/shard_map/ppermute | solution.py:310
  23.1 0.8 copy-start.3
  24.6 11.7 %all-to-all-start = ((bf16[8,8,8,128]{3,2,1,0:T(8,128)(2,1)}), bf16[8,8,8,128]{3,2,1,0:T(8,128)(2,1)S(1)}, u32[]{:S(2)}, u32[]{:S(2)}) async-start(bf16[8,8,8,128]{3,2,1,0:T(8,128)(2,1)} %shard_map.186), calls=%async_computation | async-start | bytes 262144 | tf_op jit(solution)/shard_map/all_to_all | solution.py:444
  28.2 8.1 %copy-start.4 = (bf16[8,2048]{1,0:T(8,128)(2,1)S(1)}, bf16[8,2048]{1,0:T(8,128)(2,1)}, u32[]{:S(2)}) copy-start(bf16[8,2048]{1,0:T(8,128)(2,1)} %tokens_ref.3) | copy-start | bytes 98308
  28.2 8.1 %copy-start.5 = (f32[2048]{0:T(1024)S(1)}, f32[2048]{0:T(1024)}, u32[]{:S(2)}) copy-start(f32[2048]{0:T(1024)} %param.26) | copy-start | bytes 24580
  28.2 8.0 %copy-start.6 = (f32[2048]{0:T(1024)S(1)}, f32[2048]{0:T(1024)}, u32[]{:S(2)}) copy-start(f32[2048]{0:T(1024)} %param.27) | copy-start | bytes 24580
  37.3 26.9 %all-to-all-start.1 = ((bf16[64,24,128]{2,1,0:T(8,128)(2,1)}), bf16[64,24,128]{2,1,0:T(8,128)(2,1)S(1)}, u32[]{:S(2)}, u32[]{:S(2)}) async-start(bf16[64,24,128]{2,1,0:T(8,128)(2,1)} %bitcast.6), calls=%async_computation.1 | async-start | bytes 786432 | tf_op jit(solution)/shard_map/all_to_all | solution.py:458
  50.6 17.1 %copy-start.2 = (bf16[1,112,2048]{2,1,0:T(8,128)(2,1)S(1)}, bf16[1,112,2048]{2,1,0:T(8,128)(2,1)}, u32[]{:S(2)}) copy-start(bf16[1,112,2048]{2,1,0:T(8,128)(2,1)} %param.32) | copy-start | bytes 1376260
  52.3 15.4 %copy-start = (bf16[1,2048,112]{1,2,0:T(8,128)(2,1)S(1)}, bf16[1,2048,112]{1,2,0:T(8,128)(2,1)}, u32[]{:S(2)}) copy-start(bf16[1,2048,112]{1,2,0:T(8,128)(2,1)} %param.30) | copy-start | bytes 1376260
  52.3 15.4 %copy-start.1 = (bf16[1,2048,112]{1,2,0:T(8,128)(2,1)S(1)}, bf16[1,2048,112]{1,2,0:T(8,128)(2,1)}, u32[]{:S(2)}) copy-start(bf16[1,2048,112]{1,2,0:T(8,128)(2,1)} %param.31) | copy-start | bytes 1376260
  64.2 15.3 %all-to-all-start.2 = ((bf16[8,264,128]{2,1,0:T(8,128)(2,1)}), bf16[8,264,128]{2,1,0:T(8,128)(2,1)S(1)}, u32[]{:S(2)}, u32[]{:S(2)}) async-start(bf16[8,264,128]{2,1,0:T(8,128)(2,1)} %shard_map.189), calls=%async_computation.2 | async-start | bytes 1081344 | tf_op jit(solution)/shard_map/all_to_all | solution.py:362
  68.8 8.9 %collective-permute-start.1 = (bf16[448,1024]{1,0:T(8,128)(2,1)}, bf16[448,1024]{1,0:T(8,128)(2,1)S(1)}, u32[]{:S(2)}, u32[]{:S(2)}) collective-permute-start(bf16[448,1024]{1,0:T(8,128)(2,1)} %shard_map.188), channel_id=1, source_target_pairs={{0,1},{1,0},{2,3},{3,2},{4,5},{5,4},{6,7},{7,6},{8,9},{9,8},{10,11... | collective-permute-start | bytes 2752520 | tf_op jit(solution)/shard_map/ppermute | solution.py:310
  80.1 10.0 %collective-permute-start.2 = (f32[64,896]{1,0:T(8,128)S(1)}, f32[64,896]{1,0:T(8,128)S(1)}, u32[]{:S(2)}, u32[]{:S(2)}) collective-permute-start(f32[64,896]{1,0:T(8,128)S(1)} %get-tuple-element.18), channel_id=1, source_target_pairs={{0,1},{1,0},{2,3},{3,2},{4,5},{5,4},{6,7},{7,6},{8,9},{9,8},{10,11... | collective-permute-start | bytes 688136 | tf_op jit(solution)/shard_map/ppermute | solution.py:310
  91.3 21.9 %all-to-all-start.3 = ((bf16[64,24,128]{2,1,0:T(8,128)(2,1)}), bf16[64,24,128]{2,1,0:T(8,128)(2,1)S(1)}, u32[]{:S(2)}, u32[]{:S(2)}) async-start(bf16[64,24,128]{2,1,0:T(8,128)(2,1)} %bitcast.27), calls=%async_computation.3 | async-start | bytes 786432 | tf_op jit(solution)/shard_map/all_to_all | solution.py:483
  97.8 0.7 copy-start.8
